TPU v7x, 32 devices: a whole 2x2x4 slice. The times are simulated.
32 devices in a mesh: sp: 16 (over z, y, x), tp: 2 (over core).
Axes of the slice: x: 2, y: 2, z: 4, core: 2. Of those that a mesh axis runs over, the one named last changes fastest.
Arguments:
- tokens: bfloat16 [4096, 2048], P('sp'), may hold values from -6 to 6
- input_norm_gain: float32 [2048], replicated, may hold values from 0.1 to 1.9
- mq_weight: bfloat16 [2048, 1024], P('sp', 'tp'), may hold values from -0.125 to 0.125
- mk_weight: bfloat16 [2048, 1024], P('sp', 'tp'), may hold values from -0.125 to 0.125
- mv_weight: bfloat16 [2048, 1024], P('sp', 'tp'), may hold values from -0.125 to 0.125
- mo_weight: bfloat16 [2048, 1024], P('sp', 'tp'), may hold values from -0.125 to 0.125
- gate_weight: bfloat16 [2048, 4, 8], P('sp', None, 'tp'), may hold values from -0.125 to 0.125
- gate_bias: float32 [4, 8], P(None, 'tp'), may hold values from -3 to 100
- decay_extra: float32 [2, 8, 4096], P(None, 'tp', 'sp'), may hold values from -1 to 0
- m_gain: float32 [1024], P('tp'), may hold values from 0.1 to 1.9
- aq_weight: bfloat16 [2048, 1024], P('sp', 'tp'), may hold values from -0.125 to 0.125
- ak_weight: bfloat16 [2048, 512], P('sp', 'tp'), may hold values from -8.838835 to 8.838835
- av_weight: bfloat16 [2048, 512], P('sp', 'tp'), may hold values from -0.125 to 0.125
- sink_logit: float32 [16], P('tp'), may hold values from 3 to 6
- out_m_weight: bfloat16 [1024, 2048], P('sp', 'tp'), may hold values from -0.1875 to 0.1875
- out_a_weight: bfloat16 [1024, 2048], P('sp', 'tp'), may hold values from -1.5 to 1.5
Outputs:
- mixed: bfloat16 [4096, 2048], P('sp', 'tp')
- log_total: float32 [16, 4096], P('tp', 'sp')
All inputs are finite; a program needn't handle non-finite values.
Results may differ from a plain program's by a relative error of at most 0.015.
The roundings to bfloat16 on the way count: a program that leaves them out, or rounds other values in their place, can miss the bound.
Values may be sent and summed in bfloat16 or wider, within the bound.
No kernel may reach another device: no remote copies, remote signals or barrier semaphores. Data moves between devices by JAX's collectives and lax.ppermute only.
A program may use at most 64 MiB of HBM per device.

v0:
```python
import jax
import jax.numpy as jnp
from jax import lax
from jax.sharding import PartitionSpec as P

M_DIM = 128
W_DIM = 64
WINDOW = 128
M_BLOCK = 64


EPS = 1e-06
FLOOR_LOG = -1e30
HIGHEST = lax.Precision.HIGHEST


def with_halo(x, sides, width):
    for axis, dim in sides:
        peers, length = (lax.axis_size(axis), x.shape[dim])
        up = [(i, (i + 1) % peers) for i in range(peers - 1)]
        down = [(j, i) for i, j in up]
        last = lax.slice_in_dim(x, length - width, length, axis=dim)
        first = lax.slice_in_dim(x, 0, width, axis=dim)
        before = lax.ppermute(last, axis, up)
        after = lax.ppermute(first, axis, down)
        x = jnp.concatenate([before, x, after], axis=dim)
    return x


def rms_rows(inputs, gain_vec):
    return inputs * lax.rsqrt(jnp.mean(inputs * inputs, axis=-1, keepdims=True) + EPS) * gain_vec


def stored(result):
    return lax.optimization_barrier(result.astype(jnp.bfloat16))


def flip_tokens(array_in):
    return jnp.flip(array_in, axis=1)


def block_pass(queries, key_vecs, value_vecs, in_gate, log_forget, start_state):
    head_count, length, head_width = queries.shape
    block_count = length // M_BLOCK

    def blocks(array_in):
        return jnp.moveaxis(
            array_in.reshape((head_count, block_count, M_BLOCK) + array_in.shape[2:]), 1, 0
        )

    lower_mask = jnp.tril(jnp.ones((M_BLOCK, M_BLOCK), dtype=bool))

    def advance(state_in, block_in):
        cell_mat, norm_vec, stab_max = state_in
        q_blk, k_blk, v_blk, i_blk, f_blk = block_in
        cum_log = jnp.cumsum(f_blk, axis=-1)
        seg_total = cum_log[:, -1]
        log_end = seg_total[:, None] - cum_log + i_blk
        max_next = jnp.maximum(seg_total + stab_max, jnp.max(log_end, axis=-1))
        w_end = jnp.exp(log_end - max_next[:, None])
        fade_old = jnp.exp(seg_total + stab_max - max_next)
        cell_next = fade_old[:, None, None] * cell_mat + jnp.einsum(
            "hsv,hsk->hvk", w_end[:, :, None] * v_blk, k_blk, precision=HIGHEST
        )
        norm_next = fade_old[:, None] * norm_vec + jnp.einsum(
            "hs,hsk->hk", w_end, k_blk, precision=HIGHEST
        )
        log_w = jnp.where(
            lower_mask, cum_log[:, :, None] - cum_log[:, None, :] + i_blk[:, None, :], -jnp.inf
        )
        log_inter = cum_log + stab_max[:, None]
        row_max = jnp.maximum(log_inter, jnp.max(log_w, axis=-1))
        w_intra = jnp.exp(log_w - row_max[:, :, None])
        w_inter = jnp.exp(log_inter - row_max)
        scores = jnp.einsum("htk,hsk->hts", q_blk, k_blk, precision=HIGHEST) * w_intra
        numerator = jnp.einsum("hts,hsv->htv", scores, v_blk, precision=HIGHEST) + w_inter[
            ..., None
        ] * jnp.einsum("hvk,htk->htv", cell_mat, q_blk, precision=HIGHEST)
        denominator = jnp.sum(scores, axis=-1) + w_inter * jnp.einsum(
            "hk,htk->ht", norm_vec, q_blk, precision=HIGHEST
        )
        result_rows = numerator / jnp.maximum(jnp.abs(denominator), jnp.exp(-row_max))[..., None]
        return ((cell_next, norm_next, max_next), result_rows)

    final_state, outputs = lax.scan(
        advance,
        start_state,
        tuple(
            (blocks(array_in) for array_in in (queries, key_vecs, value_vecs, in_gate, log_forget))
        ),
    )
    return (jnp.moveaxis(outputs, 0, 1).reshape(head_count, length, head_width), final_state)


def summarize(key_vecs, value_vecs, in_gate, log_forget):
    cum_log = jnp.cumsum(log_forget, axis=-1)
    seg_total = cum_log[:, -1]
    log_end = seg_total[:, None] - cum_log + in_gate
    peak_log = jnp.max(log_end, axis=-1)
    weights_end = jnp.exp(log_end - peak_log[:, None])
    cell_mat = jnp.einsum(
        "hsv,hsk->hvk", weights_end[:, :, None] * value_vecs, key_vecs, precision=HIGHEST
    )
    norm_vec = jnp.einsum("hs,hsk->hk", weights_end, key_vecs, precision=HIGHEST)
    return (seg_total, cell_mat, norm_vec, peak_log)


def merge_side(state_in, cell_mats, norm_vecs, logs, usable):
    cell_mat, norm_vec, peak_log = state_in
    masked = jnp.where(usable, logs, FLOOR_LOG)
    new_peak = jnp.maximum(peak_log, jnp.max(masked, axis=0))
    scales = jnp.where(usable, jnp.exp(masked - new_peak[None]), 0.0)
    cell_mat = jnp.einsum("jh,jhvk->hvk", scales, cell_mats, precision=HIGHEST)
    norm_vec = jnp.einsum("jh,jhk->hk", scales, norm_vecs, precision=HIGHEST)
    return (cell_mat, norm_vec, new_peak)


def gather_states(forward_sum, backward_sum):
    decay_all = (
        lax.all_gather(forward_sum[0][None], "sp", axis=0, tiled=True),
        lax.all_gather(backward_sum[0][None], "sp", axis=0, tiled=True),
    )
    own_index = lax.axis_index("sp")
    acc_fwd = jnp.cumsum(decay_all[0], axis=0)
    acc_bwd = jnp.cumsum(decay_all[1], axis=0)
    before_own = lax.dynamic_index_in_dim(acc_fwd - decay_all[0], own_index, 0, keepdims=False)
    after_own = lax.dynamic_index_in_dim(acc_bwd, own_index, 0, keepdims=False)
    lead_bwd = acc_bwd - decay_all[1]
    empty_side = (
        jnp.zeros_like(forward_sum[1]),
        jnp.zeros_like(forward_sum[2]),
        jnp.full_like(forward_sum[3], FLOOR_LOG),
    )
    state_in = empty_side + empty_side
    pieces = (
        lax.all_gather(forward_sum[1][None], "sp", axis=0, tiled=True),
        lax.all_gather(forward_sum[2][None], "sp", axis=0, tiled=True),
        lax.all_gather(forward_sum[3][None], "sp", axis=0, tiled=True),
        lax.all_gather(backward_sum[1][None], "sp", axis=0, tiled=True),
        lax.all_gather(backward_sum[2][None], "sp", axis=0, tiled=True),
        lax.all_gather(backward_sum[3][None], "sp", axis=0, tiled=True),
    )
    piece_count = pieces[0].shape[0]
    device_ids = jnp.arange(piece_count, dtype=jnp.int32)
    log_fwd = before_own[None] - acc_fwd + pieces[2]
    log_bwd = lead_bwd - after_own[None] + pieces[5]
    left_side = merge_side(
        state_in[:3], pieces[0], pieces[1], log_fwd, (device_ids < own_index)[:, None]
    )
    right_side = merge_side(
        state_in[3:], pieces[3], pieces[4], log_bwd, (device_ids > own_index)[:, None]
    )
    states = left_side + right_side
    return (states[:3], states[3:])


def window_attend(a_query, kv_pairs, sink_logit, first_row, total_rows):
    tok_rows = a_query.shape[0]
    block_len = WINDOW
    block_count = tok_rows // block_len
    kv_width = kv_pairs.shape[1] // 2
    kv_heads = kv_width // W_DIM
    q_heads = a_query.shape[1] // W_DIM
    groups = q_heads // kv_heads
    filled_margin = with_halo(kv_pairs, (("sp", 0),), WINDOW)
    windows = jnp.concatenate(
        [
            filled_margin[place_idx * block_len : place_idx * block_len + tok_rows].reshape(
                block_count, block_len, 2 * kv_width
            )
            for place_idx in range(3)
        ],
        axis=1,
    )
    key_block = windows[:, :, :kv_width].reshape(block_count, 3 * block_len, kv_heads, W_DIM)
    content_tile = windows[:, :, kv_width:].reshape(block_count, 3 * block_len, kv_heads, W_DIM)
    query_block = a_query.reshape(block_count, block_len, kv_heads, groups, W_DIM)
    scores = jnp.einsum(
        "nqgrd,nkgd->ngrqk", query_block, key_block, preferred_element_type=jnp.float32
    ) * W_DIM ** (-0.5)
    query_off = jnp.arange(block_len, dtype=jnp.int32)
    key_off = jnp.arange(3 * block_len, dtype=jnp.int32) - block_len
    in_window = jnp.abs(query_off[:, None] - key_off[None, :]) <= WINDOW
    key_place = (
        first_row + jnp.arange(block_count, dtype=jnp.int32)[:, None] * block_len + key_off[None, :]
    )
    inside = (key_place >= 0) & (key_place < total_rows)
    usable = in_window[None] & inside[:, None, :]
    scores = jnp.where(usable[:, None, None], scores, -jnp.inf)
    sink_col = sink_logit.reshape(kv_heads, groups)[None, :, :, None]
    peak_log = jnp.maximum(sink_col, jnp.max(scores, axis=-1))
    weights_exp = jnp.exp(scores - peak_log[..., None])
    weight_total_sum = jnp.exp(sink_col - peak_log) + jnp.sum(weights_exp, axis=-1)
    weighted = jnp.einsum(
        "ngrqk,nkgd->nqgrd",
        weights_exp.astype(jnp.bfloat16),
        content_tile,
        preferred_element_type=jnp.float32,
    )
    scale_back = jnp.transpose(weight_total_sum, (0, 3, 1, 2))[..., None]
    mixed_rows = (weighted / scale_back).astype(jnp.bfloat16).reshape(tok_rows, q_heads * W_DIM)
    log_total = jnp.transpose(peak_log + jnp.log(weight_total_sum), (1, 2, 0, 3)).reshape(
        q_heads, tok_rows
    )
    return (mixed_rows, log_total)


def on_device(
    tokens,
    input_norm_gain,
    mq_weight,
    mk_weight,
    mv_weight,
    mo_weight,
    gate_weight,
    gate_bias,
    decay_extra,
    m_gain,
    aq_weight,
    ak_weight,
    av_weight,
    sink_logit,
    out_m_weight,
    out_a_weight,
):
    tok_rows = tokens.shape[0]
    normed = rms_rows(tokens.astype(jnp.float32), input_norm_gain).astype(jnp.bfloat16)
    local_heads = gate_weight.shape[2]
    gate_cols = 4 * local_heads
    pieces = (
        lax.all_gather(mq_weight, "sp", axis=0, tiled=True),
        lax.all_gather(mk_weight, "sp", axis=0, tiled=True),
        lax.all_gather(mv_weight, "sp", axis=0, tiled=True),
        lax.all_gather(mo_weight, "sp", axis=0, tiled=True),
        lax.all_gather(gate_weight, "sp", axis=0, tiled=True),
        lax.all_gather(aq_weight, "sp", axis=0, tiled=True),
        lax.all_gather(ak_weight, "sp", axis=0, tiled=True),
        lax.all_gather(av_weight, "sp", axis=0, tiled=True),
    )
    piece_rows = pieces[0].shape[0]
    flat_gate = pieces[4].reshape(piece_rows, gate_cols)
    segments = (
        pieces[0],
        pieces[1],
        pieces[2],
        pieces[3],
        flat_gate,
        pieces[5],
        pieces[6],
        pieces[7],
    )
    projected = tuple(
        (jnp.dot(normed, segment, preferred_element_type=jnp.float32) for segment in segments)
    )
    m_query = stored(projected[0])
    m_key = stored(projected[1])
    m_value = stored(projected[2])
    m_out = stored(projected[3])
    gates = projected[4].reshape(tok_rows, 4, local_heads) + gate_bias[None]

    def heads_first(matrix):
        return jnp.transpose(
            matrix.astype(jnp.float32).reshape(tok_rows, local_heads, M_DIM), (1, 0, 2)
        )

    queries = heads_first(m_query)
    key_vecs = heads_first(m_key) * M_DIM ** (-0.5)
    value_vecs = heads_first(m_value)
    in_fwd = gates[:, 0, :].T
    forget_fwd = jax.nn.log_sigmoid(gates[:, 1, :].T) + decay_extra[0]
    in_bwd = flip_tokens(gates[:, 2, :].T)
    forget_bwd = flip_tokens(jax.nn.log_sigmoid(gates[:, 3, :].T) + decay_extra[1])
    queries_bwd = flip_tokens(queries)
    keys_bwd = flip_tokens(key_vecs)
    values_bwd = flip_tokens(value_vecs)
    forward_sum = summarize(key_vecs, value_vecs, in_fwd, forget_fwd)
    backward_sum = summarize(keys_bwd, values_bwd, in_bwd, forget_bwd)
    state_fwd, state_bwd = gather_states(forward_sum, backward_sum)
    hidden_fwd, forward_unused = block_pass(
        queries, key_vecs, value_vecs, in_fwd, forget_fwd, state_fwd
    )
    hidden_bwd, unused_bwd = block_pass(
        queries_bwd, keys_bwd, values_bwd, in_bwd, forget_bwd, state_bwd
    )
    cell_out = hidden_fwd + flip_tokens(hidden_bwd)
    gate_open = jax.nn.sigmoid(m_out.astype(jnp.float32)).reshape(tok_rows, local_heads, M_DIM)
    cell_rows = jnp.transpose(cell_out, (1, 0, 2)) * gate_open
    mixed_m = (
        rms_rows(cell_rows, m_gain.reshape(local_heads, M_DIM))
        .astype(jnp.bfloat16)
        .reshape(tok_rows, local_heads * M_DIM)
    )
    a_query = stored(projected[5])
    kv_pairs = jnp.concatenate([stored(projected[6]), stored(projected[7])], axis=1)
    first_row = lax.axis_index("sp") * tok_rows
    total_rows = tok_rows * lax.axis_size("sp")
    mixed_a, log_total = window_attend(a_query, kv_pairs, sink_logit, first_row, total_rows)
    full_m, full_a = (
        lax.all_gather(mixed_m, "tp", axis=1, tiled=True),
        lax.all_gather(mixed_a, "tp", axis=1, tiled=True),
    )
    pieces = (
        lax.all_gather(out_m_weight, "sp", axis=0, tiled=True),
        lax.all_gather(out_a_weight, "sp", axis=0, tiled=True),
    )
    running = jnp.dot(full_m, pieces[0], preferred_element_type=jnp.float32)
    mixed = running + jnp.dot(full_a, pieces[1], preferred_element_type=jnp.float32)
    return (mixed.astype(jnp.bfloat16), log_total)


def solution(mesh):
    in_specs = (
        P("sp", None),
        P(),
        P("sp", "tp"),
        P("sp", "tp"),
        P("sp", "tp"),
        P("sp", "tp"),
        P("sp", None, "tp"),
        P(None, "tp"),
        P(None, "tp", "sp"),
        P("tp"),
        P("sp", "tp"),
        P("sp", "tp"),
        P("sp", "tp"),
        P("tp"),
        P("sp", "tp"),
        P("sp", "tp"),
    )
    out_specs = (P("sp", "tp"), P("tp", "sp"))
    return jax.shard_map(
        on_device, mesh=mesh, in_specs=in_specs, out_specs=out_specs, check_vma=False
    )
```

profile of v0, /device:TPU:0, one launch (start us, length us, event | category | flops | bytes accessed | tf_op | source)
XLA Modules:
  0.0 723.0 jit_solution(17199120740236358637)
XLA Ops:
  7.2 0.7 all-gather.22.cloned.1.call-update
  8.0 0.7 all-gather.24.cloned.1.call-update
  8.7 0.7 all-gather.32.cloned.1.call-update
  11.2 0.7 all-gather.28.cloned.1.call-update
  12.0 43.3 %all_gather.60 = bf16[2048,4,4]{0,2,1:T(4,128)(2,1)S(1)} all-gather(bf16[128,4,4]{0,2,1:T(4,128)(2,1)} %param.26), channel_id=1, replica_groups=mesh['sp'=16,'tp'=2] {'sp'}, dimensions={0}, use_global_device_ids=true | all-gather | bytes 69632 | tf_op jit(solution)/shard_map/all_gather | solution.py:235
  55.3 1.5 fusion.73
  57.4 1.2 reduce-window.14
  59.4 14.5 %all-gather.22.cloned.1.call-done = bf16[2048,512]{1,0:T(8,128)(2,1)} async-done(((bf16[128,512]{1,0:T(8,128)(2,1)}), bf16[2048,512]{1,0:T(8,128)(2,1)}) %all-gather.22.cloned.1.call-update) | async-done | bytes 2097168 | tf_op jit(solution)/shard_map/all_gather | solution.py:233
  74.0 2.3 convolution_convert_fusion.4
  76.3 59.6 %all-gather.24.cloned.1.call-done = bf16[2048,512]{1,0:T(8,128)(2,1)} async-done(((bf16[128,512]{1,0:T(8,128)(2,1)}), bf16[2048,512]{1,0:T(8,128)(2,1)}) %all-gather.24.cloned.1.call-update) | async-done | bytes 2097168 | tf_op jit(solution)/shard_map/all_gather | solution.py:232
  135.9 2.3 convolution_convert_fusion.3
  138.4 1.9 fusion.94
  140.6 1.2 reduce-window.16
  143.5 1.9 fusion.92
  146.0 0.7 all-gather.38.cloned.1.call-update
  149.4 39.7 %all-reduce.4 = (f32[64]{0:T(128)S(1)}, f32[64]{0:T(128)S(1)}, f32[64]{0:T(128)S(1)}, f32[64]{0:T(128)S(1)}) all-reduce(f32[64]{0:T(128)S(1)} %dynamic-update-slice.3, f32[64]{0:T(128)S(1)} %dynamic-update-slice.2, f32[64]{0:T(128)S(1)} %dynamic-update-slice.1, f32[64]{0:T(128)S(1)} %dynamic-update-slice), channel_id=7, replica_groups=mesh['sp'=16,'tp'=2] {'sp'}, use_global_device_ids=true, to_apply=%add.3 | all-reduce | flops 256 | bytes 2048
  191.2 0.7 copy.150
  192.9 2.0 convolution_convert_fusion.6
  194.9 54.5 %all-gather.34.cloned.1.call-done = bf16[2048,256]{1,0:T(8,128)(2,1)} async-done(((bf16[128,256]{1,0:T(8,128)(2,1)}), bf16[2048,256]{1,0:T(8,128)(2,1)}) %all-gather.34.cloned.1.call-update) | async-done | bytes 1048592 | tf_op jit(solution)/shard_map/all_gather | solution.py:238
  249.5 2.0 convolution_convert_fusion.5
  251.5 3.4 collective-permute-start
  254.9 1.5 collective-permute-start.1
  256.4 2.4 collective-permute-done
  258.8 3.0 collective-permute-done.1
  262.2 0.9 copy.123
  263.1 48.2 %all-gather.36.cloned.1.call-done = bf16[2048,512]{1,0:T(8,128)(2,1)} async-done(((bf16[128,512]{1,0:T(8,128)(2,1)}), bf16[2048,512]{1,0:T(8,128)(2,1)}) %all-gather.36.cloned.1.call-update) | async-done | bytes 2097168 | tf_op jit(solution)/shard_map/all_gather | solution.py:236
  311.3 2.7 convolution_convert_fusion
  314.3 0.7 fusion.72
  315.0 0.7 fusion.70
  315.7 0.7 fusion.105
  316.6 0.9 fusion.86
  317.8 2.3 all_gather.78
  320.5 38.8 %all-gather.8 = f32[16,4,128]{2,1,0:T(4,128)S(1)} all-gather(f32[1,4,128]{2,1,0:T(4,128)S(1)} %bitcast.480), channel_id=5, replica_groups=mesh['sp'=16,'tp'=2] {'sp'}, dimensions={0}, use_global_device_ids=true | all-gather | bytes 34816 | tf_op jit(solution)/shard_map/all_gather | solution.py:137
  359.3 13.9 %all-gather.26.cloned.1.call-done = bf16[2048,512]{1,0:T(8,128)(2,1)} async-done(((bf16[128,512]{1,0:T(8,128)(2,1)}), bf16[2048,512]{1,0:T(8,128)(2,1)}) %all-gather.26.cloned.1.call-update) | async-done | bytes 2097168 | tf_op jit(solution)/shard_map/all_gather | solution.py:231
  373.2 2.7 convolution_convert_fusion.2
  375.9 0.9 copy_bitcast_fusion
  377.2 38.9 %all-gather.9 = f32[16,4,128]{2,1,0:T(4,128)S(1)} all-gather(f32[1,4,128]{2,1,0:T(4,128)S(1)} %bitcast.481), channel_id=9, replica_groups=mesh['sp'=16,'tp'=2] {'sp'}, dimensions={0}, use_global_device_ids=true | all-gather | bytes 34816 | tf_op jit(solution)/shard_map/all_gather | solution.py:140
  416.1 3.4 rev.24
  419.6 15.7 %all-gather.28.cloned.1.call-done = bf16[2048,512]{1,0:T(8,128)(2,1)} async-done(((bf16[128,512]{1,0:T(8,128)(2,1)}), bf16[2048,512]{1,0:T(8,128)(2,1)}) %all-gather.28.cloned.1.call-update) | async-done | bytes 2097168 | tf_op jit(solution)/shard_map/all_gather | solution.py:234
  435.3 3.4 convolution_convert_fusion.1
  439.0 73.5 %all-gather.40.cloned.1.call-done = f32[64,128,128]{2,1,0:T(8,128)} async-done(((f32[4,128,128]{2,1,0:T(8,128)}), f32[64,128,128]{2,1,0:T(8,128)}) %all-gather.40.cloned.1.call-update) | async-done | bytes 4194320 | tf_op jit(solution)/shard_map/all_gather | solution.py:136
  512.5 6.4 fusion.68
  518.9 0.8 broadcast.249.clone2.1
  519.8 17.3 %while.34 = (s32[]{:T(128)}, f32[4,128,128]{2,1,0:T(8,128)S(1)}, f32[4,128]{1,0:T(4,128)S(1)}, f32[4]{0:T(128)S(1)}, f32[4,4,64,128]{3,2,0,1:T(8,128)}, /*index=...) while((s32[]{:T(128)}, f32[4,128,128]{2,1,0:T(8,128)S(1)}, ...), condition=%wide.region_11.12_spmd.clone, body=%wide.region_6.11_spmd.clone.sunk | while | flops 152231936 | bytes 2495373 | solution.py:85
  521.8 1.3 fusion.218
  523.1 0.7 convolution_add_fusion.6
  526.1 1.3 fusion.218
  527.4 0.7 convolution_add_fusion.6
  530.5 1.3 fusion.218
  531.8 0.7 convolution_add_fusion.6
  534.8 1.3 fusion.218
  536.1 0.7 convolution_add_fusion.6
  537.1 52.6 %all-gather.42.cloned.1.call-done = f32[64,128,128]{2,1,0:T(8,128)} async-done(((f32[4,128,128]{2,1,0:T(8,128)}), f32[64,128,128]{2,1,0:T(8,128)}) %all-gather.42.cloned.1.call-update) | async-done | bytes 4194320 | tf_op jit(solution)/shard_map/all_gather | solution.py:139
  589.7 6.4 fusion.66
  596.2 15.0 %while.35 = (s32[]{:T(128)}, f32[4,128,128]{2,1,0:T(8,128)S(1)}, f32[4,128]{1,0:T(4,128)S(1)}, f32[4]{0:T(128)S(1)}, f32[4,4,64,128]{3,2,0,1:T(8,128)S(1)}, /*in...) while((s32[]{:T(128)}, f32[4,128,128]{2,1,0:T(8,128)S(1)}, ...), condition=%wide.region_22.23_spmd.clone, body=%wide.region_17.22_spmd.clone.sunk | while | flops 152231936 | bytes 2495373 | solution.py:85
  599.1 0.7 convolution_add_fusion.7
  602.8 0.7 convolution_add_fusion.7
  606.5 0.7 convolution_add_fusion.7
  610.2 0.7 convolution_add_fusion.7
  612.8 2.3 all_gather.73
  615.1 36.2 %all-gather.30.cloned.1.call-done = bf16[1024,1024]{1,0:T(8,128)(2,1)} async-done(((bf16[64,1024]{1,0:T(8,128)(2,1)}), bf16[1024,1024]{1,0:T(8,128)(2,1)}) %all-gather.30.cloned.1.call-update) | async-done | bytes 2097168 | tf_op jit(solution)/shard_map/all_gather | solution.py:303
  651.3 2.3 fusion.144
  653.6 59.7 %all-gather.38.cloned.1.call-done = bf16[1024,1024]{1,0:T(8,128)(2,1)} async-done(((bf16[64,1024]{1,0:T(8,128)(2,1)}), bf16[1024,1024]{1,0:T(8,128)(2,1)}) %all-gather.38.cloned.1.call-update) | async-done | bytes 2097168 | tf_op jit(solution)/shard_map/all_gather | solution.py:304
  713.3 3.1 fusion.79
  (288 shorter events, 36.0 us)
Async XLA Ops:
  7.2 49.6 %copy-start.4 = (bf16[256,2048]{1,0:T(8,128)(2,1)S(1)}, bf16[256,2048]{1,0:T(8,128)(2,1)}, u32[]{:S(2)}) copy-start(bf16[256,2048]{1,0:T(8,128)(2,1)} %param.20) | copy-start | bytes 3145732
  7.2 49.6 %copy-start.19 = (f32[2048]{0:T(1024)S(1)}, f32[2048]{0:T(1024)}, u32[]{:S(2)}) copy-start(f32[2048]{0:T(1024)} %param.21) | copy-start | bytes 24580
  7.2 49.6 %copy-start.22 = (f32[4,4]{1,0:T(4,128)S(1)}, f32[4,4]{1,0:T(4,128)}, u32[]{:S(2)}) copy-start(f32[4,4]{1,0:T(4,128)} %param.27) | copy-start | bytes 196
  7.2 66.8 %all-gather.22.cloned.1.call-start = ((), (), s32[]{:S(2)}) async-start(), calls=%async_computation | async-start | bytes 2228224 | tf_op jit(solution)/shard_map/all_gather | solution.py:233
  7.9 128.0 %all-gather.24.cloned.1.call-start = ((), (), s32[]{:S(2)}) async-start(), calls=%async_computation.1 | async-start | bytes 2228224 | tf_op jit(solution)/shard_map/all_gather | solution.py:232
  8.7 48.6 %copy-start.11 = (f32[2,4,256]{2,1,0:T(4,128)S(1)}, f32[2,4,256]{2,1,0:T(4,128)}, u32[]{:S(2)}) copy-start(f32[2,4,256]{2,1,0:T(4,128)} %param.28) | copy-start | bytes 24580
  8.7 184.2 %all-gather.32.cloned.1.call-start = ((), (), s32[]{:S(2)}) async-start(), calls=%async_computation.5 | async-start | bytes 1114112 | tf_op jit(solution)/shard_map/all_gather | solution.py:237
  9.4 240.0 %all-gather.34.cloned.1.call-start = ((), (), s32[]{:S(2)}) async-start(), calls=%async_computation.6 | async-start | bytes 1114112 | tf_op jit(solution)/shard_map/all_gather | solution.py:238
  10.0 301.3 %all-gather.36.cloned.1.call-start = ((), (), s32[]{:S(2)}) async-start(), calls=%async_computation.7 | async-start | bytes 2228224 | tf_op jit(solution)/shard_map/all_gather | solution.py:236
  10.6 362.6 %all-gather.26.cloned.1.call-start = ((), (), s32[]{:S(2)}) async-start(), calls=%async_computation.2 | async-start | bytes 2228224 | tf_op jit(solution)/shard_map/all_gather | solution.py:231
  11.2 424.1 %all-gather.28.cloned.1.call-start = ((), (), s32[]{:S(2)}) async-start(), calls=%async_computation.3 | async-start | bytes 2228224 | tf_op jit(solution)/shard_map/all_gather | solution.py:234
  11.9 500.6 %all-gather.40.cloned.1.call-start = ((), (), s32[]{:S(2)}) async-start(), calls=%async_computation.9 | async-start | bytes 4456448 | tf_op jit(solution)/shard_map/all_gather | solution.py:136
  56.8 192.6 %copy-start.15 = (f32[256]{0:T(256)}, f32[256]{0:T(256)S(1)}, u32[]{:S(2)}) copy-start(f32[256]{0:T(256)S(1)} %add_rsqrt_fusion.1) | copy-start | bytes 3076
  140.3 449.3 %all-gather.42.cloned.1.call-start = ((), (), s32[]{:S(2)}) async-start(), calls=%async_computation.10 | async-start | bytes 4456448 | tf_op jit(solution)/shard_map/all_gather | solution.py:139
  142.8 0.6 copy-start.7
  142.9 4.3 copy-start.18
  142.9 4.4 copy-start.23
  143.2 173.3 %copy-start = (f32[4,256,128]{2,1,0:T(8,128)}, f32[4,256,128]{2,1,0:T(8,128)S(1)}, u32[]{:S(2)}) copy-start(f32[4,256,128]{2,1,0:T(8,128)S(1)} %reverse.3) | copy-start | bytes 1572868
  145.4 505.9 %all-gather.30.cloned.1.call-start = ((), (), s32[]{:S(2)}) async-start(), calls=%async_computation.4 | async-start | bytes 2228224 | tf_op jit(solution)/shard_map/all_gather | solution.py:303
  146.0 567.3 %all-gather.38.cloned.1.call-start = ((), (), s32[]{:S(2)}) async-start(), calls=%async_computation.8 | async-start | bytes 2228224 | tf_op jit(solution)/shard_map/all_gather | solution.py:304
  251.5 7.3 %collective-permute-start = (bf16[128,512]{1,0:T(8,128)(2,1)S(1)}, bf16[128,512]{1,0:T(8,128)(2,1)S(1)}, u32[]{:S(2)}, u32[]{:S(2)}) collective-permute-start(bf16[128,512]{1,0:T(8,128)(2,1)S(1)} %get-tuple-element.297), channel_id=1, source_target_pairs={{0,2},{2,4},{4,6},{6,8},{8,10},{10,12},{12,14},{14,16},{16,18},{18... | collective-permute-start | bytes 393224 | tf_op jit(solution)/shard_map/ppermute | solution.py:24
  254.9 6.9 collective-permute-start.1
  261.9 49.4 %copy-start.16 = (f32[256]{0:T(256)S(1)}, f32[256]{0:T(256)}, u32[]{:S(2)}) copy-start(f32[256]{0:T(256)} %copy-done.15) | copy-start | bytes 3076
  261.9 49.4 %copy-start.20 = (f32[2048]{0:T(1024)S(1)}, f32[2048]{0:T(1024)}, u32[]{:S(2)}) copy-start(f32[2048]{0:T(1024)} %param.21) | copy-start | bytes 24580
  315.0 1.6 copy-start.6
  317.5 55.8 %copy-start.17 = (f32[256]{0:T(256)S(1)}, f32[256]{0:T(256)}, u32[]{:S(2)}) copy-start(f32[256]{0:T(256)} %copy-done.15) | copy-start | bytes 3076
  317.5 55.8 %copy-start.21 = (f32[2048]{0:T(1024)S(1)}, f32[2048]{0:T(1024)}, u32[]{:S(2)}) copy-start(f32[2048]{0:T(1024)} %param.21) | copy-start | bytes 24580
  359.3 17.5 %copy-start.1 = (f32[4,256,128]{2,1,0:T(8,128)S(1)}, f32[4,256,128]{2,1,0:T(8,128)}, u32[]{:S(2)}) copy-start(f32[4,256,128]{2,1,0:T(8,128)} %copy-done) | copy-start | bytes 1572868
  359.3 17.5 %copy-start.8 = (f32[4,256]{1,0:T(4,128)S(1)}, f32[4,256]{1,0:T(4,128)}, u32[]{:S(2)}) copy-start(f32[4,256]{1,0:T(4,128)} %copy-done.7) | copy-start | bytes 12292
  419.6 19.1 %copy-start.12 = (f32[16,4,1]{0,2,1:T(1,128)S(1)}, f32[16,4,1]{0,2,1:T(1,128)}, u32[]{:S(2)}) copy-start(f32[16,4,1]{0,2,1:T(1,128)} %copy.146) | copy-start | bytes 772
  419.6 19.3 %copy-start.13 = (f32[16,4,1]{0,2,1:T(1,128)S(1)}, f32[16,4,1]{0,2,1:T(1,128)}, u32[]{:S(2)}) copy-start(f32[16,4,1]{0,2,1:T(1,128)} %copy.155) | copy-start | bytes 772
  419.6 92.9 %copy-start.10 = (f32[16,4,1,1]{0,2,3,1:T(1,128)S(1)}, f32[16,4,1,1]{0,2,3,1:T(1,128)}, u32[]{:S(2)}) copy-start(f32[16,4,1,1]{0,2,3,1:T(1,128)} %copy.141) | copy-start | bytes 772
  519.8 69.9 %copy-start.9 = (f32[16,4,1,1]{0,2,3,1:T(1,128)S(1)}, f32[16,4,1,1]{0,2,3,1:T(1,128)}, u32[]{:S(2)}) copy-start(f32[16,4,1,1]{0,2,3,1:T(1,128)} %copy.150) | copy-start | bytes 772
  596.1 15.3 %copy-start.2 = (f32[4,4,64,128]{3,2,0,1:T(8,128)S(1)}, f32[4,4,64,128]{3,2,0,1:T(8,128)}, u32[]{:S(2)}) copy-start(f32[4,4,64,128]{3,2,0,1:T(8,128)} %get-tuple-element.116) | copy-start | bytes 1572868
  611.2 1.0 copy-start.5
  611.2 1.2 copy-start.14
  612.7 100.6 %copy-start.3 = (bf16[256,1024]{0,1:T(8,128)(2,1)S(1)}, bf16[256,1024]{0,1:T(8,128)(2,1)}, u32[]{:S(2)}) copy-start(bf16[256,1024]{0,1:T(8,128)(2,1)} %all_gather.78) | copy-start | bytes 1572868
Sparse Core Ops, SparseCore 0:
  10.8 63.1 all-gather.21
  76.7 59.1 all-gather.23
  138.7 54.1 all-gather.31
  195.5 53.9 all-gather.33
  252.1 59.1 all-gather.35
  313.9 59.2 all-gather.25
  376.0 59.2 all-gather.27
  438.1 74.3 all-gather.39
  515.3 74.3 all-gather.41
  592.3 58.9 all-gather.29
  654.1 59.1 all-gather.37
where the time goes:
time: 724 us; the launch traced here: 723 us
  waiting for transfers between devices  440 us (61%)
  blocking collectives  165 us (23%)
  matrix products  66.3 us (9%)
  local copies, waits for them, and re-layouts  15.5 us (2%)
  other arithmetic  15.4 us (2%)
  between operations  15.1 us (2%)
    all_gather x1, waiting for transfers between devices, gather_states(): lax.all_gather(forward_sum[1][None], 'sp', axis=0, tiled=True)  73.5 us
    all_gather x1, waiting for transfers between devices, on_device(): lax.all_gather(out_a_weight, 'sp', axis=0, tiled=True)  59.7 us
    all_gather x1, waiting for transfers between devices, on_device(): lax.all_gather(mk_weight, 'sp', axis=0, tiled=True)  59.6 us
    all_gather x1, waiting for transfers between devices, on_device(): lax.all_gather(av_weight, 'sp', axis=0, tiled=True)  54.5 us
    all_gather x1, waiting for transfers between devices, gather_states(): lax.all_gather(backward_sum[1][None], 'sp', axis=0, tiled=True)  52.6 us
    all_gather x1, waiting for transfers between devices, on_device(): lax.all_gather(aq_weight, 'sp', axis=0, tiled=True)  48.2 us
    all_gather x1, blocking collectives, on_device(): lax.all_gather(gate_weight, 'sp', axis=0, tiled=True)  43.3 us
    unnamed x1, blocking collectives  39.7 us
  transfers between devices with their start and end apart: 13, of which 13 were waited for; matrix products, arithmetic and copies ran while one was open for 13% of the time, Pallas kernels for 0%

commit v1 on v0

--- a/solution.py
+++ b/solution.py
@@ -1,6 +1,8 @@
 import jax
 import jax.numpy as jnp
 from jax import lax
+from jax.experimental import pallas as pl
+from jax.experimental.pallas import tpu as pltpu
 from jax.sharding import PartitionSpec as P
 
 M_DIM = 128
@@ -308,6 +310,521 @@
     return (mixed.astype(jnp.bfloat16), log_total)
 
 
+CHUNK = 256
+LANES = 128
+EMPTY = -1e30
+
+
+def split_plan(mesh, args):
+    sp, tp = mesh.shape["sp"], mesh.shape["tp"]
+    tok_rows, width = args[0].shape
+    rows = args[2].shape[0]
+    local_heads = args[6].shape[2]
+    group = local_heads * tp
+    if tp != 2 or sp != 2 * group or group % 4 or (group // 2) & (group // 2 - 1):
+        return None
+    plane = group // 2
+    ok = (
+        args[2].shape[1] == local_heads * M_DIM
+        and args[10].shape[1] == local_heads * LANES
+        and args[11].shape[1] == local_heads * W_DIM
+        and args[12].shape[1] == local_heads * W_DIM
+        and 2 * W_DIM == LANES
+        and M_DIM == LANES
+        and WINDOW == LANES
+        and tok_rows == CHUNK
+        and rows == LANES
+        and args[14].shape[0] * sp == group * M_DIM
+        and args[15].shape[0] * sp == group * LANES
+    )
+    if not ok:
+        return None
+    return dict(
+        sp=sp, tp=tp, tok=tok_rows, width=width, rows=rows, lh=local_heads, group=group, plane=plane
+    )
+
+
+def mm(a, b, ca=1, cb=0, precision=None):
+    return lax.dot_general(
+        a, b, (((ca,), (cb,)), ((), ())), precision=precision, preferred_element_type=jnp.float32
+    )
+
+
+def vmem_call(kernel, outs, scratch=(), smem=0, n_in=0, flops=0):
+    return pl.pallas_call(
+        kernel,
+        out_shape=outs,
+        in_specs=[pl.BlockSpec(memory_space=pltpu.SMEM)] * smem
+        + [pl.BlockSpec(memory_space=pltpu.VMEM)] * n_in,
+        out_specs=jax.tree.map(lambda _: pl.BlockSpec(memory_space=pltpu.VMEM), outs),
+        scratch_shapes=scratch,
+        cost_estimate=pl.CostEstimate(flops=flops, bytes_accessed=0, transcendentals=0),
+        compiler_params=pltpu.CompilerParams(vmem_limit_bytes=56 * 1024 * 1024),
+    )
+
+
+def pack_kernel(mq, mk, mv, mo, aq, ak, av, small, out):
+    halves, heads = out.shape[0], out.shape[1]
+    rows = mq.shape[0] // halves
+    for u in range(halves):
+        for h in range(heads):
+            for c, ref in enumerate((mq, mk, mv, mo, aq)):
+                out[u, h, c * rows : (c + 1) * rows, :] = ref[
+                    u * rows : (u + 1) * rows, h * LANES : (h + 1) * LANES
+                ]
+            pair = jnp.concatenate(
+                [
+                    ref[u * rows : (u + 1) * rows, h * W_DIM : (h + 1) * W_DIM]
+                    for ref in (ak, av)
+                ],
+                axis=1,
+            )
+            out[u, h, 5 * rows : 6 * rows, :] = pair
+            out[u, h, 6 * rows :, :] = small[u, h]
+
+
+def chunk_vecs(rows):
+    n = rows.shape[1]
+    r = lax.broadcasted_iota(jnp.int32, (n, n), 0)
+    c = lax.broadcasted_iota(jnp.int32, (n, n), 1)
+    lower = jnp.where(r >= c, 1.0, 0.0).astype(jnp.float32)
+    eye = jnp.where(r == c, 1.0, 0.0).astype(jnp.float32)
+    cum_col = mm(lower, rows, 1, 1, HIGHEST)
+    raw_col = mm(eye, rows, 1, 1, HIGHEST)
+    cum_row = mm(rows, lower, 1, 1, HIGHEST)
+    f_col, f_row = cum_col[:, 1:2], cum_row[1:2]
+    e_col = cum_col[:, 3:4] - raw_col[:, 3:4]
+    e_row = cum_row[3:4] - rows[3:4]
+    fwd = (f_col, rows[0:1] - f_row, raw_col[:, 0:1] - f_col, cum_row[1:2, n - 1 : n])
+    bwd = (-e_col, rows[2:3] + e_row, raw_col[:, 2:3] + e_col, cum_row[3:4, n - 1 : n])
+    return fwd, bwd
+
+
+def advance_state(state, key, value, end_col, end_row, total):
+    cell, norm, peak = state
+    new_peak = jnp.maximum(total + peak, jnp.max(end_row, axis=1, keepdims=True))
+    weighted = key * jnp.exp(end_col - new_peak)
+    fade = jnp.exp(total + peak - new_peak)
+    cell = fade * cell + mm(weighted, value, 0, 0, HIGHEST)
+    norm = fade * norm + jnp.sum(weighted, axis=0, keepdims=True)
+    return cell, norm, new_peak
+
+
+def forward_state(state, key, value, vecs):
+    return advance_state(state, key, value, vecs[2] + vecs[3], vecs[1] + vecs[3], vecs[3])
+
+
+def backward_state(state, key, value, vecs):
+    return advance_state(state, key, value, vecs[2], vecs[1], vecs[3])
+
+
+def empty_state():
+    return (
+        jnp.zeros((M_DIM, M_DIM), jnp.float32),
+        jnp.zeros((1, M_DIM), jnp.float32),
+        jnp.full((1, 1), EMPTY, jnp.float32),
+    )
+
+
+def project_kernel(meta, bias, *refs):
+    plan_plane = 4
+    xs = refs[:plan_plane]
+    own, partner, gate_t, decay, proj, gates, summary, halo, weight = refs[plan_plane:]
+    t, k, sel, jl = meta[0], meta[1], meta[2], meta[3]
+    sources = own.shape[0]
+    rows = weight.shape[0] // sources // 2
+    cols = weight.shape[1] // LANES
+
+    def place(i, carry):
+        for c in range(cols):
+            lanes = slice(c * LANES, (c + 1) * LANES)
+            span = slice(c * rows, (c + 1) * rows)
+            first = pl.multiple_of((2 * i + t) * rows, rows)
+            second = pl.multiple_of((2 * i + 1 - t) * rows, rows)
+            weight[pl.ds(first, rows), lanes] = own[i, span, :]
+            weight[pl.ds(second, rows), lanes] = partner[i, span, :]
+        return carry
+
+    lax.fori_loop(0, sources, place, 0)
+    tok = xs[0].shape[0]
+    for r, x in enumerate(xs):
+        at = pl.ds(pl.multiple_of((k ^ r) * tok, tok), tok)
+        proj[at, :] = mm(x[...], weight[...]).astype(jnp.bfloat16)
+        gates[k ^ r] = mm(gate_t[...], x[...], 1, 1)[:8]
+    heads = bias.shape[1] // 4
+    b = [bias[sel, g * heads + jl] for g in range(4)]
+    lead = jnp.concatenate([jnp.full((1, tok), b[g], jnp.float32) for g in range(4)], axis=0)
+    forget = lax.broadcasted_iota(jnp.int32, (4, tok), 0) % 2 == 1
+    fwd, bwd = empty_state(), empty_state()
+    total_f = jnp.zeros((1, 1), jnp.float32)
+    total_b = jnp.zeros((1, 1), jnp.float32)
+    chunks = []
+    for c in range(plan_plane):
+        g = gates[c][:4] + lead
+        d = decay[c]
+        extra = jnp.concatenate([d[0:1], d[0:1], d[1:2], d[1:2]], axis=0)
+        logs = jnp.minimum(g, 0.0) - jnp.log1p(jnp.exp(-jnp.abs(g))) + extra
+        g = jnp.where(forget, logs, g)
+        gates[c] = jnp.concatenate([g, jnp.zeros((4, tok), jnp.float32)], axis=0)
+        vecs = chunk_vecs(gates[c])
+        span = slice(c * tok, (c + 1) * tok)
+        key = proj[span, LANES : 2 * LANES].astype(jnp.float32)
+        value = proj[span, 2 * LANES : 3 * LANES].astype(jnp.float32)
+        chunks.append((key, value, vecs))
+    for key, value, vecs in chunks:
+        fwd = forward_state(fwd, key, value, vecs[0])
+        total_f = total_f + vecs[0][3]
+    for key, value, vecs in chunks[::-1]:
+        bwd = backward_state(bwd, key, value, vecs[1])
+        total_b = total_b + vecs[1][3]
+    for i, ((cell, norm, peak), total) in enumerate(((fwd, total_f), (bwd, total_b))):
+        summary[i, :M_DIM, :] = cell
+        summary[i, M_DIM:, :] = jnp.concatenate(
+            [
+                norm,
+                jnp.broadcast_to(peak, (1, LANES)),
+                jnp.broadcast_to(total, (1, LANES)),
+                jnp.zeros((5, LANES), jnp.float32),
+            ],
+            axis=0,
+        )
+    last = proj.shape[0]
+    halo[0] = proj[:WINDOW, 5 * LANES :].astype(jnp.float32)
+    halo[1] = proj[last - WINDOW :, 5 * LANES :].astype(jnp.float32)
+
+
+def read_state(ref, i):
+    return (
+        ref[i, :M_DIM, :],
+        ref[i, M_DIM : M_DIM + 1, :],
+        ref[i, M_DIM + 1 : M_DIM + 2, 0:1],
+        ref[i, M_DIM + 2 : M_DIM + 3, 0:1],
+    )
+
+
+def merge_states(earlier, later, later_total):
+    peak = jnp.maximum(later_total + earlier[2], later[2])
+    old = jnp.exp(later_total + earlier[2] - peak)
+    new = jnp.exp(later[2] - peak)
+    return old * earlier[0] + new * later[0], old * earlier[1] + new * later[1], peak
+
+
+def combine_kernel(meta, own, partner, halo_partner, out):
+    t, hi = meta[0], meta[4]
+    forward = hi == 0
+    i = jnp.where(forward, 0, 1)
+    mine, other = read_state(own, i), read_state(partner, i)
+    mine_later = (t == 1) == forward
+    a = tuple(jnp.where(mine_later, y, x) for x, y in zip(mine, other))
+    b = tuple(jnp.where(mine_later, x, y) for x, y in zip(mine, other))
+    cell, norm, peak = merge_states(a[:3], b[:3], b[3])
+    out[:M_DIM, :] = cell
+    out[M_DIM : M_DIM + 8, :] = jnp.concatenate(
+        [norm, jnp.broadcast_to(peak, (1, LANES)), jnp.zeros((6, LANES), jnp.float32)], axis=0
+    )
+    out[M_DIM + 8 :, :] = halo_partner[jnp.where(forward, 1, 0)]
+
+
+def mixer_kernel(meta, sink, proj, gates, partner, halo_partner, across, gain, out_m, out_a, kv, logs):
+    t, sel, jl, hi = meta[0], meta[2], meta[3], meta[4]
+    chunks = gates.shape[0]
+    tok = gates.shape[2]
+    far = (
+        across[:M_DIM, :],
+        across[M_DIM : M_DIM + 1, :],
+        across[M_DIM + 1 : M_DIM + 2, 0:1],
+    )
+
+    def incoming(i, use_far, use_near):
+        near = read_state(partner, i)
+        far_peak = jnp.where(use_far, far[2], EMPTY)
+        near_peak = jnp.where(use_near, near[2], EMPTY)
+        near_total = jnp.where(use_near, near[3], 0.0)
+        return merge_states((far[0], far[1], far_peak), (near[0], near[1], near_peak), near_total)
+
+    scale = M_DIM ** (-0.5)
+    fwd = incoming(0, hi == 1, t == 1)
+    bwd = incoming(1, hi == 0, t == 0)
+    vecs = [chunk_vecs(gates[c]) for c in range(chunks)]
+
+    def kv_of(c):
+        span = slice(c * tok, (c + 1) * tok)
+        return (
+            proj[span, LANES : 2 * LANES].astype(jnp.float32),
+            proj[span, 2 * LANES : 3 * LANES].astype(jnp.float32),
+        )
+
+    back_states = [None] * chunks
+    for c in range(chunks - 1, -1, -1):
+        back_states[c] = bwd
+        if c:
+            bwd = backward_state(bwd, *kv_of(c), vecs[c][1])
+    r = lax.broadcasted_iota(jnp.int32, (tok, tok), 0)
+    col = lax.broadcasted_iota(jnp.int32, (tok, tok), 1)
+    gain_row = gain[sel, pl.ds(jl, 1), :]
+    for c in range(chunks):
+        span = slice(c * tok, (c + 1) * tok)
+        q = proj[span, :LANES]
+        qf = q.astype(jnp.float32)
+        scores = mm(q, proj[span, LANES : 2 * LANES], 1, 1) * scale
+        total_w = None
+        inter = None
+        for state, vec, mask in ((fwd, vecs[c][0], r >= col), (back_states[c], vecs[c][1], r <= col)):
+            cell, norm, peak = state
+            lead_col, src_row = vec[0], vec[1]
+            if mask is not None and vec is vecs[c][1]:
+                reach = peak + vec[3]
+            else:
+                reach = peak
+            masked = jnp.where(mask, src_row, EMPTY)
+            top = jnp.maximum(jnp.max(masked, axis=1, keepdims=True), reach)
+            w = jnp.exp(masked - top)
+            w_in = jnp.exp(reach - top)
+            denom = jnp.sum(scores * w, axis=1, keepdims=True) + w_in * scale * jnp.sum(
+                qf * norm, axis=1, keepdims=True
+            )
+            inv = 1.0 / jnp.maximum(jnp.abs(denom), jnp.exp(-(lead_col + top)))
+            part = w * inv
+            add = mm(qf, cell, 1, 0, HIGHEST) * (scale * w_in * inv)
+            total_w = part if total_w is None else total_w + part
+            inter = add if inter is None else inter + add
+        key, value = kv_of(c)
+        cell_out = mm(scores * total_w, value, 1, 0, HIGHEST) + inter
+        fwd = forward_state(fwd, key, value, vecs[c][0])
+        gate = proj[span, 3 * LANES : 4 * LANES].astype(jnp.float32)
+        u = cell_out / (1.0 + jnp.exp(-gate))
+        u = u * lax.rsqrt(jnp.mean(u * u, axis=1, keepdims=True) + EPS) * gain_row
+        out_m[c, :tok, :] = u.astype(jnp.bfloat16)
+        out_m[c, tok:, :] = jnp.zeros((out_m.shape[1] - tok, LANES), jnp.bfloat16)
+
+    length = proj.shape[0]
+    inner_edge = halo_partner[jnp.where(t == 0, 0, 1)].astype(jnp.bfloat16)
+    outer_edge = across[M_DIM + 8 :, :].astype(jnp.bfloat16)
+    kv[:WINDOW, :] = jnp.where(t == 0, outer_edge, inner_edge)
+    kv[WINDOW : WINDOW + length, :] = proj[:, 5 * LANES :]
+    kv[WINDOW + length :, :] = jnp.where(t == 0, inner_edge, outer_edge)
+    at_start = (hi == 0) & (t == 0)
+    at_end = (hi == 1) & (t == 1)
+    qi = lax.broadcasted_iota(jnp.int32, (WINDOW, 3 * WINDOW), 0)
+    ki = lax.broadcasted_iota(jnp.int32, (WINDOW, 3 * WINDOW), 1) - WINDOW
+    band = jnp.abs(ki - qi) <= WINDOW
+    diag = lax.broadcasted_iota(jnp.int32, (WINDOW, WINDOW), 0) == lax.broadcasted_iota(
+        jnp.int32, (WINDOW, WINDOW), 1
+    )
+    blocks = length // WINDOW
+    per = tok // WINDOW
+    for b in range(blocks):
+        usable = band
+        if b == 0:
+            usable = usable & ((ki >= 0) | jnp.logical_not(at_start))
+        if b == blocks - 1:
+            usable = usable & ((ki < WINDOW) | jnp.logical_not(at_end))
+        keys = kv[b * WINDOW : (b + 3) * WINDOW, :W_DIM]
+        values = kv[b * WINDOW : (b + 3) * WINDOW, W_DIM:]
+        mixed = []
+        for h in range(2):
+            lanes = slice(4 * LANES + h * W_DIM, 4 * LANES + (h + 1) * W_DIM)
+            q = proj[b * WINDOW : (b + 1) * WINDOW, lanes]
+            s = mm(q, keys, 1, 1) * W_DIM ** (-0.5)
+            s = jnp.where(usable, s, EMPTY)
+            sink_h = sink[sel, 2 * jl + h]
+            peak = jnp.maximum(jnp.max(s, axis=1, keepdims=True), sink_h)
+            e = jnp.exp(s - peak)
+            total = jnp.exp(sink_h - peak) + jnp.sum(e, axis=1, keepdims=True)
+            mixed.append(mm(e.astype(jnp.bfloat16), values) / total)
+            log_col = peak + jnp.log(total)
+            log_row = jnp.sum(jnp.where(diag, log_col, 0.0), axis=0, keepdims=True)
+            at = h * per + b % per
+            logs[b // per, at : at + 1, :] = log_row
+        out_a[b // per, (b % per) * WINDOW : (b % per + 1) * WINDOW, :] = jnp.concatenate(
+            mixed, axis=1
+        ).astype(jnp.bfloat16)
+    for c in range(chunks):
+        x = logs[c]
+        high = x.astype(jnp.bfloat16).astype(jnp.float32)
+        mid = (x - high).astype(jnp.bfloat16).astype(jnp.float32)
+        low = x - high - mid
+        n = x.shape[0]
+        pad = jnp.zeros((out_a.shape[1] - tok - 3 * n, LANES), jnp.float32)
+        out_a[c, tok:, :] = jnp.concatenate([high, mid, low, pad], axis=0).astype(jnp.bfloat16)
+
+
+def output_kernel(meta, own, partner, weight, mixed, log_total, left):
+    t = meta[0]
+    heads, tok = own.shape[0], mixed.shape[0]
+    for j in range(heads):
+        left[t * heads + j] = own[j, :tok, :]
+        left[(1 - t) * heads + j] = partner[j, :tok, :]
+    lhs = jnp.concatenate([left[i] for i in range(2 * heads)], axis=1)
+    half = weight.shape[1] // 2
+    rhs = jnp.concatenate(
+        [weight[s, :half, :] for s in range(weight.shape[0])]
+        + [weight[s, half:, :] for s in range(weight.shape[0])],
+        axis=0,
+    )
+    mixed[...] = mm(lhs, rhs).astype(jnp.bfloat16)
+    per = tok // LANES
+    n = 2 * per
+    for i in range(heads // 2):
+        j = t * (heads // 2) + i
+        rows = jnp.where(t == 1, own[j, tok:, :], partner[j, tok:, :]).astype(jnp.float32)
+        x = rows[:n] + rows[n : 2 * n] + rows[2 * n : 3 * n]
+        for h in range(2):
+            log_total[2 * i + h : 2 * i + h + 1, :] = jnp.concatenate(
+                [x[h * per + p : h * per + p + 1] for p in range(per)], axis=1
+            )
+
+
+def bf16_parts(x):
+    high = lax.reduce_precision(x, 8, 7)
+    mid = lax.reduce_precision(x - high, 8, 7)
+    return jnp.stack([high, mid, x - high - mid]).astype(jnp.bfloat16)
+
+
+def on_device_split(
+    plan,
+    tokens,
+    input_norm_gain,
+    mq_weight,
+    mk_weight,
+    mv_weight,
+    mo_weight,
+    gate_weight,
+    gate_bias,
+    decay_extra,
+    m_gain,
+    aq_weight,
+    ak_weight,
+    av_weight,
+    sink_logit,
+    out_m_weight,
+    out_a_weight,
+):
+    sp, group, plane, lh, tok = (plan[n] for n in ("sp", "group", "plane", "lh", "tok"))
+    width, rows = plan["width"], plan["rows"]
+    half = rows // 2
+    f32, bf16 = jnp.float32, jnp.bfloat16
+    s = lax.axis_index("sp").astype(jnp.int32)
+    t = lax.axis_index("tp").astype(jnp.int32)
+    hi, j = s // group, s % group
+    near_plane = (s // plane) % 2
+    meta = jnp.stack([t, s % plane, jnp.where(j // lh == t, 0, 1), j % lh, hi]).astype(jnp.int32)
+    swap = [(0, 1), (1, 0)]
+
+    def flip(x):
+        return lax.ppermute(x, "tp", swap)
+
+    normed = rms_rows(tokens.astype(f32), input_norm_gain).astype(bf16)
+    out_full = lax.all_gather(
+        jnp.concatenate([out_m_weight, out_a_weight], axis=0), "sp", axis=0, tiled=True
+    ).reshape(sp, 2 * out_m_weight.shape[0], out_m_weight.shape[1])
+
+    cross = [
+        (2 * a + (a // plane) % 2, 2 * (a ^ plane) + (a // plane) % 2) for a in range(sp)
+    ]
+    other = lax.ppermute(normed, ("sp", "tp"), cross)
+    base = jnp.where(t == near_plane, normed, other)
+    xs = [base] + [
+        lax.ppermute(base, "sp", [(a, a ^ r) for a in range(sp)]) for r in range(1, plane)
+    ]
+
+    gate_rows = jnp.transpose(gate_weight.reshape(2, half, 4, lh), (0, 3, 2, 1)).reshape(
+        2, lh, 4 * half // LANES, LANES
+    )
+    decay_rows = jnp.transpose(bf16_parts(decay_extra), (1, 2, 0, 3)).reshape(
+        2, lh, 3 * tok // LANES, LANES
+    )
+    small = jnp.concatenate([gate_rows, decay_rows], axis=2)
+    n_gate, n_small = gate_rows.shape[2], small.shape[2]
+    n_rows = 6 * half + n_small
+    packed = vmem_call(
+        pack_kernel, jax.ShapeDtypeStruct((2, lh, n_rows, LANES), bf16), n_in=8
+    )(mq_weight, mk_weight, mv_weight, mo_weight, aq_weight, ak_weight, av_weight, small)
+    keep = lax.dynamic_index_in_dim(packed, t, 0, keepdims=False)
+    got = flip(lax.dynamic_index_in_dim(packed, 1 - t, 0, keepdims=False))
+    by_head = jnp.concatenate(
+        [jnp.where(t == 0, keep, got), jnp.where(t == 0, got, keep)], axis=0
+    )
+    spread = jnp.concatenate([by_head, by_head], axis=0).reshape(sp * n_rows, LANES)
+    own_w = lax.all_to_all(spread, "sp", 0, 0, tiled=True)
+    partner_w = flip(own_w)
+    own_w = own_w.reshape(sp, n_rows, LANES)
+    partner_w = partner_w.reshape(sp, n_rows, LANES)
+    small_both = jnp.stack([own_w[:, 6 * half :], partner_w[:, 6 * half :]])
+    small_both = jnp.where(t == 0, small_both, small_both[::-1])
+    gate_t = jnp.transpose(small_both[:, :, :n_gate].reshape(2, sp, 4, half), (2, 1, 0, 3))
+    gate_t = jnp.pad(gate_t.reshape(4, width), ((0, 12), (0, 0)))
+    first = (2 * hi + t) * plane
+    decay = lax.dynamic_slice_in_dim(small_both[:, :, n_gate:], first, plane, 1)
+    decay = jnp.sum(decay.reshape(2, plane, 3, tok).astype(f32), axis=2)
+    decay = jnp.transpose(decay, (1, 0, 2))
+    params = jnp.concatenate(
+        [m_gain, gate_bias.reshape(-1), sink_logit, jnp.zeros((LANES - 6 * lh,), f32)]
+    ).reshape(-1, LANES)
+    params = jnp.stack([params, flip(params)])
+    gain = params[:, :lh]
+    bias = params[:, lh, : 4 * lh]
+    sink = params[:, lh, 4 * lh : 6 * lh]
+
+    quarter = plane * tok
+    cols = 6 * LANES
+    proj, gates, summary, halo = vmem_call(
+        project_kernel,
+        (
+            jax.ShapeDtypeStruct((quarter, cols), bf16),
+            jax.ShapeDtypeStruct((plane, 8, tok), f32),
+            jax.ShapeDtypeStruct((2, M_DIM + 8, LANES), f32),
+            jax.ShapeDtypeStruct((2, WINDOW, LANES), f32),
+        ),
+        scratch=[pltpu.VMEM((width, cols), bf16)],
+        smem=2,
+        n_in=plane + 4,
+        flops=2 * quarter * width * cols,
+    )(meta, bias, *xs, own_w, partner_w, gate_t, decay)
+    both = flip(jnp.concatenate([summary, halo], axis=1))
+    partner_sum, partner_halo = both[:, : M_DIM + 8], both[:, M_DIM + 8 :]
+    sent = vmem_call(
+        combine_kernel,
+        jax.ShapeDtypeStruct((M_DIM + 8 + WINDOW, LANES), f32),
+        smem=1,
+        n_in=3,
+    )(meta, summary, partner_sum, partner_halo)
+    across = lax.ppermute(sent, "sp", [(a, (a + group) % sp) for a in range(sp)])
+    part = jax.ShapeDtypeStruct((plane, tok + 16, LANES), bf16)
+    out_m, out_a = vmem_call(
+        mixer_kernel,
+        (part, part),
+        scratch=[
+            pltpu.VMEM((quarter + 2 * WINDOW, LANES), bf16),
+            pltpu.VMEM((plane, 2 * tok // WINDOW, LANES), f32),
+        ],
+        smem=2,
+        n_in=6,
+        flops=2 * quarter * width * cols,
+    )(meta, sink, proj, gates, partner_sum, partner_halo, across, gain)
+
+    lead = jnp.where(t == 0, out_m, out_a)
+    got = flip(jnp.where(t == 0, out_a, out_m))
+    spread = jnp.concatenate(
+        [jnp.where(t == 0, lead, got), jnp.where(t == 0, got, lead)], axis=0
+    ).reshape(group * (tok + 16), LANES)
+    groups = [list(range(g * group, (g + 1) * group)) for g in range(sp // group)]
+    mine = lax.all_to_all(spread, "sp", 0, 0, axis_index_groups=groups, tiled=True)
+    theirs = flip(mine)
+    shape = (group, tok + 16, LANES)
+    return vmem_call(
+        output_kernel,
+        (
+            jax.ShapeDtypeStruct((tok, out_m_weight.shape[1]), bf16),
+            jax.ShapeDtypeStruct((2 * lh, tok), f32),
+        ),
+        scratch=[pltpu.VMEM((2 * group, tok, LANES), bf16)],
+        smem=1,
+        n_in=3,
+        flops=2 * tok * width * out_m_weight.shape[1],
+    )(meta, mine.reshape(shape), theirs.reshape(shape), out_full)
+
+
 def solution(mesh):
     in_specs = (
         P("sp", None),
@@ -328,6 +845,10 @@
         P("sp", "tp"),
     )
     out_specs = (P("sp", "tp"), P("tp", "sp"))
+    def per_device(*args):
+        plan = split_plan(mesh, args)
+        return on_device(*args) if plan is None else on_device_split(plan, *args)
+
     return jax.shard_map(
-        on_device, mesh=mesh, in_specs=in_specs, out_specs=out_specs, check_vma=False
-    )
+        per_device, mesh=mesh, in_specs=in_specs, out_specs=out_specs, check_vma=False
+    )

time: 724 us -> 226 us (0.31)
  waiting for transfers between devices: 440 us -> 103 us
  blocking collectives: 165 us -> 13.4 us
  matrix products: 66.3 us -> 0 us
  Pallas kernels: 0 us -> 43.9 us
  starting transfers between devices: 5.25 us -> 31 us
  local copies, waits for them, and re-layouts: 15.5 us -> 7.69 us
    all_gather x11 -> x1, waiting for transfers between devices: 429 us -> 0.01 us  [on_device_split(): lax.all_gather(jnp.concatenate([out_m_weight, out_a_weight], axis=0), 'sp...]
    all_gather x5 -> x0, blocking collectives: 126 us -> none  [the longest x1 43.3 us: on_device(): lax.all_gather(gate_weight, 'sp', axis=0, tiled=True)]
    dot_general x68 -> x0, matrix products: 66.3 us -> none  [the longest x8 17.9 us: on_device(): jnp.dot(normed, segment, preferred_element_type=jnp.float32)]
    ppermute x2 -> x11, waiting for transfers between devices: 5.37 us -> 69.9 us  [the longest x3 48.2 us: on_device_split(): lax.ppermute(base, 'sp', [(a, a ^ r) for a in range(sp)])]
    pallas_call x0 -> x5, Pallas kernels: none -> 43.9 us  [the longest x1 22.1 us: on_device_split(): vmem_call(mixer_kernel, (part, part), scratch=[pltpu.VMEM((quarter + 2 *...]
    unnamed x1 -> x0, blocking collectives: 39.7 us -> none
    all_to_all x0 -> x1, waiting for transfers between devices: none -> 32.9 us  [on_device_split(): own_w = lax.all_to_all(spread, 'sp', 0, 0, tiled=True)]
    ppermute x2 -> x11, starting transfers between devices: 4.83 us -> 22.6 us  [the longest x6 10.4 us: flip(): return lax.ppermute(x, 'tp', swap)]
  transfers between devices with their start and end apart: 13 -> 13, of which waited for: 13 -> 11; matrix products, arithmetic and copies ran while one was open for 13% -> 6% of each run, Pallas kernels for 0% -> 16%
where the time goes in v1:
time: 226 us
  waiting for transfers between devices  103 us (46%)
  Pallas kernels  43.9 us (19%)
  starting transfers between devices  31 us (14%)
  between operations  14.2 us (6%)
  blocking collectives  13.4 us (6%)
  other arithmetic  12.5 us (6%)
  local copies, waits for them, and re-layouts  7.69 us (3%)
    ppermute x3, waiting for transfers between devices, on_device_split(): lax.ppermute(base, 'sp', [(a, a ^ r) for a in range(sp)])  48.2 us
    all_to_all x1, waiting for transfers between devices, on_device_split(): own_w = lax.all_to_all(spread, 'sp', 0, 0, tiled=True)  32.9 us
    pallas_call x1, Pallas kernels, on_device_split(): vmem_call(mixer_kernel, (part, part), scratch=[pltpu.VMEM((quarter + 2 *...  22.1 us
    all_to_all x1, blocking collectives, on_device_split(): lax.all_to_all(spread, 'sp', 0, 0, axis_index_groups=groups, tiled=True)  13.4 us
    pallas_call x1, Pallas kernels, on_device_split(): vmem_call(project_kernel, (jax.ShapeDtypeStruct((quarter, cols), bf16), j...  13.1 us
    ppermute x6, starting transfers between devices, flip(): return lax.ppermute(x, 'tp', swap)  10.4 us
    ppermute x1, waiting for transfers between devices, on_device_split(): other = lax.ppermute(normed, ('sp', 'tp'), cross)  9.41 us
    all_to_all x1, starting transfers between devices, on_device_split(): own_w = lax.all_to_all(spread, 'sp', 0, 0, tiled=True)  8.37 us
  transfers between devices with their start and end apart: 13, of which 11 were waited for; matrix products, arithmetic and copies ran while one was open for 6% of the time, Pallas kernels for 16%

profile of v1, /device:TPU:0, one launch (start us, length us, event | category | flops | bytes accessed | tf_op | source)
XLA Modules:
  0.0 225.6 jit_solution(985627403959734535)
XLA Ops:
  7.2 0.7 fusion.5
  7.9 0.8 reshape.60
  8.7 0.1 reshape.61
  8.8 0.6 pad_maximum_fusion.5.small
  9.4 2.2 shard_map.167
  11.7 1.0 dynamic-slice_bitcast_fusion
  12.7 0.6 collective-permute-start.5
  13.2 1.4 collective-permute-done.5
  14.6 1.1 bitcast_select_fusion.1
  15.7 1.4 pad_maximum_fusion
  17.1 8.4 %all-to-all-start = ((bf16[16,392,128]{2,1,0:T(8,128)(2,1)}), bf16[16,392,128]{2,1,0:T(8,128)(2,1)S(1)}, u32[]{:S(2)}, u32[]{:S(2)}) async-start(bf16[16,392,128]{2,1,0:T(8,128)(2,1)} %pad_maximum_fusion), calls=%async_computation | async-start | bytes 3211264 | tf_op jit(solution)/shard_map/all_to_all | solution.py:749
  25.4 0.0 copy-start.7
  25.4 0.0 all-gather.2.cloned.1.call-start
  25.5 0.7 pad_maximum_fusion.3
  26.2 0.0 all-gather.2.cloned.1.call-update
  26.3 0.3 fusion
  26.6 1.3 fusion.2
  27.9 5.0 %collective-permute-start.1 = (bf16[256,2048]{1,0:T(8,128)(2,1)}, bf16[256,2048]{1,0:T(8,128)(2,1)}, u32[]{:S(2)}, u32[]{:S(2)}) collective-permute-start(bf16[256,2048]{1,0:T(8,128)(2,1)} %fusion.2), channel_id=1, source_target_pairs={{0,8},{2,10},{4,12},{6,14},{9,1},{11,3},{13,5},{15,7},{16,24},{18,... | collective-permute-start | bytes 3145736 | tf_op jit(solution)/shard_map/ppermute | solution.py:725
  32.9 32.9 %all-to-all-done.refs_4_ = bf16[16,392,128]{2,1,0:T(8,128)(2,1)S(1)} async-done(((bf16[16,392,128]{2,1,0:T(8,128)(2,1)}), bf16[16,392,128]{2,1,0:T(8,128)(2,1)S(1)}, u32[]{:S(2)}, u32[]{:S(2)}) %all-to-all-start) | async-done | bytes 1605664 | tf_op jit(solution)/shard_map/all_to_all | solution.py:749
  65.8 0.0 collective-permute-start.6
  65.8 0.1 reshape.58
  65.9 9.4 %collective-permute-done.1 = bf16[256,2048]{1,0:T(8,128)(2,1)} collective-permute-done((bf16[256,2048]{1,0:T(8,128)(2,1)}, bf16[256,2048]{1,0:T(8,128)(2,1)}, u32[]{:S(2)}, u32[]{:S(2)}) %collective-permute-start.1) | collective-permute-done | bytes 1048608 | tf_op jit(solution)/shard_map/ppermute | solution.py:725
  75.3 1.4 broadcast_select_fusion.refs_0_
  76.8 1.7 collective-permute-start.2
  78.4 1.2 collective-permute-start.3
  79.6 0.7 collective-permute-start.4
  80.2 0.0 copy-done.9
  80.3 0.1 fusion.8
  80.3 4.6 %collective-permute-start = (f32[5,128]{1,0:T(8,128)S(1)}, f32[5,128]{1,0:T(8,128)S(1)}, u32[]{:S(2)}, u32[]{:S(2)}) collective-permute-start(f32[5,128]{1,0:T(8,128)S(1)} %get-tuple-element.22), channel_id=1, source_target_pairs={{0,1},{1,0},{2,3},{3,2},{4,5},{5,4},{6,7},{7,6},{8,9},{9,8},{10,11... | collective-permute-start | bytes 7688 | tf_op jit(solution)/shard_map/ppermute | solution.py:715
  84.9 0.6 stack.54.meta
  85.5 0.3 collective-permute-done
  85.7 0.6 pad_maximum_fusion.8
  86.3 0.0 collective-permute-done.6
  86.3 0.8 slice_bitcast_fusion
  87.2 0.6 copy.32
  87.8 0.1 reshape.64
  88.0 0.1 reshape.65
  88.1 0.6 pad.4.refs_6_
  88.7 21.8 %collective-permute-done.2.refs_1_ = bf16[256,2048]{1,0:T(8,128)(2,1)} collective-permute-done((bf16[256,2048]{1,0:T(8,128)(2,1)}, bf16[256,2048]{1,0:T(8,128)(2,1)}, u32[]{:S(2)}, u32[]{:S(2)}) %collective-permute-start.2) | collective-permute-done | bytes 1048608 | tf_op jit(solution)/shard_map/ppermute | solution.py:728
  110.5 3.8 %collective-permute-done.3.refs_2_ = bf16[256,2048]{1,0:T(8,128)(2,1)} collective-permute-done((bf16[256,2048]{1,0:T(8,128)(2,1)}, bf16[256,2048]{1,0:T(8,128)(2,1)}, u32[]{:S(2)}, u32[]{:S(2)}) %collective-permute-start.3) | collective-permute-done | bytes 1048608 | tf_op jit(solution)/shard_map/ppermute | solution.py:728
  114.3 22.6 %collective-permute-done.4.refs_3_ = bf16[256,2048]{1,0:T(8,128)(2,1)} collective-permute-done((bf16[256,2048]{1,0:T(8,128)(2,1)}, bf16[256,2048]{1,0:T(8,128)(2,1)}, u32[]{:S(2)}, u32[]{:S(2)}) %collective-permute-start.4) | collective-permute-done | bytes 1048608 | tf_op jit(solution)/shard_map/ppermute | solution.py:728
  136.9 13.1 %shard_map.168 = (bf16[1024,768]{1,0:T(8,128)(2,1)}, f32[4,8,256]{2,1,0:T(8,128)}, f32[2,136,128]{2,1,0:T(8,128)}, f32[2,128,128]{2,1,0:T(8,128)}) custom-call(s32[5]{0:T(128)} %stack.54.meta, f32[2,16]{1,0:T(2,128)} %bitcast.55, bf16[256,2048]{1,0:T(8,128)(2,1)} %broadcast_select_fusion.refs_0_, bf16[256,2048]{1,0:T(8,128)(2,1)} %collective-permute-done.2.refs_1_, ...), custom_call_target="tpu_custom_call" | custom-call | flops 3221225472 | tf_op jit(solution)/shard_map/pallas_call | solution.py:771
  150.0 1.0 pad_maximum_fusion.2
  151.0 5.2 %collective-permute-start.7 = (f32[2,264,128]{2,1,0:T(8,128)S(1)}, f32[2,264,128]{2,1,0:T(8,128)S(1)}, u32[]{:S(2)}, u32[]{:S(2)}) collective-permute-start(f32[2,264,128]{2,1,0:T(8,128)S(1)} %pad_maximum_fusion.2), channel_id=1, source_target_pairs={{0,1},{1,0},{2,3},{3,2},{4,5},{5,4},{6,7},{7,6},{8,9},{9,8},{10,11... | collective-permute-start | bytes 811016 | tf_op jit(solution)/shard_map/ppermute | solution.py:715
  156.1 1.2 collective-permute-done.7
  157.3 0.7 slice.40.partner
  158.0 0.7 slice.41.halo_partner
  158.7 1.8 shard_map.169
  160.5 3.8 %collective-permute-start.8 = (f32[264,128]{1,0:T(8,128)}, f32[264,128]{1,0:T(8,128)S(1)}, u32[]{:S(2)}, u32[]{:S(2)}) collective-permute-start(f32[264,128]{1,0:T(8,128)} %shard_map.169), channel_id=1, source_target_pairs={{0,16},{2,18},{4,20},{6,22},{8,24},{10,26},{12,28},{14,30},{16,0},... | collective-permute-start | bytes 405512 | tf_op jit(solution)/shard_map/ppermute | solution.py:792
  164.2 0.6 pad_maximum_fusion.9
  164.8 0.6 pad_maximum_fusion.6.gain
  165.4 6.0 %collective-permute-done.8.across = f32[264,128]{1,0:T(8,128)S(1)} collective-permute-done((f32[264,128]{1,0:T(8,128)}, f32[264,128]{1,0:T(8,128)S(1)}, u32[]{:S(2)}, u32[]{:S(2)}) %collective-permute-start.8) | collective-permute-done | bytes 135200 | tf_op jit(solution)/shard_map/ppermute | solution.py:792
  171.5 0.6 copy-done.10
  172.1 22.1 %shard_map.170 = (bf16[4,272,128]{2,1,0:T(8,128)(2,1)}, bf16[4,272,128]{2,1,0:T(8,128)(2,1)}) custom-call(s32[5]{0:T(128)} %stack.54.meta, f32[2,8]{1,0:T(2,128)} %bitcast.56, bf16[1024,768]{1,0:T(8,128)(2,1)} %get-tuple-element.8.proj, f32[4,8,256]{2,1,0:T(8,128)} %get-tuple-element.9.gates, f32[2,136,128]{2,1,0:T(8,128)} %slice.40.partner, ...), custom_call_target="tpu_custom_call" | custom-call | flops 3221225472 | tf_op jit(solution)/shard_map/pallas_call | solution.py:794
  194.2 1.0 broadcast_select_fusion.3
  195.2 0.1 collective-permute-start.9
  195.3 1.5 collective-permute-done.9
  196.8 1.0 broadcast_select_fusion.2
  197.8 0.1 pad_maximum_fusion.1
  197.9 13.4 %all_to_all.18.own = bf16[8,272,128]{2,1,0:T(8,128)(2,1)S(1)} all-to-all(bf16[8,272,128]{2,1,0:T(8,128)(2,1)S(1)} %pad_maximum_fusion.1), channel_id=1, replica_groups={{0,2,4,6,8,10,12,14},{16,18,20,22,24,26,28,30},{1,3,5,7,9,11,13,15},{17..., dimensions={0} | all-to-all | bytes 1114112 | tf_op jit(solution)/shard_map/all_to_all | solution.py:812
  211.3 0.0 collective-permute-start.10
  211.3 2.0 collective-permute-done.10
  213.3 0.8 copy-done.3
  214.1 4.6 %shard_map.171 = (bf16[256,1024]{1,0:T(8,128)(2,1)}, f32[8,256]{1,0:T(8,128)}) custom-call(s32[5]{0:T(128)} %stack.54.meta, bf16[8,272,128]{2,1,0:T(8,128)(2,1)} %copy-done.1, bf16[8,272,128]{2,1,0:T(8,128)(2,1)} %bitcast.48, bf16[16,128,1024]{2,1,0:T(8,128)(2,1)} %bitcast.45), custom_call_target="tpu_custom_call" | custom-call | flops 1073741824 | tf_op jit(solution)/shard_map/pallas_call | solution.py:815
  (34 shorter events, 0.3 us)
Async XLA Ops:
  12.7 1.9 collective-permute-start.5
  17.1 8.4 %copy-start.4 = (bf16[64,1024]{1,0:T(8,128)(2,1)S(1)}, bf16[64,1024]{1,0:T(8,128)(2,1)}, u32[]{:S(2)}) copy-start(bf16[64,1024]{1,0:T(8,128)(2,1)} %param.31) | copy-start | bytes 393220
  17.1 8.5 %copy-start.5 = (bf16[64,1024]{1,0:T(8,128)(2,1)S(1)}, bf16[64,1024]{1,0:T(8,128)(2,1)}, u32[]{:S(2)}) copy-start(bf16[64,1024]{1,0:T(8,128)(2,1)} %param.30) | copy-start | bytes 393220
  17.1 9.2 %copy-start = (bf16[256,2048]{1,0:T(8,128)(2,1)S(1)}, bf16[256,2048]{1,0:T(8,128)(2,1)}, u32[]{:S(2)}) copy-start(bf16[256,2048]{1,0:T(8,128)(2,1)} %param.16) | copy-start | bytes 3145732
  17.1 9.5 %copy-start.6 = (f32[2048]{0:T(1024)S(1)}, f32[2048]{0:T(1024)}, u32[]{:S(2)}) copy-start(f32[2048]{0:T(1024)} %param.17) | copy-start | bytes 24580
  17.1 48.8 %all-to-all-start = ((bf16[16,392,128]{2,1,0:T(8,128)(2,1)}), bf16[16,392,128]{2,1,0:T(8,128)(2,1)S(1)}, u32[]{:S(2)}, u32[]{:S(2)}) async-start(bf16[16,392,128]{2,1,0:T(8,128)(2,1)} %pad_maximum_fusion), calls=%async_computation | async-start | bytes 3211264 | tf_op jit(solution)/shard_map/all_to_all | solution.py:749
  25.4 40.4 %copy-start.7 = (f32[4,4]{1,0:T(4,128)S(1)}, f32[4,4]{1,0:T(4,128)}, u32[]{:S(2)}) copy-start(f32[4,4]{1,0:T(4,128)} %param.23) | copy-start | bytes 196
  25.4 187.9 %all-gather.2.cloned.1.call-start = ((), (), s32[]{:S(2)}) async-start(), calls=%async_computation.2 | async-start | bytes 4456448 | tf_op jit(solution)/shard_map/all_gather | solution.py:718
  27.9 52.3 %copy-start.8 = (f32[512]{0:T(512)S(1)}, f32[512]{0:T(512)}, u32[]{:S(2)}) copy-start(f32[512]{0:T(512)} %param.25) | copy-start | bytes 6148
  27.9 52.3 %copy-start.9 = (f32[8]{0:T(128)S(1)}, f32[8]{0:T(128)}, u32[]{:S(2)}) copy-start(f32[8]{0:T(128)} %param.29) | copy-start | bytes 100
  27.9 47.4 %collective-permute-start.1 = (bf16[256,2048]{1,0:T(8,128)(2,1)}, bf16[256,2048]{1,0:T(8,128)(2,1)}, u32[]{:S(2)}, u32[]{:S(2)}) collective-permute-start(bf16[256,2048]{1,0:T(8,128)(2,1)} %fusion.2), channel_id=1, source_target_pairs={{0,8},{2,10},{4,12},{6,14},{9,1},{11,3},{13,5},{15,7},{16,24},{18,... | collective-permute-start | bytes 3145736 | tf_op jit(solution)/shard_map/ppermute | solution.py:725
  65.8 22.1 %copy-start.2 = (bf16[16,392,128]{2,1,0:T(8,128)(2,1)}, bf16[16,392,128]{2,1,0:T(8,128)(2,1)S(1)}, u32[]{:S(2)}) copy-start(bf16[16,392,128]{2,1,0:T(8,128)(2,1)S(1)} %all-to-all-done.refs_4_) | copy-start | bytes 4816900
  65.8 20.5 %collective-permute-start.6 = (bf16[6272,128]{1,0:T(8,128)(2,1)S(1)}, bf16[6272,128]{1,0:T(8,128)(2,1)}, u32[]{:S(2)}, u32[]{:S(2)}) collective-permute-start(bf16[6272,128]{1,0:T(8,128)(2,1)S(1)} %bitcast.47), channel_id=1, source_target_pairs={{0,1},{1,0},{2,3},{3,2},{4,5},{5,4},{6,7},{7,6},{8,9},{9,8},{10,11... | collective-permute-start | bytes 4816904 | tf_op jit(solution)/shard_map/ppermute | solution.py:715
  76.8 33.7 %collective-permute-start.2 = (bf16[256,2048]{1,0:T(8,128)(2,1)}, bf16[256,2048]{1,0:T(8,128)(2,1)}, u32[]{:S(2)}, u32[]{:S(2)}) collective-permute-start(bf16[256,2048]{1,0:T(8,128)(2,1)} %broadcast_select_fusion.refs_0_), channel_id=1, source_target_pairs={{0,2},{2,0},{4,6},{6,4},{8,10},{10,8},{12,14},{14,12},{16,18},{18,... | collective-permute-start | bytes 3145736 | tf_op jit(solution)/shard_map/ppermute | solution.py:728
  78.4 35.8 %collective-permute-start.3 = (bf16[256,2048]{1,0:T(8,128)(2,1)}, bf16[256,2048]{1,0:T(8,128)(2,1)}, u32[]{:S(2)}, u32[]{:S(2)}) collective-permute-start(bf16[256,2048]{1,0:T(8,128)(2,1)} %broadcast_select_fusion.refs_0_), channel_id=1, source_target_pairs={{0,4},{2,6},{4,0},{6,2},{8,12},{10,14},{12,8},{14,10},{16,20},{18,... | collective-permute-start | bytes 3145736 | tf_op jit(solution)/shard_map/ppermute | solution.py:728
  79.6 57.3 %collective-permute-start.4 = (bf16[256,2048]{1,0:T(8,128)(2,1)}, bf16[256,2048]{1,0:T(8,128)(2,1)}, u32[]{:S(2)}, u32[]{:S(2)}) collective-permute-start(bf16[256,2048]{1,0:T(8,128)(2,1)} %broadcast_select_fusion.refs_0_), channel_id=1, source_target_pairs={{0,6},{2,4},{4,2},{6,0},{8,14},{10,12},{12,10},{14,8},{16,22},{18,... | collective-permute-start | bytes 3145736 | tf_op jit(solution)/shard_map/ppermute | solution.py:728
  80.3 5.4 %collective-permute-start = (f32[5,128]{1,0:T(8,128)S(1)}, f32[5,128]{1,0:T(8,128)S(1)}, u32[]{:S(2)}, u32[]{:S(2)}) collective-permute-start(f32[5,128]{1,0:T(8,128)S(1)} %get-tuple-element.22), channel_id=1, source_target_pairs={{0,1},{1,0},{2,3},{3,2},{4,5},{5,4},{6,7},{7,6},{8,9},{9,8},{10,11... | collective-permute-start | bytes 7688 | tf_op jit(solution)/shard_map/ppermute | solution.py:715
  151.0 6.3 %collective-permute-start.7 = (f32[2,264,128]{2,1,0:T(8,128)S(1)}, f32[2,264,128]{2,1,0:T(8,128)S(1)}, u32[]{:S(2)}, u32[]{:S(2)}) collective-permute-start(f32[2,264,128]{2,1,0:T(8,128)S(1)} %pad_maximum_fusion.2), channel_id=1, source_target_pairs={{0,1},{1,0},{2,3},{3,2},{4,5},{5,4},{6,7},{7,6},{8,9},{9,8},{10,11... | collective-permute-start | bytes 811016 | tf_op jit(solution)/shard_map/ppermute | solution.py:715
  160.5 11.0 %collective-permute-start.8 = (f32[264,128]{1,0:T(8,128)}, f32[264,128]{1,0:T(8,128)S(1)}, u32[]{:S(2)}, u32[]{:S(2)}) collective-permute-start(f32[264,128]{1,0:T(8,128)} %shard_map.169), channel_id=1, source_target_pairs={{0,16},{2,18},{4,20},{6,22},{8,24},{10,26},{12,28},{14,30},{16,0},... | collective-permute-start | bytes 405512 | tf_op jit(solution)/shard_map/ppermute | solution.py:792
  171.5 0.7 copy-start.10
  195.2 1.6 collective-permute-start.9
  211.3 2.0 copy-start.1
  211.3 2.0 collective-permute-start.10
  213.3 0.8 copy-start.3
Sparse Core Ops, SparseCore 0:
  29.0 104.4 all-gather.1

commit v2 on v1

--- a/solution.py
+++ b/solution.py
@@ -278,12 +278,8 @@
     forward_sum = summarize(key_vecs, value_vecs, in_fwd, forget_fwd)
     backward_sum = summarize(keys_bwd, values_bwd, in_bwd, forget_bwd)
     state_fwd, state_bwd = gather_states(forward_sum, backward_sum)
-    hidden_fwd, forward_unused = block_pass(
-        queries, key_vecs, value_vecs, in_fwd, forget_fwd, state_fwd
-    )
-    hidden_bwd, unused_bwd = block_pass(
-        queries_bwd, keys_bwd, values_bwd, in_bwd, forget_bwd, state_bwd
-    )
+    hidden_fwd, _ = block_pass(queries, key_vecs, value_vecs, in_fwd, forget_fwd, state_fwd)
+    hidden_bwd, _ = block_pass(queries_bwd, keys_bwd, values_bwd, in_bwd, forget_bwd, state_bwd)
     cell_out = hidden_fwd + flip_tokens(hidden_bwd)
     gate_open = jax.nn.sigmoid(m_out.astype(jnp.float32)).reshape(tok_rows, local_heads, M_DIM)
     cell_rows = jnp.transpose(cell_out, (1, 0, 2)) * gate_open
@@ -350,12 +346,14 @@
     )
 
 
-def vmem_call(kernel, outs, scratch=(), smem=0, n_in=0, flops=0):
+def vmem_call(kernel, outs, scratch=(), smem=0, n_in=0, flops=0, n_any=0, n_tail=0):
     return pl.pallas_call(
         kernel,
         out_shape=outs,
         in_specs=[pl.BlockSpec(memory_space=pltpu.SMEM)] * smem
-        + [pl.BlockSpec(memory_space=pltpu.VMEM)] * n_in,
+        + [pl.BlockSpec(memory_space=pltpu.VMEM)] * n_in
+        + [pl.BlockSpec(memory_space=pl.ANY)] * n_any
+        + [pl.BlockSpec(memory_space=pltpu.VMEM)] * n_tail,
         out_specs=jax.tree.map(lambda _: pl.BlockSpec(memory_space=pltpu.VMEM), outs),
         scratch_shapes=scratch,
         cost_estimate=pl.CostEstimate(flops=flops, bytes_accessed=0, transcendentals=0),
@@ -363,24 +361,30 @@
     )
 
 
-def pack_kernel(mq, mk, mv, mo, aq, ak, av, small, out):
-    halves, heads = out.shape[0], out.shape[1]
-    rows = mq.shape[0] // halves
-    for u in range(halves):
-        for h in range(heads):
-            for c, ref in enumerate((mq, mk, mv, mo, aq)):
-                out[u, h, c * rows : (c + 1) * rows, :] = ref[
-                    u * rows : (u + 1) * rows, h * LANES : (h + 1) * LANES
-                ]
-            pair = jnp.concatenate(
-                [
-                    ref[u * rows : (u + 1) * rows, h * W_DIM : (h + 1) * W_DIM]
-                    for ref in (ak, av)
-                ],
-                axis=1,
+def pack_kernel(meta, mq, mk, mv, mo, aq, ak, av, small, keep, send):
+    t = meta[0]
+    copies, heads = keep.shape[0], keep.shape[2]
+    rows = mq.shape[0] // 2
+    at = pl.multiple_of(t * rows, rows)
+    away = pl.multiple_of((1 - t) * rows, rows)
+    for h in range(heads):
+        lanes = slice(h * LANES, (h + 1) * LANES)
+        narrow = slice(h * W_DIM, (h + 1) * W_DIM)
+        for start, mine in ((at, True), (away, False)):
+            parts = [ref[pl.ds(start, rows), lanes] for ref in (mq, mk, mv, mo, aq)]
+            parts.append(
+                jnp.concatenate([ref[pl.ds(start, rows), narrow] for ref in (ak, av)], axis=1)
             )
-            out[u, h, 5 * rows : 6 * rows, :] = pair
-            out[u, h, 6 * rows :, :] = small[u, h]
+            parts.append(small[t if mine else 1 - t, h])
+            row = 0
+            for part in parts:
+                span = slice(row, row + part.shape[0])
+                row += part.shape[0]
+                if mine:
+                    for i in range(copies):
+                        keep[i, t, h, span, :] = part
+                else:
+                    send[h, span, :] = part
 
 
 def chunk_vecs(rows):
@@ -405,7 +409,7 @@
     new_peak = jnp.maximum(total + peak, jnp.max(end_row, axis=1, keepdims=True))
     weighted = key * jnp.exp(end_col - new_peak)
     fade = jnp.exp(total + peak - new_peak)
-    cell = fade * cell + mm(weighted, value, 0, 0, HIGHEST)
+    cell = fade * cell + mm(weighted.astype(jnp.bfloat16), value, 0, 0)
     norm = fade * norm + jnp.sum(weighted, axis=0, keepdims=True)
     return cell, norm, new_peak
 
@@ -427,30 +431,46 @@
 
 
 def project_kernel(meta, bias, *refs):
-    plan_plane = 4
-    xs = refs[:plan_plane]
-    own, partner, gate_t, decay, proj, gates, summary, halo, weight = refs[plan_plane:]
-    t, k, sel, jl = meta[0], meta[1], meta[2], meta[3]
+    plane = (len(refs) - 11) // 2
+    same, other = refs[:plane], refs[plane : 2 * plane]
+    own, partner, gate_t, decay, proj, gates, summary, weight, xs, raw, sems = refs[2 * plane :]
+    t, k, sel, jl, near = meta[0], meta[1], meta[2], meta[3], meta[5]
+    copies = [
+        pltpu.make_async_copy(own, raw.at[0], sems.at[plane]),
+        pltpu.make_async_copy(partner, raw.at[1], sems.at[plane + 1]),
+    ]
+    for copy in copies:
+        copy.start()
+
+    @pl.when(t == near)
+    def _():
+        for r in range(plane):
+            pltpu.make_async_copy(same[r], xs.at[r], sems.at[r]).start()
+
+    @pl.when(t != near)
+    def _():
+        for r in range(plane):
+            pltpu.make_async_copy(other[r], xs.at[r], sems.at[r]).start()
+
+    for copy in copies:
+        copy.wait()
     sources = own.shape[0]
     rows = weight.shape[0] // sources // 2
     cols = weight.shape[1] // LANES
-
-    def place(i, carry):
+    for i in range(sources):
         for c in range(cols):
             lanes = slice(c * LANES, (c + 1) * LANES)
             span = slice(c * rows, (c + 1) * rows)
             first = pl.multiple_of((2 * i + t) * rows, rows)
             second = pl.multiple_of((2 * i + 1 - t) * rows, rows)
-            weight[pl.ds(first, rows), lanes] = own[i, span, :]
-            weight[pl.ds(second, rows), lanes] = partner[i, span, :]
-        return carry
-
-    lax.fori_loop(0, sources, place, 0)
-    tok = xs[0].shape[0]
-    for r, x in enumerate(xs):
+            weight[pl.ds(first, rows), lanes] = raw[0, i, span, :]
+            weight[pl.ds(second, rows), lanes] = raw[1, i, span, :]
+    tok = xs.shape[1]
+    for r in range(plane):
+        pltpu.make_async_copy(same[r], xs.at[r], sems.at[r]).wait()
         at = pl.ds(pl.multiple_of((k ^ r) * tok, tok), tok)
-        proj[at, :] = mm(x[...], weight[...]).astype(jnp.bfloat16)
-        gates[k ^ r] = mm(gate_t[...], x[...], 1, 1)[:8]
+        proj[at, :] = mm(xs[r], weight[...]).astype(jnp.bfloat16)
+        gates[k ^ r] = jnp.transpose(mm(xs[r], gate_t[...], 1, 1))[:8]
     heads = bias.shape[1] // 4
     b = [bias[sel, g * heads + jl] for g in range(4)]
     lead = jnp.concatenate([jnp.full((1, tok), b[g], jnp.float32) for g in range(4)], axis=0)
@@ -459,7 +479,7 @@
     total_f = jnp.zeros((1, 1), jnp.float32)
     total_b = jnp.zeros((1, 1), jnp.float32)
     chunks = []
-    for c in range(plan_plane):
+    for c in range(plane):
         g = gates[c][:4] + lead
         d = decay[c]
         extra = jnp.concatenate([d[0:1], d[0:1], d[1:2], d[1:2]], axis=0)
@@ -469,7 +489,7 @@
         vecs = chunk_vecs(gates[c])
         span = slice(c * tok, (c + 1) * tok)
         key = proj[span, LANES : 2 * LANES].astype(jnp.float32)
-        value = proj[span, 2 * LANES : 3 * LANES].astype(jnp.float32)
+        value = proj[span, 2 * LANES : 3 * LANES]
         chunks.append((key, value, vecs))
     for key, value, vecs in chunks:
         fwd = forward_state(fwd, key, value, vecs[0])
@@ -479,7 +499,7 @@
         total_b = total_b + vecs[1][3]
     for i, ((cell, norm, peak), total) in enumerate(((fwd, total_f), (bwd, total_b))):
         summary[i, :M_DIM, :] = cell
-        summary[i, M_DIM:, :] = jnp.concatenate(
+        summary[i, M_DIM : M_DIM + 8, :] = jnp.concatenate(
             [
                 norm,
                 jnp.broadcast_to(peak, (1, LANES)),
@@ -489,8 +509,8 @@
             axis=0,
         )
     last = proj.shape[0]
-    halo[0] = proj[:WINDOW, 5 * LANES :].astype(jnp.float32)
-    halo[1] = proj[last - WINDOW :, 5 * LANES :].astype(jnp.float32)
+    summary[0, M_DIM + 8 :, :] = proj[:WINDOW, 5 * LANES :].astype(jnp.float32)
+    summary[1, M_DIM + 8 :, :] = proj[last - WINDOW :, 5 * LANES :].astype(jnp.float32)
 
 
 def read_state(ref, i):
@@ -509,7 +529,7 @@
     return old * earlier[0] + new * later[0], old * earlier[1] + new * later[1], peak
 
 
-def combine_kernel(meta, own, partner, halo_partner, out):
+def combine_kernel(meta, own, partner, out):
     t, hi = meta[0], meta[4]
     forward = hi == 0
     i = jnp.where(forward, 0, 1)
@@ -522,10 +542,10 @@
     out[M_DIM : M_DIM + 8, :] = jnp.concatenate(
         [norm, jnp.broadcast_to(peak, (1, LANES)), jnp.zeros((6, LANES), jnp.float32)], axis=0
     )
-    out[M_DIM + 8 :, :] = halo_partner[jnp.where(forward, 1, 0)]
-
-
-def mixer_kernel(meta, sink, proj, gates, partner, halo_partner, across, gain, out_m, out_a, kv, logs):
+    out[M_DIM + 8 :, :] = partner[jnp.where(forward, 1, 0), M_DIM + 8 :, :]
+
+
+def mixer_kernel(meta, sink, proj, gates, partner, across, gain, keep, send, kv, logs):
     t, sel, jl, hi = meta[0], meta[2], meta[3], meta[4]
     chunks = gates.shape[0]
     tok = gates.shape[2]
@@ -551,8 +571,18 @@
         span = slice(c * tok, (c + 1) * tok)
         return (
             proj[span, LANES : 2 * LANES].astype(jnp.float32),
-            proj[span, 2 * LANES : 3 * LANES].astype(jnp.float32),
+            proj[span, 2 * LANES : 3 * LANES],
         )
+
+    def store(is_cell, c, span, value):
+        @pl.when((t == 0) == is_cell)
+        def _():
+            keep[t, c, span, :] = value
+
+        @pl.when((t == 0) != is_cell)
+        def _():
+            send[c, span, :] = value
+
 
     back_states = [None] * chunks
     for c in range(chunks - 1, -1, -1):
@@ -585,20 +615,22 @@
             )
             inv = 1.0 / jnp.maximum(jnp.abs(denom), jnp.exp(-(lead_col + top)))
             part = w * inv
-            add = mm(qf, cell, 1, 0, HIGHEST) * (scale * w_in * inv)
+            high = cell.astype(jnp.bfloat16)
+            low = (cell - high.astype(jnp.float32)).astype(jnp.bfloat16)
+            add = (mm(q, high) + mm(q, low)) * (scale * w_in * inv)
             total_w = part if total_w is None else total_w + part
             inter = add if inter is None else inter + add
         key, value = kv_of(c)
-        cell_out = mm(scores * total_w, value, 1, 0, HIGHEST) + inter
+        cell_out = mm((scores * total_w).astype(jnp.bfloat16), value) + inter
         fwd = forward_state(fwd, key, value, vecs[c][0])
         gate = proj[span, 3 * LANES : 4 * LANES].astype(jnp.float32)
         u = cell_out / (1.0 + jnp.exp(-gate))
         u = u * lax.rsqrt(jnp.mean(u * u, axis=1, keepdims=True) + EPS) * gain_row
-        out_m[c, :tok, :] = u.astype(jnp.bfloat16)
-        out_m[c, tok:, :] = jnp.zeros((out_m.shape[1] - tok, LANES), jnp.bfloat16)
+        store(True, c, slice(0, tok), u.astype(jnp.bfloat16))
+        store(True, c, slice(tok, tok + 16), jnp.zeros((16, LANES), jnp.bfloat16))
 
     length = proj.shape[0]
-    inner_edge = halo_partner[jnp.where(t == 0, 0, 1)].astype(jnp.bfloat16)
+    inner_edge = partner[jnp.where(t == 0, 0, 1), M_DIM + 8 :, :].astype(jnp.bfloat16)
     outer_edge = across[M_DIM + 8 :, :].astype(jnp.bfloat16)
     kv[:WINDOW, :] = jnp.where(t == 0, outer_edge, inner_edge)
     kv[WINDOW : WINDOW + length, :] = proj[:, 5 * LANES :]
@@ -636,33 +668,51 @@
             log_row = jnp.sum(jnp.where(diag, log_col, 0.0), axis=0, keepdims=True)
             at = h * per + b % per
             logs[b // per, at : at + 1, :] = log_row
-        out_a[b // per, (b % per) * WINDOW : (b % per + 1) * WINDOW, :] = jnp.concatenate(
-            mixed, axis=1
-        ).astype(jnp.bfloat16)
+        span = slice((b % per) * WINDOW, (b % per + 1) * WINDOW)
+        store(False, b // per, span, jnp.concatenate(mixed, axis=1).astype(jnp.bfloat16))
     for c in range(chunks):
         x = logs[c]
         high = x.astype(jnp.bfloat16).astype(jnp.float32)
         mid = (x - high).astype(jnp.bfloat16).astype(jnp.float32)
         low = x - high - mid
         n = x.shape[0]
-        pad = jnp.zeros((out_a.shape[1] - tok - 3 * n, LANES), jnp.float32)
-        out_a[c, tok:, :] = jnp.concatenate([high, mid, low, pad], axis=0).astype(jnp.bfloat16)
-
-
-def output_kernel(meta, own, partner, weight, mixed, log_total, left):
-    t = meta[0]
+        pad = jnp.zeros((16 - 3 * n, LANES), jnp.float32)
+        tail = jnp.concatenate([high, mid, low, pad], axis=0).astype(jnp.bfloat16)
+        store(False, c, slice(tok, tok + 16), tail)
+
+
+def output_kernel(meta, own, partner, *refs):
+    mixed, log_total, left, weight, sems = refs[-5:]
+    blocks = refs[:-5]
+    t, p, z = meta[0], meta[1], meta[6]
+    plane = len(blocks)
     heads, tok = own.shape[0], mixed.shape[0]
+    planes = sems.shape[0] // plane
+    rows = blocks[0].shape[0] // planes
+    half = rows // 2
+    total = weight.shape[0] // 2
+    copies = []
+    for r in range(plane):
+        for zr in range(planes):
+            source = (z ^ zr) * plane + (p ^ r)
+            for i in range(2):
+                to = pl.multiple_of(i * total + source * half, half)
+                copies.append(
+                    pltpu.make_async_copy(
+                        blocks[r].at[pl.ds(zr * rows + i * half, half)],
+                        weight.at[pl.ds(to, half)],
+                        sems.at[r * planes + zr, i],
+                    )
+                )
+    for copy in copies:
+        copy.start()
     for j in range(heads):
         left[t * heads + j] = own[j, :tok, :]
         left[(1 - t) * heads + j] = partner[j, :tok, :]
     lhs = jnp.concatenate([left[i] for i in range(2 * heads)], axis=1)
-    half = weight.shape[1] // 2
-    rhs = jnp.concatenate(
-        [weight[s, :half, :] for s in range(weight.shape[0])]
-        + [weight[s, half:, :] for s in range(weight.shape[0])],
-        axis=0,
-    )
-    mixed[...] = mm(lhs, rhs).astype(jnp.bfloat16)
+    for copy in copies:
+        copy.wait()
+    mixed[...] = mm(lhs, weight[...]).astype(jnp.bfloat16)
     per = tok // LANES
     n = 2 * per
     for i in range(heads // 2):
@@ -708,25 +758,28 @@
     t = lax.axis_index("tp").astype(jnp.int32)
     hi, j = s // group, s % group
     near_plane = (s // plane) % 2
-    meta = jnp.stack([t, s % plane, jnp.where(j // lh == t, 0, 1), j % lh, hi]).astype(jnp.int32)
+    meta = jnp.stack(
+        [t, s % plane, jnp.where(j // lh == t, 0, 1), j % lh, hi, near_plane, s // plane]
+    ).astype(jnp.int32)
     swap = [(0, 1), (1, 0)]
 
     def flip(x):
         return lax.ppermute(x, "tp", swap)
 
     normed = rms_rows(tokens.astype(f32), input_norm_gain).astype(bf16)
-    out_full = lax.all_gather(
-        jnp.concatenate([out_m_weight, out_a_weight], axis=0), "sp", axis=0, tiled=True
-    ).reshape(sp, 2 * out_m_weight.shape[0], out_m_weight.shape[1])
-
-    cross = [
-        (2 * a + (a // plane) % 2, 2 * (a ^ plane) + (a // plane) % 2) for a in range(sp)
-    ]
-    other = lax.ppermute(normed, ("sp", "tp"), cross)
-    base = jnp.where(t == near_plane, normed, other)
-    xs = [base] + [
-        lax.ppermute(base, "sp", [(a, a ^ r) for a in range(sp)]) for r in range(1, plane)
-    ]
+
+    def core(a, same):
+        return 2 * a + ((a // plane) % 2 if same else 1 - (a // plane) % 2)
+
+    both_axes = ("sp", "tp")
+    other = lax.ppermute(
+        normed, both_axes, [(core(a, True), core(a ^ plane, False)) for a in range(sp)]
+    )
+    same_xs, other_xs = [normed], [other]
+    for r in range(1, plane):
+        same_xs.append(
+            lax.ppermute(normed, both_axes, [(core(a, True), core(a ^ r, True)) for a in range(sp)])
+        )
 
     gate_rows = jnp.transpose(gate_weight.reshape(2, half, 4, lh), (0, 3, 2, 1)).reshape(
         2, lh, 4 * half // LANES, LANES
@@ -737,23 +790,36 @@
     small = jnp.concatenate([gate_rows, decay_rows], axis=2)
     n_gate, n_small = gate_rows.shape[2], small.shape[2]
     n_rows = 6 * half + n_small
-    packed = vmem_call(
-        pack_kernel, jax.ShapeDtypeStruct((2, lh, n_rows, LANES), bf16), n_in=8
-    )(mq_weight, mk_weight, mv_weight, mo_weight, aq_weight, ak_weight, av_weight, small)
-    keep = lax.dynamic_index_in_dim(packed, t, 0, keepdims=False)
-    got = flip(lax.dynamic_index_in_dim(packed, 1 - t, 0, keepdims=False))
-    by_head = jnp.concatenate(
-        [jnp.where(t == 0, keep, got), jnp.where(t == 0, got, keep)], axis=0
-    )
-    spread = jnp.concatenate([by_head, by_head], axis=0).reshape(sp * n_rows, LANES)
-    own_w = lax.all_to_all(spread, "sp", 0, 0, tiled=True)
+    spread, send = vmem_call(
+        pack_kernel,
+        (
+            jax.ShapeDtypeStruct((2, 2, lh, n_rows, LANES), bf16),
+            jax.ShapeDtypeStruct((lh, n_rows, LANES), bf16),
+        ),
+        smem=1,
+        n_in=8,
+    )(meta, mq_weight, mk_weight, mv_weight, mo_weight, aq_weight, ak_weight, av_weight, small)
+    got = flip(send)
+    got = jnp.broadcast_to(got[None, None], (2, 1) + got.shape)
+    spread = lax.dynamic_update_slice_in_dim(spread, got, 1 - t, 1)
+    own_w = lax.all_to_all(spread.reshape(sp * n_rows, LANES), "sp", 0, 0, tiled=True)
+    for r in range(1, plane):
+        other_xs.append(
+            lax.ppermute(
+                other, both_axes, [(core(a, False), core(a ^ r, False)) for a in range(sp)]
+            )
+        )
+    out_block = jnp.concatenate([out_m_weight, out_a_weight], axis=0)
+    column = [out_block]
+    for r in range(1, sp // plane):
+        column.append(lax.ppermute(out_block, "sp", [(a, a ^ (r * plane)) for a in range(sp)]))
     partner_w = flip(own_w)
     own_w = own_w.reshape(sp, n_rows, LANES)
     partner_w = partner_w.reshape(sp, n_rows, LANES)
     small_both = jnp.stack([own_w[:, 6 * half :], partner_w[:, 6 * half :]])
     small_both = jnp.where(t == 0, small_both, small_both[::-1])
     gate_t = jnp.transpose(small_both[:, :, :n_gate].reshape(2, sp, 4, half), (2, 1, 0, 3))
-    gate_t = jnp.pad(gate_t.reshape(4, width), ((0, 12), (0, 0)))
+    gate_t = jnp.pad(gate_t.reshape(4, width), ((0, LANES - 4), (0, 0)))
     first = (2 * hi + t) * plane
     decay = lax.dynamic_slice_in_dim(small_both[:, :, n_gate:], first, plane, 1)
     decay = jnp.sum(decay.reshape(2, plane, 3, tok).astype(f32), axis=2)
@@ -768,61 +834,78 @@
 
     quarter = plane * tok
     cols = 6 * LANES
-    proj, gates, summary, halo = vmem_call(
+    sum_rows = M_DIM + 8 + WINDOW
+    proj, gates, summary = vmem_call(
         project_kernel,
         (
             jax.ShapeDtypeStruct((quarter, cols), bf16),
             jax.ShapeDtypeStruct((plane, 8, tok), f32),
-            jax.ShapeDtypeStruct((2, M_DIM + 8, LANES), f32),
-            jax.ShapeDtypeStruct((2, WINDOW, LANES), f32),
+            jax.ShapeDtypeStruct((2, sum_rows, LANES), f32),
         ),
-        scratch=[pltpu.VMEM((width, cols), bf16)],
+        scratch=[
+            pltpu.VMEM((width, cols), bf16),
+            pltpu.VMEM((plane, tok, width), bf16),
+            pltpu.VMEM((2, sp, n_rows, LANES), bf16),
+            pltpu.SemaphoreType.DMA((plane + 2,)),
+        ],
         smem=2,
-        n_in=plane + 4,
+        n_any=2 * plane + 2,
+        n_tail=2,
         flops=2 * quarter * width * cols,
-    )(meta, bias, *xs, own_w, partner_w, gate_t, decay)
-    both = flip(jnp.concatenate([summary, halo], axis=1))
-    partner_sum, partner_halo = both[:, : M_DIM + 8], both[:, M_DIM + 8 :]
+    )(meta, bias, *same_xs, *other_xs, own_w, partner_w, gate_t, decay)
+    column = jnp.concatenate(column, axis=0)
+    out_blocks = [column]
+    for r in range(1, plane):
+        out_blocks.append(lax.ppermute(column, "sp", [(a, a ^ r) for a in range(sp)]))
+    partner_sum = flip(summary)
     sent = vmem_call(
-        combine_kernel,
-        jax.ShapeDtypeStruct((M_DIM + 8 + WINDOW, LANES), f32),
-        smem=1,
-        n_in=3,
-    )(meta, summary, partner_sum, partner_halo)
+        combine_kernel, jax.ShapeDtypeStruct((sum_rows, LANES), f32), smem=1, n_in=2
+    )(meta, summary, partner_sum)
     across = lax.ppermute(sent, "sp", [(a, (a + group) % sp) for a in range(sp)])
-    part = jax.ShapeDtypeStruct((plane, tok + 16, LANES), bf16)
-    out_m, out_a = vmem_call(
+    spread, send = vmem_call(
         mixer_kernel,
-        (part, part),
+        (
+            jax.ShapeDtypeStruct((2, plane, tok + 16, LANES), bf16),
+            jax.ShapeDtypeStruct((plane, tok + 16, LANES), bf16),
+        ),
         scratch=[
             pltpu.VMEM((quarter + 2 * WINDOW, LANES), bf16),
             pltpu.VMEM((plane, 2 * tok // WINDOW, LANES), f32),
         ],
         smem=2,
-        n_in=6,
+        n_in=5,
         flops=2 * quarter * width * cols,
-    )(meta, sink, proj, gates, partner_sum, partner_halo, across, gain)
-
-    lead = jnp.where(t == 0, out_m, out_a)
-    got = flip(jnp.where(t == 0, out_a, out_m))
-    spread = jnp.concatenate(
-        [jnp.where(t == 0, lead, got), jnp.where(t == 0, got, lead)], axis=0
-    ).reshape(group * (tok + 16), LANES)
+    )(meta, sink, proj, gates, partner_sum, across, gain)
+    got = flip(send)
+    spread = lax.dynamic_update_slice_in_dim(spread, got[None], 1 - t, 0)
     groups = [list(range(g * group, (g + 1) * group)) for g in range(sp // group)]
-    mine = lax.all_to_all(spread, "sp", 0, 0, axis_index_groups=groups, tiled=True)
+    mine = lax.all_to_all(
+        spread.reshape(group * (tok + 16), LANES),
+        "sp",
+        0,
+        0,
+        axis_index_groups=groups,
+        tiled=True,
+    )
     theirs = flip(mine)
     shape = (group, tok + 16, LANES)
+    inner = 2 * group * LANES
     return vmem_call(
         output_kernel,
         (
             jax.ShapeDtypeStruct((tok, out_m_weight.shape[1]), bf16),
             jax.ShapeDtypeStruct((2 * lh, tok), f32),
         ),
-        scratch=[pltpu.VMEM((2 * group, tok, LANES), bf16)],
+        scratch=[
+            pltpu.VMEM((2 * group, tok, LANES), bf16),
+            pltpu.VMEM((inner, out_m_weight.shape[1]), bf16),
+            pltpu.SemaphoreType.DMA((sp, 2)),
+        ],
         smem=1,
-        n_in=3,
-        flops=2 * tok * width * out_m_weight.shape[1],
-    )(meta, mine.reshape(shape), theirs.reshape(shape), out_full)
+        n_in=2,
+        n_any=plane,
+        flops=2 * tok * inner * out_m_weight.shape[1],
+    )(meta, mine.reshape(shape), theirs.reshape(shape), *out_blocks)
 
 
 def solution(mesh):
@@ -845,9 +928,12 @@
         P("sp", "tp"),
     )
     out_specs = (P("sp", "tp"), P("tp", "sp"))
+
     def per_device(*args):
         plan = split_plan(mesh, args)
-        return on_device(*args) if plan is None else on_device_split(plan, *args)
+        if plan is None:
+            return on_device(*args)
+        return on_device_split(plan, *args)
 
     return jax.shard_map(
         per_device, mesh=mesh, in_specs=in_specs, out_specs=out_specs, check_vma=False

time: 226 us -> 243 us (1.075)
  waiting for transfers between devices: 103 us -> 130 us
  starting transfers between devices: 31 us -> 55.9 us
  blocking collectives: 13.4 us -> 0 us
  between operations: 14.2 us -> 1.2 us
  other arithmetic: 12.5 us -> 5.07 us
    ppermute x4 -> x13, waiting for transfers between devices: 57.6 us -> 85.8 us  [the longest x3 44.9 us: on_device_split(): lax.ppermute(column, 'sp', [(a, a ^ r) for a in range(sp)])]
    ppermute x4 -> x13, starting transfers between devices: 8.52 us -> 29.7 us  [the longest x3 9.22 us: on_device_split(): lax.ppermute(normed, both_axes, [(core(a, True), core(a ^ r, True)) for a...]
    all_to_all x1 -> x0, blocking collectives: 13.4 us -> none  [on_device_split(): lax.all_to_all(spread, 'sp', 0, 0, axis_index_groups=groups, tiled=True)]
    select_n x4 -> x0, other arithmetic: 4.47 us -> none  [the longest x1 1.42 us: on_device_split(): base = jnp.where(t == near_plane, normed, other)]
    all_to_all x1 -> x2, starting transfers between devices: 8.37 us -> 11.9 us  [the longest x1 8.35 us: on_device_split(): lax.all_to_all(spread.reshape(sp * n_rows, LANES), 'sp', 0, 0, tiled=True)]
    ppermute x6, waiting for transfers between devices: 6.29 us -> 2.97 us  [flip(): return lax.ppermute(x, 'tp', swap)]
    concatenate x4 -> x0, other arithmetic: 3.14 us -> none  [the longest x1 1.39 us: on_device_split(): jnp.concatenate([by_head, by_head], axis=0).reshape(sp * n_rows, LANES)]
    ppermute x6, starting transfers between devices: 10.4 us -> 13.3 us  [flip(): return lax.ppermute(x, 'tp', swap)]
  transfers between devices with their start and end apart: 13 -> 22, of which waited for: 11 -> 13; matrix products, arithmetic and copies ran while one was open for 6% -> 3% of each run, Pallas kernels for 16% -> 0%
where the time goes in v2:
time: 243 us; the launch traced here: 242 us
  waiting for transfers between devices  130 us (53%)
  starting transfers between devices  55.9 us (23%)
  Pallas kernels  41.8 us (17%)
  local copies, waits for them, and re-layouts  8.18 us (3%)
  other arithmetic  5.07 us (2%)
    ppermute x3, waiting for transfers between devices, on_device_split(): lax.ppermute(column, 'sp', [(a, a ^ r) for a in range(sp)])  44.9 us
    all_to_all x1, waiting for transfers between devices, on_device_split(): lax.all_to_all(spread.reshape(sp * n_rows, LANES), 'sp', 0, 0, tiled=True)  34.5 us
    ppermute x3, waiting for transfers between devices, on_device_split(): lax.ppermute(normed, both_axes, [(core(a, True), core(a ^ r, True)) for a...  20.2 us
    pallas_call x1, Pallas kernels, on_device_split(): vmem_call(mixer_kernel, (jax.ShapeDtypeStruct((2, plane, tok + 16, LANES)...  18.9 us
    ppermute x3, waiting for transfers between devices, on_device_split(): lax.ppermute(out_block, 'sp', [(a, a ^ r * plane) for a in range(sp)])  17.5 us
    ppermute x6, starting transfers between devices, flip(): return lax.ppermute(x, 'tp', swap)  13.3 us
    pallas_call x1, Pallas kernels, on_device_split(): vmem_call(project_kernel, (jax.ShapeDtypeStruct((quarter, cols), bf16), j...  12.6 us
    ppermute x3, starting transfers between devices, on_device_split(): lax.ppermute(normed, both_axes, [(core(a, True), core(a ^ r, True)) for a...  9.22 us
  transfers between devices with their start and end apart: 22, of which 13 were waited for; matrix products, arithmetic and copies ran while one was open for 3% of the time, Pallas kernels for 0%

profile of v2, /device:TPU:0, one launch (start us, length us, event | category | flops | bytes accessed | tf_op | source)
XLA Modules:
  0.0 241.8 jit_solution(17256532330659445764)
XLA Ops:
  0.7 0.7 fusion.5
  1.5 0.8 reshape.60
  2.3 0.1 reshape.61
  2.3 0.6 pad_maximum_fusion.1.small
  3.0 0.7 stack.62.meta
  3.6 2.7 %shard_map.167 = (bf16[2,2,4,392,128]{4,3,2,1,0:T(8,128)(2,1)}, bf16[4,392,128]{2,1,0:T(8,128)(2,1)}) custom-call(s32[7]{0:T(128)} %stack.62.meta, bf16[128,512]{1,0:T(8,128)(2,1)} %mq.1, bf16[128,512]{1,0:T(8,128)(2,1)} %mk.1, bf16[128,512]{1,0:T(8,128)(2,1)} %mv.1, bf16[128,512]{1,0:T(8,128)(2,1)} %mo.1, bf16[128,512]{1,0:T(8,128)(2,1)} %aq.1, ...), custom_call_target="tpu_custom_call" | custom-call | tf_op jit(solution)/shard_map/pallas_call | solution.py:793
  6.3 0.5 collective-permute-start.8
  6.8 1.6 collective-permute-done.8
  8.4 1.0 broadcast_dynamic-update-slice_fusion
  9.4 8.4 %all-to-all-start = ((bf16[16,392,128]{2,1,0:T(8,128)(2,1)}), bf16[16,392,128]{2,1,0:T(8,128)(2,1)S(1)}, u32[]{:S(2)}, u32[]{:S(2)}) async-start(bf16[16,392,128]{2,1,0:T(8,128)(2,1)} %bitcast.47), calls=%async_computation | async-start | bytes 3211264 | tf_op jit(solution)/shard_map/all_to_all | solution.py:805
  17.7 0.0 copy-start.11
  17.7 0.0 copy-start.12
  17.7 0.0 copy-start.13
  17.8 0.3 fusion
  18.0 34.5 %all-to-all-done.refs_8_ = bf16[16,392,128]{2,1,0:T(8,128)(2,1)S(1)} async-done(((bf16[16,392,128]{2,1,0:T(8,128)(2,1)}), bf16[16,392,128]{2,1,0:T(8,128)(2,1)S(1)}, u32[]{:S(2)}, u32[]{:S(2)}) %all-to-all-start) | async-done | bytes 1605664 | tf_op jit(solution)/shard_map/all_to_all | solution.py:805
  52.5 1.5 fusion.2.refs_0_
  54.0 6.8 %collective-permute-start.4 = (bf16[256,2048]{1,0:T(8,128)(2,1)}, bf16[256,2048]{1,0:T(8,128)(2,1)S(1)}, u32[]{:S(2)}, u32[]{:S(2)}) collective-permute-start(bf16[256,2048]{1,0:T(8,128)(2,1)} %fusion.2.refs_0_), channel_id=1, source_target_pairs={{0,8},{2,10},{4,12},{6,14},{9,1},{11,3},{13,5},{15,7},{16,24},{18,... | collective-permute-start | bytes 3145736 | tf_op jit(solution)/shard_map/ppermute | solution.py:775
  60.8 3.0 %collective-permute-start.1 = (bf16[256,2048]{1,0:T(8,128)(2,1)}, bf16[256,2048]{1,0:T(8,128)(2,1)}, u32[]{:S(2)}, u32[]{:S(2)}) collective-permute-start(bf16[256,2048]{1,0:T(8,128)(2,1)} %fusion.2.refs_0_), channel_id=1, source_target_pairs={{0,2},{2,0},{4,6},{6,4},{9,11},{11,9},{13,15},{15,13},{16,18},{18,... | collective-permute-start | bytes 3145736 | tf_op jit(solution)/shard_map/ppermute | solution.py:781
  63.8 0.1 reshape.58
  63.9 0.1 fusion.8
  64.0 0.0 collective-permute-start
  64.0 3.7 %collective-permute-start.2 = (bf16[256,2048]{1,0:T(8,128)(2,1)}, bf16[256,2048]{1,0:T(8,128)(2,1)}, u32[]{:S(2)}, u32[]{:S(2)}) collective-permute-start(bf16[256,2048]{1,0:T(8,128)(2,1)} %fusion.2.refs_0_), channel_id=1, source_target_pairs={{0,4},{2,6},{4,0},{6,2},{9,13},{11,15},{13,9},{15,11},{16,20},{18,... | collective-permute-start | bytes 3145736 | tf_op jit(solution)/shard_map/ppermute | solution.py:781
  67.7 0.0 collective-permute-done
  67.7 2.6 %collective-permute-start.3 = (bf16[256,2048]{1,0:T(8,128)(2,1)}, bf16[256,2048]{1,0:T(8,128)(2,1)}, u32[]{:S(2)}, u32[]{:S(2)}) collective-permute-start(bf16[256,2048]{1,0:T(8,128)(2,1)} %fusion.2.refs_0_), channel_id=1, source_target_pairs={{0,6},{2,4},{4,2},{6,0},{9,15},{11,13},{13,11},{15,9},{16,22},{18,... | collective-permute-start | bytes 3145736 | tf_op jit(solution)/shard_map/ppermute | solution.py:781
  70.3 3.1 %collective-permute-done.4.refs_4_ = bf16[256,2048]{1,0:T(8,128)(2,1)S(1)} collective-permute-done((bf16[256,2048]{1,0:T(8,128)(2,1)}, bf16[256,2048]{1,0:T(8,128)(2,1)S(1)}, u32[]{:S(2)}, u32[]{:S(2)}) %collective-permute-start.4) | collective-permute-done | bytes 1048608 | tf_op jit(solution)/shard_map/ppermute | solution.py:775
  73.4 1.7 collective-permute-start.5
  75.0 3.1 %collective-permute-done.1.refs_1_ = bf16[256,2048]{1,0:T(8,128)(2,1)} collective-permute-done((bf16[256,2048]{1,0:T(8,128)(2,1)}, bf16[256,2048]{1,0:T(8,128)(2,1)}, u32[]{:S(2)}, u32[]{:S(2)}) %collective-permute-start.1) | collective-permute-done | bytes 1048608 | tf_op jit(solution)/shard_map/ppermute | solution.py:781
  78.1 1.7 collective-permute-start.6
  79.8 1.7 collective-permute-start.7
  81.5 0.6 pad_maximum_fusion.4
  82.1 0.8 slice_bitcast_fusion
  82.9 0.1 reshape.64
  83.0 0.1 reshape.65
  83.2 0.6 copy.32
  83.8 0.8 pad.4.refs_10_
  84.7 2.3 collective-permute-done.2.refs_2_
  87.0 14.8 %collective-permute-done.3.refs_3_ = bf16[256,2048]{1,0:T(8,128)(2,1)} collective-permute-done((bf16[256,2048]{1,0:T(8,128)(2,1)}, bf16[256,2048]{1,0:T(8,128)(2,1)}, u32[]{:S(2)}, u32[]{:S(2)}) %collective-permute-start.3) | collective-permute-done | bytes 1048608 | tf_op jit(solution)/shard_map/ppermute | solution.py:781
  101.9 12.6 %shard_map.168 = (bf16[1024,768]{1,0:T(8,128)(2,1)}, f32[4,8,256]{2,1,0:T(8,128)}, f32[2,264,128]{2,1,0:T(8,128)}) custom-call(s32[7]{0:T(128)} %stack.62.meta, f32[2,16]{1,0:T(2,128)} %bitcast.56, bf16[256,2048]{1,0:T(8,128)(2,1)} %fusion.2.refs_0_, bf16[256,2048]{1,0:T(8,128)(2,1)} %collective-permute-done.1.refs_1_, ...), custom_call_target="tpu_custom_call" | custom-call | flops 3221225472 | tf_op jit(solution)/shard_map/pallas_call | solution.py:838
  114.4 12.8 %collective-permute-start.10 = (f32[2,264,128]{2,1,0:T(8,128)}, f32[2,264,128]{2,1,0:T(8,128)S(1)}, u32[]{:S(2)}, u32[]{:S(2)}) collective-permute-start(f32[2,264,128]{2,1,0:T(8,128)} %get-tuple-element.13.own), channel_id=1, source_target_pairs={{0,1},{1,0},{2,3},{3,2},{4,5},{5,4},{6,7},{7,6},{8,9},{9,8},{10,11... | collective-permute-start | bytes 811016 | tf_op jit(solution)/shard_map/ppermute | solution.py:767
  127.2 1.4 collective-permute-done.10.partner
  128.6 0.7 copy-done.7
  129.3 1.8 shard_map.169
  131.1 1.0 collective-permute-start.11
  132.1 0.6 pad_maximum_fusion.5
  132.7 0.6 pad_maximum_fusion.2.gain
  133.3 6.5 %collective-permute-done.11.across = f32[264,128]{1,0:T(8,128)S(1)} collective-permute-done((f32[264,128]{1,0:T(8,128)}, f32[264,128]{1,0:T(8,128)S(1)}, u32[]{:S(2)}, u32[]{:S(2)}) %collective-permute-start.11) | collective-permute-done | bytes 135200 | tf_op jit(solution)/shard_map/ppermute | solution.py:864
  139.8 0.7 copy-done.14
  140.5 18.9 %shard_map.170 = (bf16[2,4,272,128]{3,2,1,0:T(8,128)(2,1)}, bf16[4,272,128]{2,1,0:T(8,128)(2,1)}) custom-call(s32[7]{0:T(128)} %stack.62.meta, f32[2,8]{1,0:T(2,128)} %bitcast.57, bf16[1024,768]{1,0:T(8,128)(2,1)} %get-tuple-element.11.proj, f32[4,8,256]{2,1,0:T(8,128)} %get-tuple-element.12.gates, f32[2,264,128]{2,1,0:T(8,128)} %copy-done.7, ...), custom_call_target="tpu_custom_call" | custom-call | flops 3221225472 | tf_op jit(solution)/shard_map/pallas_call | solution.py:865
  159.4 0.1 collective-permute-start.12
  159.6 0.1 collective-permute-start.14
  159.6 3.1 %collective-permute-start.15 = (bf16[128,1024]{1,0:T(8,128)(2,1)S(1)}, bf16[128,1024]{1,0:T(8,128)(2,1)S(1)}, u32[]{:S(2)}, u32[]{:S(2)}) collective-permute-start(bf16[128,1024]{1,0:T(8,128)(2,1)S(1)} %get-tuple-element.16), channel_id=1, source_target_pairs={{0,16},{2,18},{4,20},{6,22},{8,24},{10,26},{12,28},{14,30},{16,0},... | collective-permute-start | bytes 786440 | tf_op jit(solution)/shard_map/ppermute | solution.py:815
  162.8 0.7 bitcast_dynamic-update-slice_fusion
  163.5 3.5 %all-to-all-start.1 = ((bf16[8,272,128]{2,1,0:T(8,128)(2,1)}), bf16[8,272,128]{2,1,0:T(8,128)(2,1)S(1)}, u32[]{:S(2)}, u32[]{:S(2)}) async-start(bf16[8,272,128]{2,1,0:T(8,128)(2,1)} %bitcast.48), calls=%async_computation.1 | async-start | bytes 1114112 | tf_op jit(solution)/shard_map/all_to_all | solution.py:882
  167.1 1.9 collective-permute-start.16
  168.9 5.3 %collective-permute-done.14 = bf16[128,1024]{1,0:T(8,128)(2,1)S(1)} collective-permute-done((bf16[128,1024]{1,0:T(8,128)(2,1)S(1)}, bf16[128,1024]{1,0:T(8,128)(2,1)S(1)}, u32[]{:S(2)}, u32[]{:S(2)}) %collective-permute-start.14) | collective-permute-done | bytes 262176 | tf_op jit(solution)/shard_map/ppermute | solution.py:815
  174.2 1.2 collective-permute-done.15
  175.4 11.1 %collective-permute-done.16 = bf16[128,1024]{1,0:T(8,128)(2,1)S(1)} collective-permute-done((bf16[128,1024]{1,0:T(8,128)(2,1)S(1)}, bf16[128,1024]{1,0:T(8,128)(2,1)S(1)}, u32[]{:S(2)}, u32[]{:S(2)}) %collective-permute-start.16) | collective-permute-done | bytes 262176 | tf_op jit(solution)/shard_map/ppermute | solution.py:815
  186.5 1.2 collective-permute-start.17
  187.7 0.6 collective-permute-start.18
  188.3 1.7 collective-permute-start.19
  190.0 22.5 %collective-permute-done.17.refs_1_ = bf16[512,1024]{1,0:T(8,128)(2,1)S(1)} collective-permute-done((bf16[512,1024]{1,0:T(8,128)(2,1)S(1)}, bf16[512,1024]{1,0:T(8,128)(2,1)S(1)}, u32[]{:S(2)}, u32[]{:S(2)}) %collective-permute-start.17) | collective-permute-done | bytes 1048608 | tf_op jit(solution)/shard_map/ppermute | solution.py:859
  212.6 22.4 %collective-permute-done.18.refs_2_ = bf16[512,1024]{1,0:T(8,128)(2,1)} collective-permute-done((bf16[512,1024]{1,0:T(8,128)(2,1)S(1)}, bf16[512,1024]{1,0:T(8,128)(2,1)}, u32[]{:S(2)}, u32[]{:S(2)}) %collective-permute-start.18) | collective-permute-done | bytes 1048608 | tf_op jit(solution)/shard_map/ppermute | solution.py:859
  235.0 0.8 copy-done.6
  235.9 5.8 %shard_map.171 = (bf16[256,1024]{1,0:T(8,128)(2,1)}, f32[8,256]{1,0:T(8,128)}) custom-call(s32[7]{0:T(128)} %stack.62.meta, bf16[8,272,128]{2,1,0:T(8,128)(2,1)} %copy-done.2, bf16[8,272,128]{2,1,0:T(8,128)(2,1)} %bitcast.49, bf16[512,1024]{1,0:T(8,128)(2,1)} %copy-done.3, bf16[512,1024]{1,0:T(8,128)(2,1)} %copy-done.4, ...), custom_call_target="tpu_custom_call" | custom-call | flops 1073741824 | tf_op jit(solution)/shard_map/pallas_call | solution.py:893
  (54 shorter events, 0.4 us)
Async XLA Ops:
  6.3 2.1 collective-permute-start.8
  9.3 8.4 %copy-start.1 = (bf16[256,2048]{1,0:T(8,128)(2,1)S(1)}, bf16[256,2048]{1,0:T(8,128)(2,1)}, u32[]{:S(2)}) copy-start(bf16[256,2048]{1,0:T(8,128)(2,1)} %param.16) | copy-start | bytes 3145732
  9.3 43.2 %copy-start.10 = (f32[2048]{0:T(1024)S(1)}, f32[2048]{0:T(1024)}, u32[]{:S(2)}) copy-start(f32[2048]{0:T(1024)} %param.17) | copy-start | bytes 24580
  9.4 43.2 %all-to-all-start = ((bf16[16,392,128]{2,1,0:T(8,128)(2,1)}), bf16[16,392,128]{2,1,0:T(8,128)(2,1)S(1)}, u32[]{:S(2)}, u32[]{:S(2)}) async-start(bf16[16,392,128]{2,1,0:T(8,128)(2,1)} %bitcast.47), calls=%async_computation | async-start | bytes 3211264 | tf_op jit(solution)/shard_map/all_to_all | solution.py:805
  17.7 46.1 %copy-start.11 = (f32[4,4]{1,0:T(4,128)S(1)}, f32[4,4]{1,0:T(4,128)}, u32[]{:S(2)}) copy-start(f32[4,4]{1,0:T(4,128)} %param.23) | copy-start | bytes 196
  17.7 46.2 %copy-start.12 = (f32[512]{0:T(512)S(1)}, f32[512]{0:T(512)}, u32[]{:S(2)}) copy-start(f32[512]{0:T(512)} %param.25) | copy-start | bytes 6148
  17.7 46.2 %copy-start.13 = (f32[8]{0:T(128)S(1)}, f32[8]{0:T(128)}, u32[]{:S(2)}) copy-start(f32[8]{0:T(128)} %param.29) | copy-start | bytes 100
  52.5 32.2 %copy-start = (bf16[16,392,128]{2,1,0:T(8,128)(2,1)}, bf16[16,392,128]{2,1,0:T(8,128)(2,1)S(1)}, u32[]{:S(2)}) copy-start(bf16[16,392,128]{2,1,0:T(8,128)(2,1)S(1)} %all-to-all-done.refs_8_) | copy-start | bytes 4816900
  52.5 27.3 %collective-permute-start.9 = (bf16[6272,128]{1,0:T(8,128)(2,1)S(1)}, bf16[6272,128]{1,0:T(8,128)(2,1)}, u32[]{:S(2)}, u32[]{:S(2)}) collective-permute-start(bf16[6272,128]{1,0:T(8,128)(2,1)S(1)} %bitcast.45), channel_id=1, source_target_pairs={{0,1},{1,0},{2,3},{3,2},{4,5},{5,4},{6,7},{7,6},{8,9},{9,8},{10,11... | collective-permute-start | bytes 4816904 | tf_op jit(solution)/shard_map/ppermute | solution.py:767
  54.0 19.4 %collective-permute-start.4 = (bf16[256,2048]{1,0:T(8,128)(2,1)}, bf16[256,2048]{1,0:T(8,128)(2,1)S(1)}, u32[]{:S(2)}, u32[]{:S(2)}) collective-permute-start(bf16[256,2048]{1,0:T(8,128)(2,1)} %fusion.2.refs_0_), channel_id=1, source_target_pairs={{0,8},{2,10},{4,12},{6,14},{9,1},{11,3},{13,5},{15,7},{16,24},{18,... | collective-permute-start | bytes 3145736 | tf_op jit(solution)/shard_map/ppermute | solution.py:775
  60.8 17.3 %collective-permute-start.1 = (bf16[256,2048]{1,0:T(8,128)(2,1)}, bf16[256,2048]{1,0:T(8,128)(2,1)}, u32[]{:S(2)}, u32[]{:S(2)}) collective-permute-start(bf16[256,2048]{1,0:T(8,128)(2,1)} %fusion.2.refs_0_), channel_id=1, source_target_pairs={{0,2},{2,0},{4,6},{6,4},{9,11},{11,9},{13,15},{15,13},{16,18},{18,... | collective-permute-start | bytes 3145736 | tf_op jit(solution)/shard_map/ppermute | solution.py:781
  64.0 3.7 %collective-permute-start = (f32[5,128]{1,0:T(8,128)S(1)}, f32[5,128]{1,0:T(8,128)S(1)}, u32[]{:S(2)}, u32[]{:S(2)}) collective-permute-start(f32[5,128]{1,0:T(8,128)S(1)} %get-tuple-element.24), channel_id=1, source_target_pairs={{0,1},{1,0},{2,3},{3,2},{4,5},{5,4},{6,7},{7,6},{8,9},{9,8},{10,11... | collective-permute-start | bytes 7688 | tf_op jit(solution)/shard_map/ppermute | solution.py:767
  64.0 23.0 %collective-permute-start.2 = (bf16[256,2048]{1,0:T(8,128)(2,1)}, bf16[256,2048]{1,0:T(8,128)(2,1)}, u32[]{:S(2)}, u32[]{:S(2)}) collective-permute-start(bf16[256,2048]{1,0:T(8,128)(2,1)} %fusion.2.refs_0_), channel_id=1, source_target_pairs={{0,4},{2,6},{4,0},{6,2},{9,13},{11,15},{13,9},{15,11},{16,20},{18,... | collective-permute-start | bytes 3145736 | tf_op jit(solution)/shard_map/ppermute | solution.py:781
  67.7 34.1 %collective-permute-start.3 = (bf16[256,2048]{1,0:T(8,128)(2,1)}, bf16[256,2048]{1,0:T(8,128)(2,1)}, u32[]{:S(2)}, u32[]{:S(2)}) collective-permute-start(bf16[256,2048]{1,0:T(8,128)(2,1)} %fusion.2.refs_0_), channel_id=1, source_target_pairs={{0,6},{2,4},{4,2},{6,0},{9,15},{11,13},{13,11},{15,9},{16,22},{18,... | collective-permute-start | bytes 3145736 | tf_op jit(solution)/shard_map/ppermute | solution.py:781
  73.4 28.5 %copy-start.5 = (bf16[256,2048]{1,0:T(8,128)(2,1)}, bf16[256,2048]{1,0:T(8,128)(2,1)S(1)}, u32[]{:S(2)}) copy-start(bf16[256,2048]{1,0:T(8,128)(2,1)S(1)} %collective-permute-done.4.refs_4_) | copy-start | bytes 3145732
  73.4 28.5 %collective-permute-start.5 = (bf16[256,2048]{1,0:T(8,128)(2,1)S(1)}, bf16[256,2048]{1,0:T(8,128)(2,1)}, u32[]{:S(2)}, u32[]{:S(2)}) collective-permute-start(bf16[256,2048]{1,0:T(8,128)(2,1)S(1)} %collective-permute-done.4.refs_4_), channel_id=1, source_target_pairs={{1,3},{3,1},{5,7},{7,5},{8,10},{10,8},{12,14},{14,12},{17,19},{19,... | collective-permute-start | bytes 3145736 | tf_op jit(solution)/shard_map/ppermute | solution.py:808
  78.1 23.7 %collective-permute-start.6 = (bf16[256,2048]{1,0:T(8,128)(2,1)S(1)}, bf16[256,2048]{1,0:T(8,128)(2,1)}, u32[]{:S(2)}, u32[]{:S(2)}) collective-permute-start(bf16[256,2048]{1,0:T(8,128)(2,1)S(1)} %collective-permute-done.4.refs_4_), channel_id=1, source_target_pairs={{1,5},{3,7},{5,1},{7,3},{8,12},{10,14},{12,8},{14,10},{17,21},{19,... | collective-permute-start | bytes 3145736 | tf_op jit(solution)/shard_map/ppermute | solution.py:808
  79.8 22.1 %collective-permute-start.7 = (bf16[256,2048]{1,0:T(8,128)(2,1)S(1)}, bf16[256,2048]{1,0:T(8,128)(2,1)}, u32[]{:S(2)}, u32[]{:S(2)}) collective-permute-start(bf16[256,2048]{1,0:T(8,128)(2,1)S(1)} %collective-permute-done.4.refs_4_), channel_id=1, source_target_pairs={{1,7},{3,5},{5,3},{7,1},{8,14},{10,12},{12,10},{14,8},{17,23},{19,... | collective-permute-start | bytes 3145736 | tf_op jit(solution)/shard_map/ppermute | solution.py:808
  114.4 14.1 %collective-permute-start.10 = (f32[2,264,128]{2,1,0:T(8,128)}, f32[2,264,128]{2,1,0:T(8,128)S(1)}, u32[]{:S(2)}, u32[]{:S(2)}) collective-permute-start(f32[2,264,128]{2,1,0:T(8,128)} %get-tuple-element.13.own), channel_id=1, source_target_pairs={{0,1},{1,0},{2,3},{3,2},{4,5},{5,4},{6,7},{7,6},{8,9},{9,8},{10,11... | collective-permute-start | bytes 811016 | tf_op jit(solution)/shard_map/ppermute | solution.py:767
  128.6 0.7 copy-start.7
  131.1 8.8 %collective-permute-start.11 = (f32[264,128]{1,0:T(8,128)}, f32[264,128]{1,0:T(8,128)S(1)}, u32[]{:S(2)}, u32[]{:S(2)}) collective-permute-start(f32[264,128]{1,0:T(8,128)} %shard_map.169), channel_id=1, source_target_pairs={{0,16},{2,18},{4,20},{6,22},{8,24},{10,26},{12,28},{14,30},{16,0},... | collective-permute-start | bytes 405512 | tf_op jit(solution)/shard_map/ppermute | solution.py:864
  139.8 0.7 copy-start.14
  140.5 19.0 %copy-start.8 = (bf16[64,1024]{1,0:T(8,128)(2,1)S(1)}, bf16[64,1024]{1,0:T(8,128)(2,1)}, u32[]{:S(2)}) copy-start(bf16[64,1024]{1,0:T(8,128)(2,1)} %param.30) | copy-start | bytes 393220
  140.5 19.0 %copy-start.9 = (bf16[64,1024]{1,0:T(8,128)(2,1)S(1)}, bf16[64,1024]{1,0:T(8,128)(2,1)}, u32[]{:S(2)}) copy-start(bf16[64,1024]{1,0:T(8,128)(2,1)} %param.31) | copy-start | bytes 393220
  159.4 3.4 %collective-permute-start.12 = (bf16[4,272,128]{2,1,0:T(8,128)(2,1)}, bf16[4,272,128]{2,1,0:T(8,128)(2,1)S(1)}, u32[]{:S(2)}, u32[]{:S(2)}) collective-permute-start(bf16[4,272,128]{2,1,0:T(8,128)(2,1)} %get-tuple-element.15), channel_id=1, source_target_pairs={{0,1},{1,0},{2,3},{3,2},{4,5},{5,4},{6,7},{7,6},{8,9},{9,8},{10,11... | collective-permute-start | bytes 835592 | tf_op jit(solution)/shard_map/ppermute | solution.py:767
  159.6 14.6 %collective-permute-start.14 = (bf16[128,1024]{1,0:T(8,128)(2,1)S(1)}, bf16[128,1024]{1,0:T(8,128)(2,1)S(1)}, u32[]{:S(2)}, u32[]{:S(2)}) collective-permute-start(bf16[128,1024]{1,0:T(8,128)(2,1)S(1)} %get-tuple-element.16), channel_id=1, source_target_pairs={{0,8},{2,10},{4,12},{6,14},{8,0},{10,2},{12,4},{14,6},{16,24},{18,... | collective-permute-start | bytes 786440 | tf_op jit(solution)/shard_map/ppermute | solution.py:815
  159.6 15.7 %collective-permute-start.15 = (bf16[128,1024]{1,0:T(8,128)(2,1)S(1)}, bf16[128,1024]{1,0:T(8,128)(2,1)S(1)}, u32[]{:S(2)}, u32[]{:S(2)}) collective-permute-start(bf16[128,1024]{1,0:T(8,128)(2,1)S(1)} %get-tuple-element.16), channel_id=1, source_target_pairs={{0,16},{2,18},{4,20},{6,22},{8,24},{10,26},{12,28},{14,30},{16,0},... | collective-permute-start | bytes 786440 | tf_op jit(solution)/shard_map/ppermute | solution.py:815
  163.5 26.5 %all-to-all-start.1 = ((bf16[8,272,128]{2,1,0:T(8,128)(2,1)}), bf16[8,272,128]{2,1,0:T(8,128)(2,1)S(1)}, u32[]{:S(2)}, u32[]{:S(2)}) async-start(bf16[8,272,128]{2,1,0:T(8,128)(2,1)} %bitcast.48), calls=%async_computation.1 | async-start | bytes 1114112 | tf_op jit(solution)/shard_map/all_to_all | solution.py:882
  167.1 19.4 %collective-permute-start.16 = (bf16[128,1024]{1,0:T(8,128)(2,1)S(1)}, bf16[128,1024]{1,0:T(8,128)(2,1)S(1)}, u32[]{:S(2)}, u32[]{:S(2)}) collective-permute-start(bf16[128,1024]{1,0:T(8,128)(2,1)S(1)} %get-tuple-element.16), channel_id=1, source_target_pairs={{0,24},{2,26},{4,28},{6,30},{8,16},{10,18},{12,20},{14,22},{16,8},... | collective-permute-start | bytes 786440 | tf_op jit(solution)/shard_map/ppermute | solution.py:815
  186.5 48.5 %copy-start.3 = (bf16[512,1024]{1,0:T(8,128)(2,1)}, bf16[512,1024]{1,0:T(8,128)(2,1)S(1)}, u32[]{:S(2)}) copy-start(bf16[512,1024]{1,0:T(8,128)(2,1)S(1)} %constant_dynamic-update-slice_fusion.2.refs_0_) | copy-start | bytes 3145732
  186.5 26.1 %collective-permute-start.17 = (bf16[512,1024]{1,0:T(8,128)(2,1)S(1)}, bf16[512,1024]{1,0:T(8,128)(2,1)S(1)}, u32[]{:S(2)}, u32[]{:S(2)}) collective-permute-start(bf16[512,1024]{1,0:T(8,128)(2,1)S(1)} %constant_dynamic-update-slice_fusion.2.refs_0_), channel_id=1, source_target_pairs={{0,2},{2,0},{4,6},{6,4},{8,10},{10,8},{12,14},{14,12},{16,18},{18,... | collective-permute-start | bytes 3145736 | tf_op jit(solution)/shard_map/ppermute | solution.py:859
  187.7 47.3 %collective-permute-start.18 = (bf16[512,1024]{1,0:T(8,128)(2,1)S(1)}, bf16[512,1024]{1,0:T(8,128)(2,1)}, u32[]{:S(2)}, u32[]{:S(2)}) collective-permute-start(bf16[512,1024]{1,0:T(8,128)(2,1)S(1)} %constant_dynamic-update-slice_fusion.2.refs_0_), channel_id=1, source_target_pairs={{0,4},{2,6},{4,0},{6,2},{8,12},{10,14},{12,8},{14,10},{16,20},{18,... | collective-permute-start | bytes 3145736 | tf_op jit(solution)/shard_map/ppermute | solution.py:859
  188.3 46.7 %collective-permute-start.19 = (bf16[512,1024]{1,0:T(8,128)(2,1)S(1)}, bf16[512,1024]{1,0:T(8,128)(2,1)}, u32[]{:S(2)}, u32[]{:S(2)}) collective-permute-start(bf16[512,1024]{1,0:T(8,128)(2,1)S(1)} %constant_dynamic-update-slice_fusion.2.refs_0_), channel_id=1, source_target_pairs={{0,6},{2,4},{4,2},{6,0},{8,14},{10,12},{12,10},{14,8},{16,22},{18,... | collective-permute-start | bytes 3145736 | tf_op jit(solution)/shard_map/ppermute | solution.py:859
  190.0 45.0 %copy-start.2 = (bf16[8,272,128]{2,1,0:T(8,128)(2,1)}, bf16[8,272,128]{2,1,0:T(8,128)(2,1)S(1)}, u32[]{:S(2)}) copy-start(bf16[8,272,128]{2,1,0:T(8,128)(2,1)S(1)} %all-to-all-done.1.own) | copy-start | bytes 1671172
  190.0 45.0 %collective-permute-start.13 = (bf16[2176,128]{1,0:T(8,128)(2,1)S(1)}, bf16[2176,128]{1,0:T(8,128)(2,1)S(1)}, u32[]{:S(2)}, u32[]{:S(2)}) collective-permute-start(bf16[2176,128]{1,0:T(8,128)(2,1)S(1)} %bitcast.46), channel_id=1, source_target_pairs={{0,1},{1,0},{2,3},{3,2},{4,5},{5,4},{6,7},{7,6},{8,9},{9,8},{10,11... | collective-permute-start | bytes 1671176 | tf_op jit(solution)/shard_map/ppermute | solution.py:767
  212.6 22.5 %copy-start.4 = (bf16[512,1024]{1,0:T(8,128)(2,1)}, bf16[512,1024]{1,0:T(8,128)(2,1)S(1)}, u32[]{:S(2)}) copy-start(bf16[512,1024]{1,0:T(8,128)(2,1)S(1)} %collective-permute-done.17.refs_1_) | copy-start | bytes 3145732
  235.0 0.9 copy-start.6

commit v3 on v2

--- a/solution.py
+++ b/solution.py
@@ -1,6 +1,8 @@
 import jax
 import jax.numpy as jnp
 from jax import lax
+import math
+
 from jax.experimental import pallas as pl
 from jax.experimental.pallas import tpu as pltpu
 from jax.sharding import PartitionSpec as P
@@ -317,7 +319,7 @@
     rows = args[2].shape[0]
     local_heads = args[6].shape[2]
     group = local_heads * tp
-    if tp != 2 or sp != 2 * group or group % 4 or (group // 2) & (group // 2 - 1):
+    if tp != 2 or sp != 2 * group or group != 8:
         return None
     plane = group // 2
     ok = (
@@ -387,53 +389,38 @@
                     send[h, span, :] = part
 
 
-def chunk_vecs(rows):
-    n = rows.shape[1]
-    r = lax.broadcasted_iota(jnp.int32, (n, n), 0)
-    c = lax.broadcasted_iota(jnp.int32, (n, n), 1)
-    lower = jnp.where(r >= c, 1.0, 0.0).astype(jnp.float32)
-    eye = jnp.where(r == c, 1.0, 0.0).astype(jnp.float32)
-    cum_col = mm(lower, rows, 1, 1, HIGHEST)
-    raw_col = mm(eye, rows, 1, 1, HIGHEST)
-    cum_row = mm(rows, lower, 1, 1, HIGHEST)
-    f_col, f_row = cum_col[:, 1:2], cum_row[1:2]
-    e_col = cum_col[:, 3:4] - raw_col[:, 3:4]
-    e_row = cum_row[3:4] - rows[3:4]
-    fwd = (f_col, rows[0:1] - f_row, raw_col[:, 0:1] - f_col, cum_row[1:2, n - 1 : n])
-    bwd = (-e_col, rows[2:3] + e_row, raw_col[:, 2:3] + e_col, cum_row[3:4, n - 1 : n])
-    return fwd, bwd
-
-
-def advance_state(state, key, value, end_col, end_row, total):
-    cell, norm, peak = state
-    new_peak = jnp.maximum(total + peak, jnp.max(end_row, axis=1, keepdims=True))
-    weighted = key * jnp.exp(end_col - new_peak)
-    fade = jnp.exp(total + peak - new_peak)
-    cell = fade * cell + mm(weighted.astype(jnp.bfloat16), value, 0, 0)
-    norm = fade * norm + jnp.sum(weighted, axis=0, keepdims=True)
-    return cell, norm, new_peak
-
-
-def forward_state(state, key, value, vecs):
-    return advance_state(state, key, value, vecs[2] + vecs[3], vecs[1] + vecs[3], vecs[3])
-
-
-def backward_state(state, key, value, vecs):
-    return advance_state(state, key, value, vecs[2], vecs[1], vecs[3])
-
-
-def empty_state():
-    return (
-        jnp.zeros((M_DIM, M_DIM), jnp.float32),
-        jnp.zeros((1, M_DIM), jnp.float32),
-        jnp.full((1, 1), EMPTY, jnp.float32),
-    )
+def running_max(x, backward):
+    n = x.shape[1]
+    lane = lax.broadcasted_iota(jnp.int32, x.shape, 1)
+    step = 1
+    while step < n:
+        if backward:
+            moved = jnp.where(lane < n - step, pltpu.roll(x, n - step, 1), EMPTY)
+        else:
+            moved = jnp.where(lane >= step, pltpu.roll(x, step, 1), EMPTY)
+        x = jnp.maximum(x, moved)
+        step *= 2
+    return x
+
+
+def with_ones(value):
+    lane = lax.broadcasted_iota(jnp.int32, value.shape, 1)
+    ones = jnp.where(lane == 0, 1.0, 0.0).astype(value.dtype)
+    return jnp.concatenate([value, ones], axis=1)
+
+
+def merge(earlier, later, later_total):
+    peak = jnp.maximum(later_total + earlier[1], later[1])
+    old = jnp.exp(later_total + earlier[1] - peak)
+    new = jnp.exp(later[1] - peak)
+    return old * earlier[0] + new * later[0], peak
 
 
 def project_kernel(meta, bias, *refs):
-    plane = (len(refs) - 11) // 2
+    plane = (len(refs) - 14) // 2
     same, other = refs[:plane], refs[plane : 2 * plane]
-    own, partner, gate_t, decay, proj, gates, summary, weight, xs, raw, sems = refs[2 * plane :]
+    own, partner, gate_t, decay = refs[2 * plane : 2 * plane + 4]
+    proj, vrows, vcols, local, summary, weight, xs, raw, gates, sems = refs[2 * plane + 4 :]
     t, k, sel, jl, near = meta[0], meta[1], meta[2], meta[3], meta[5]
     copies = [
         pltpu.make_async_copy(own, raw.at[0], sems.at[plane]),
@@ -473,36 +460,58 @@
         gates[k ^ r] = jnp.transpose(mm(xs[r], gate_t[...], 1, 1))[:8]
     heads = bias.shape[1] // 4
     b = [bias[sel, g * heads + jl] for g in range(4)]
-    lead = jnp.concatenate([jnp.full((1, tok), b[g], jnp.float32) for g in range(4)], axis=0)
-    forget = lax.broadcasted_iota(jnp.int32, (4, tok), 0) % 2 == 1
-    fwd, bwd = empty_state(), empty_state()
-    total_f = jnp.zeros((1, 1), jnp.float32)
-    total_b = jnp.zeros((1, 1), jnp.float32)
-    chunks = []
-    for c in range(plane):
-        g = gates[c][:4] + lead
-        d = decay[c]
-        extra = jnp.concatenate([d[0:1], d[0:1], d[1:2], d[1:2]], axis=0)
-        logs = jnp.minimum(g, 0.0) - jnp.log1p(jnp.exp(-jnp.abs(g))) + extra
-        g = jnp.where(forget, logs, g)
-        gates[c] = jnp.concatenate([g, jnp.zeros((4, tok), jnp.float32)], axis=0)
-        vecs = chunk_vecs(gates[c])
-        span = slice(c * tok, (c + 1) * tok)
+    g = [
+        jnp.concatenate([gates[c, i : i + 1] for c in range(plane)], axis=0) + b[i]
+        for i in range(4)
+    ]
+
+    def forget(i, direction):
+        x = g[i]
+        return jnp.minimum(x, 0.0) - jnp.log1p(jnp.exp(-jnp.abs(x))) + decay[direction]
+
+    lf_f, lf_b = forget(1, 0), forget(3, 1)
+    r = lax.broadcasted_iota(jnp.int32, (tok, tok), 0)
+    c = lax.broadcasted_iota(jnp.int32, (tok, tok), 1)
+    lower = jnp.where(r >= c, 1.0, 0.0).astype(jnp.float32)
+    cum = mm(jnp.concatenate([lf_f, lf_b], axis=0), lower, 1, 1, HIGHEST)
+    lead_f, lead_b = cum[:plane], lf_b - cum[plane:]
+    src_f, src_b = g[0] - lead_f, g[2] - lead_b
+    top_f, top_b = running_max(src_f, False), running_max(src_b, True)
+    total_f, total_b = lead_f[:, tok - 1 :], cum[plane:, tok - 1 :]
+    best_f, best_b = top_f[:, tok - 1 :], top_b[:, :1]
+    end_f, end_b = jnp.exp(src_f - best_f), jnp.exp(src_b - best_b)
+    peak_f, peak_b = best_f + total_f, best_b
+
+    def wide(x):
+        return jnp.broadcast_to(x, (plane, tok))
+
+    vrows[...] = jnp.concatenate(
+        [src_f, src_b, wide(total_f), wide(total_b), wide(peak_f), wide(peak_b)], axis=0
+    )
+    stack = [top_f, top_b, lead_f, lead_b, end_f, end_b]
+    stack.append(jnp.zeros((LANES - 6 * plane, tok), jnp.float32))
+    cols_all = jnp.transpose(jnp.concatenate(stack, axis=0))
+    vcols[...] = cols_all
+    for ch in range(plane):
+        span = slice(ch * tok, (ch + 1) * tok)
         key = proj[span, LANES : 2 * LANES].astype(jnp.float32)
-        value = proj[span, 2 * LANES : 3 * LANES]
-        chunks.append((key, value, vecs))
-    for key, value, vecs in chunks:
-        fwd = forward_state(fwd, key, value, vecs[0])
-        total_f = total_f + vecs[0][3]
-    for key, value, vecs in chunks[::-1]:
-        bwd = backward_state(bwd, key, value, vecs[1])
-        total_b = total_b + vecs[1][3]
-    for i, ((cell, norm, peak), total) in enumerate(((fwd, total_f), (bwd, total_b))):
-        summary[i, :M_DIM, :] = cell
+        value = with_ones(proj[span, 2 * LANES : 3 * LANES])
+        for i in range(2):
+            at = (4 + i) * plane + ch
+            weighted = (key * cols_all[:, at : at + 1]).astype(jnp.bfloat16)
+            local[i, ch] = mm(weighted, value, 0, 0)
+    for i in range(2):
+        state = (jnp.zeros((M_DIM, 2 * LANES), jnp.float32), jnp.full((1, 1), EMPTY, jnp.float32))
+        total = jnp.zeros((1, 1), jnp.float32)
+        for ch in range(plane) if i == 0 else range(plane - 1, -1, -1):
+            chunk_total, chunk_peak = chunk_scalars(vrows, i, ch, plane)
+            state = merge(state, (local[i, ch], chunk_peak), chunk_total)
+            total = total + chunk_total
+        summary[i, :M_DIM, :] = state[0][:, :LANES]
         summary[i, M_DIM : M_DIM + 8, :] = jnp.concatenate(
             [
-                norm,
-                jnp.broadcast_to(peak, (1, LANES)),
+                jnp.transpose(state[0][:, LANES:])[:1],
+                jnp.broadcast_to(state[1], (1, LANES)),
                 jnp.broadcast_to(total, (1, LANES)),
                 jnp.zeros((5, LANES), jnp.float32),
             ],
@@ -513,66 +522,98 @@
     summary[1, M_DIM + 8 :, :] = proj[last - WINDOW :, 5 * LANES :].astype(jnp.float32)
 
 
-def read_state(ref, i):
-    return (
-        ref[i, :M_DIM, :],
-        ref[i, M_DIM : M_DIM + 1, :],
-        ref[i, M_DIM + 1 : M_DIM + 2, 0:1],
-        ref[i, M_DIM + 2 : M_DIM + 3, 0:1],
-    )
-
-
-def merge_states(earlier, later, later_total):
-    peak = jnp.maximum(later_total + earlier[2], later[2])
-    old = jnp.exp(later_total + earlier[2] - peak)
-    new = jnp.exp(later[2] - peak)
-    return old * earlier[0] + new * later[0], old * earlier[1] + new * later[1], peak
+def chunk_scalars(vrows, i, ch, plane):
+    total, peak = (2 + i) * plane + ch, (4 + i) * plane + ch
+    return vrows[total : total + 1, :1], vrows[peak : peak + 1, :1]
+
+
+def packed_state(ref, i):
+    rows = ref[i, : M_DIM + 8, :]
+    return (rows, rows[M_DIM + 1 : M_DIM + 2, :1]), rows[M_DIM + 2 : M_DIM + 3, :1]
+
+
+def open_state(packed):
+    rows, peak = packed
+    first = lax.broadcasted_iota(jnp.int32, (LANES, LANES), 0) == 0
+    norm = jnp.transpose(jnp.where(first, rows[M_DIM : M_DIM + 1], 0.0))
+    return jnp.concatenate([rows[:M_DIM], norm], axis=1), peak
 
 
 def combine_kernel(meta, own, partner, out):
     t, hi = meta[0], meta[4]
     forward = hi == 0
     i = jnp.where(forward, 0, 1)
-    mine, other = read_state(own, i), read_state(partner, i)
+    (mine, mine_peak), mine_total = packed_state(own, i)
+    (other, other_peak), other_total = packed_state(partner, i)
     mine_later = (t == 1) == forward
-    a = tuple(jnp.where(mine_later, y, x) for x, y in zip(mine, other))
-    b = tuple(jnp.where(mine_later, x, y) for x, y in zip(mine, other))
-    cell, norm, peak = merge_states(a[:3], b[:3], b[3])
-    out[:M_DIM, :] = cell
-    out[M_DIM : M_DIM + 8, :] = jnp.concatenate(
-        [norm, jnp.broadcast_to(peak, (1, LANES)), jnp.zeros((6, LANES), jnp.float32)], axis=0
-    )
+
+    def pick(x, y):
+        return jnp.where(mine_later, x, y)
+
+    rows, peak = merge(
+        (pick(other, mine), pick(other_peak, mine_peak)),
+        (pick(mine, other), pick(mine_peak, other_peak)),
+        pick(mine_total, other_total),
+    )
+    out[: M_DIM + 8, :] = rows
+    out[M_DIM + 1 : M_DIM + 2, :] = jnp.broadcast_to(peak, (1, LANES))
     out[M_DIM + 8 :, :] = partner[jnp.where(forward, 1, 0), M_DIM + 8 :, :]
 
 
-def mixer_kernel(meta, sink, proj, gates, partner, across, gain, keep, send, kv, logs):
+def attend(q, kv, sinks, drop_first, drop_last):
+    n = q.shape[0]
+    q = q * jnp.bfloat16(W_DIM ** (-0.5))
+    q = jnp.concatenate([q[:, :W_DIM], q[:, W_DIM:]], axis=0)
+    r = lax.broadcasted_iota(jnp.int32, (2 * n, n), 0)
+    c = lax.broadcasted_iota(jnp.int32, (2 * n, n), 1)
+    row = jnp.where(r >= n, r - n, r)
+    sink = jnp.where(
+        lax.broadcasted_iota(jnp.int32, (2 * n, 1), 0) < n, sinks[0], sinks[1]
+    )
+    s = [mm(q, kv[i * n : (i + 1) * n, :W_DIM], 1, 1) for i in range(3)]
+    before, after = c >= row, c <= row
+    if drop_first is not None:
+        before = before & jnp.logical_not(drop_first)
+        after = after & jnp.logical_not(drop_last)
+    s[0] = jnp.where(before, s[0], EMPTY)
+    s[2] = jnp.where(after, s[2], EMPTY)
+    peak = jnp.max(jnp.maximum(jnp.maximum(s[0], s[1]), s[2]), axis=1, keepdims=True)
+    peak = jnp.maximum(peak, sink)
+    e = [jnp.exp(x - peak) for x in s]
+    total = jnp.exp(sink - peak) + jnp.sum(e[0] + e[1] + e[2], axis=1, keepdims=True)
+    weights = jnp.concatenate([x.astype(jnp.bfloat16) for x in e], axis=1)
+    mixed = mm(weights, kv[:, W_DIM:]) / total
+    mixed = jnp.concatenate([mixed[:n], mixed[n:]], axis=1).astype(jnp.bfloat16)
+    log_col = peak + jnp.log(total)
+    diag = (c == row)
+    logs = [
+        jnp.sum(jnp.where(diag[:n], log_col[h * n : (h + 1) * n], 0.0), axis=0, keepdims=True)
+        for h in range(2)
+    ]
+    return mixed, jnp.concatenate(logs + [jnp.zeros((6, n), jnp.float32)], axis=0)
+
+
+def attend_kernel(meta, sink, proj, partner, mixed, logs, kv):
+    t, sel, jl = meta[0], meta[2], meta[3]
+    length = proj.shape[0]
+    edge = partner[jnp.where(t == 0, 0, 1), M_DIM + 8 :, :].astype(jnp.bfloat16)
+    kv[:WINDOW, :] = edge
+    kv[WINDOW : WINDOW + length, :] = proj[:, 5 * LANES :]
+    kv[WINDOW + length :, :] = edge
+    sinks = (sink[sel, 2 * jl], sink[sel, 2 * jl + 1])
+    for i in range(length // WINDOW - 1):
+        b = i + 1 - t
+        at = pl.multiple_of(b * WINDOW, WINDOW)
+        q = proj[pl.ds(at, WINDOW), 4 * LANES : 5 * LANES]
+        mixed[b], logs[b] = attend(q, kv[pl.ds(at, 3 * WINDOW), :], sinks, None, None)
+
+
+def mixer_kernel(
+    meta, sink, proj, vrows, vcols, local, partner, across, gain, att, att_logs, keep, send, am, al
+):
     t, sel, jl, hi = meta[0], meta[2], meta[3], meta[4]
-    chunks = gates.shape[0]
-    tok = gates.shape[2]
-    far = (
-        across[:M_DIM, :],
-        across[M_DIM : M_DIM + 1, :],
-        across[M_DIM + 1 : M_DIM + 2, 0:1],
-    )
-
-    def incoming(i, use_far, use_near):
-        near = read_state(partner, i)
-        far_peak = jnp.where(use_far, far[2], EMPTY)
-        near_peak = jnp.where(use_near, near[2], EMPTY)
-        near_total = jnp.where(use_near, near[3], 0.0)
-        return merge_states((far[0], far[1], far_peak), (near[0], near[1], near_peak), near_total)
-
-    scale = M_DIM ** (-0.5)
-    fwd = incoming(0, hi == 1, t == 1)
-    bwd = incoming(1, hi == 0, t == 0)
-    vecs = [chunk_vecs(gates[c]) for c in range(chunks)]
-
-    def kv_of(c):
-        span = slice(c * tok, (c + 1) * tok)
-        return (
-            proj[span, LANES : 2 * LANES].astype(jnp.float32),
-            proj[span, 2 * LANES : 3 * LANES],
-        )
+    tok = vrows.shape[1]
+    chunks = vrows.shape[0] // 6
 
     def store(is_cell, c, span, value):
         @pl.when((t == 0) == is_cell)
@@ -583,112 +624,101 @@
         def _():
             send[c, span, :] = value
 
-
-    back_states = [None] * chunks
+    length = proj.shape[0]
+    blocks = length // WINDOW
+    am[...] = att[...]
+    al[...] = att_logs[...]
+    outer = across[M_DIM + 8 :, :].astype(jnp.bfloat16)
+    inside = proj[pl.ds(pl.multiple_of(t * (length - 2 * WINDOW), WINDOW), 2 * WINDOW), 5 * LANES :]
+    kv = jnp.where(
+        t == 0,
+        jnp.concatenate([outer, inside], axis=0),
+        jnp.concatenate([inside, outer], axis=0),
+    )
+    sinks = (sink[sel, 2 * jl], sink[sel, 2 * jl + 1])
+    at = pl.multiple_of(t * (length - WINDOW), WINDOW)
+    q = proj[pl.ds(at, WINDOW), 4 * LANES : 5 * LANES]
+    edge = t * (blocks - 1)
+    am[edge], al[edge] = attend(q, kv, sinks, (t == 0) & (hi == 0), (t == 1) & (hi == 1))
+
+    far = across[: M_DIM + 8, :]
+    far_peak = across[M_DIM + 1 : M_DIM + 2, :1]
+
+    def incoming(i, use_far, use_near):
+        (near, near_peak), near_total = packed_state(partner, i)
+        return open_state(
+            merge(
+                (far, jnp.where(use_far, far_peak, EMPTY)),
+                (near, jnp.where(use_near, near_peak, EMPTY)),
+                jnp.where(use_near, near_total, 0.0),
+            )
+        )
+
+    fwd = incoming(0, hi == 1, t == 1)
+    bwd = incoming(1, hi == 0, t == 0)
+    entering = [[None, None] for _ in range(chunks)]
+    for c in range(chunks):
+        entering[c][0] = fwd
+        total, peak = chunk_scalars(vrows, 0, c, chunks)
+        if c + 1 < chunks:
+            fwd = merge(fwd, (local[0, c], peak), total)
     for c in range(chunks - 1, -1, -1):
-        back_states[c] = bwd
+        total, peak = chunk_scalars(vrows, 1, c, chunks)
+        entering[c][1] = (bwd[0], bwd[1] + total)
         if c:
-            bwd = backward_state(bwd, *kv_of(c), vecs[c][1])
+            bwd = merge(bwd, (local[1, c], peak), total)
     r = lax.broadcasted_iota(jnp.int32, (tok, tok), 0)
     col = lax.broadcasted_iota(jnp.int32, (tok, tok), 1)
     gain_row = gain[sel, pl.ds(jl, 1), :]
+    floor_lift = 0.5 * math.log(M_DIM)
     for c in range(chunks):
         span = slice(c * tok, (c + 1) * tok)
         q = proj[span, :LANES]
-        qf = q.astype(jnp.float32)
-        scores = mm(q, proj[span, LANES : 2 * LANES], 1, 1) * scale
-        total_w = None
-        inter = None
-        for state, vec, mask in ((fwd, vecs[c][0], r >= col), (back_states[c], vecs[c][1], r <= col)):
-            cell, norm, peak = state
-            lead_col, src_row = vec[0], vec[1]
-            if mask is not None and vec is vecs[c][1]:
-                reach = peak + vec[3]
-            else:
-                reach = peak
-            masked = jnp.where(mask, src_row, EMPTY)
-            top = jnp.maximum(jnp.max(masked, axis=1, keepdims=True), reach)
-            w = jnp.exp(masked - top)
-            w_in = jnp.exp(reach - top)
-            denom = jnp.sum(scores * w, axis=1, keepdims=True) + w_in * scale * jnp.sum(
-                qf * norm, axis=1, keepdims=True
+        value = with_ones(proj[span, 2 * LANES : 3 * LANES])
+        scores = mm(q, proj[span, LANES : 2 * LANES], 1, 1)
+        cell_out = None
+        for i, mask in enumerate((r >= col, r <= col)):
+            cell, reach = entering[c][i]
+            at = i * chunks + c
+            src = vrows[at : at + 1, :]
+            top = jnp.maximum(vcols[:, at : at + 1], reach)
+            lead = vcols[:, at + 2 * chunks : at + 2 * chunks + 1]
+            w = jnp.where(mask, jnp.exp(src - top), 0.0)
+            both = mm((scores * w).astype(jnp.bfloat16), value) + jnp.exp(reach - top) * mm(
+                q, cell.astype(jnp.bfloat16)
             )
-            inv = 1.0 / jnp.maximum(jnp.abs(denom), jnp.exp(-(lead_col + top)))
-            part = w * inv
-            high = cell.astype(jnp.bfloat16)
-            low = (cell - high.astype(jnp.float32)).astype(jnp.bfloat16)
-            add = (mm(q, high) + mm(q, low)) * (scale * w_in * inv)
-            total_w = part if total_w is None else total_w + part
-            inter = add if inter is None else inter + add
-        key, value = kv_of(c)
-        cell_out = mm((scores * total_w).astype(jnp.bfloat16), value) + inter
-        fwd = forward_state(fwd, key, value, vecs[c][0])
+            denom = jnp.abs(both[:, LANES : LANES + 1])
+            inv = 1.0 / jnp.maximum(denom, jnp.exp(floor_lift - (lead + top)))
+            part = both[:, :LANES] * inv
+            cell_out = part if cell_out is None else cell_out + part
         gate = proj[span, 3 * LANES : 4 * LANES].astype(jnp.float32)
         u = cell_out / (1.0 + jnp.exp(-gate))
         u = u * lax.rsqrt(jnp.mean(u * u, axis=1, keepdims=True) + EPS) * gain_row
-        store(True, c, slice(0, tok), u.astype(jnp.bfloat16))
-        store(True, c, slice(tok, tok + 16), jnp.zeros((16, LANES), jnp.bfloat16))
-
-    length = proj.shape[0]
-    inner_edge = partner[jnp.where(t == 0, 0, 1), M_DIM + 8 :, :].astype(jnp.bfloat16)
-    outer_edge = across[M_DIM + 8 :, :].astype(jnp.bfloat16)
-    kv[:WINDOW, :] = jnp.where(t == 0, outer_edge, inner_edge)
-    kv[WINDOW : WINDOW + length, :] = proj[:, 5 * LANES :]
-    kv[WINDOW + length :, :] = jnp.where(t == 0, inner_edge, outer_edge)
-    at_start = (hi == 0) & (t == 0)
-    at_end = (hi == 1) & (t == 1)
-    qi = lax.broadcasted_iota(jnp.int32, (WINDOW, 3 * WINDOW), 0)
-    ki = lax.broadcasted_iota(jnp.int32, (WINDOW, 3 * WINDOW), 1) - WINDOW
-    band = jnp.abs(ki - qi) <= WINDOW
-    diag = lax.broadcasted_iota(jnp.int32, (WINDOW, WINDOW), 0) == lax.broadcasted_iota(
-        jnp.int32, (WINDOW, WINDOW), 1
-    )
-    blocks = length // WINDOW
+        tail = jnp.zeros((16, LANES), jnp.bfloat16)
+        store(True, c, slice(0, tok + 16), jnp.concatenate([u.astype(jnp.bfloat16), tail], axis=0))
+
     per = tok // WINDOW
-    for b in range(blocks):
-        usable = band
-        if b == 0:
-            usable = usable & ((ki >= 0) | jnp.logical_not(at_start))
-        if b == blocks - 1:
-            usable = usable & ((ki < WINDOW) | jnp.logical_not(at_end))
-        keys = kv[b * WINDOW : (b + 3) * WINDOW, :W_DIM]
-        values = kv[b * WINDOW : (b + 3) * WINDOW, W_DIM:]
-        mixed = []
-        for h in range(2):
-            lanes = slice(4 * LANES + h * W_DIM, 4 * LANES + (h + 1) * W_DIM)
-            q = proj[b * WINDOW : (b + 1) * WINDOW, lanes]
-            s = mm(q, keys, 1, 1) * W_DIM ** (-0.5)
-            s = jnp.where(usable, s, EMPTY)
-            sink_h = sink[sel, 2 * jl + h]
-            peak = jnp.maximum(jnp.max(s, axis=1, keepdims=True), sink_h)
-            e = jnp.exp(s - peak)
-            total = jnp.exp(sink_h - peak) + jnp.sum(e, axis=1, keepdims=True)
-            mixed.append(mm(e.astype(jnp.bfloat16), values) / total)
-            log_col = peak + jnp.log(total)
-            log_row = jnp.sum(jnp.where(diag, log_col, 0.0), axis=0, keepdims=True)
-            at = h * per + b % per
-            logs[b // per, at : at + 1, :] = log_row
-        span = slice((b % per) * WINDOW, (b % per + 1) * WINDOW)
-        store(False, b // per, span, jnp.concatenate(mixed, axis=1).astype(jnp.bfloat16))
     for c in range(chunks):
-        x = logs[c]
+        x = jnp.concatenate(
+            [al[c * per + p][h : h + 1] for h in range(2) for p in range(per)], axis=0
+        )
         high = x.astype(jnp.bfloat16).astype(jnp.float32)
         mid = (x - high).astype(jnp.bfloat16).astype(jnp.float32)
         low = x - high - mid
-        n = x.shape[0]
-        pad = jnp.zeros((16 - 3 * n, LANES), jnp.float32)
+        pad = jnp.zeros((16 - 3 * 2 * per, LANES), jnp.float32)
         tail = jnp.concatenate([high, mid, low, pad], axis=0).astype(jnp.bfloat16)
-        store(False, c, slice(tok, tok + 16), tail)
+        rows = [am[c * per + p] for p in range(per)] + [tail]
+        store(False, c, slice(0, tok + 16), jnp.concatenate(rows, axis=0))
 
 
 def output_kernel(meta, own, partner, *refs):
     mixed, log_total, left, weight, sems = refs[-5:]
     blocks = refs[:-5]
     t, p, z = meta[0], meta[1], meta[6]
-    plane = len(blocks)
+    plane = len(blocks) // 2
     heads, tok = own.shape[0], mixed.shape[0]
     planes = sems.shape[0] // plane
-    rows = blocks[0].shape[0] // planes
+    rows = 2 * blocks[0].shape[0] // planes
     half = rows // 2
     total = weight.shape[0] // 2
     copies = []
@@ -699,7 +729,9 @@
                 to = pl.multiple_of(i * total + source * half, half)
                 copies.append(
                     pltpu.make_async_copy(
-                        blocks[r].at[pl.ds(zr * rows + i * half, half)],
+                        blocks[2 * r + 2 * zr // planes].at[
+                            pl.ds(zr % (planes // 2) * rows + i * half, half)
+                        ],
                         weight.at[pl.ds(to, half)],
                         sems.at[r * planes + zr, i],
                     )
@@ -823,7 +855,6 @@
     first = (2 * hi + t) * plane
     decay = lax.dynamic_slice_in_dim(small_both[:, :, n_gate:], first, plane, 1)
     decay = jnp.sum(decay.reshape(2, plane, 3, tok).astype(f32), axis=2)
-    decay = jnp.transpose(decay, (1, 0, 2))
     params = jnp.concatenate(
         [m_gain, gate_bias.reshape(-1), sink_logit, jnp.zeros((LANES - 6 * lh,), f32)]
     ).reshape(-1, LANES)
@@ -835,17 +866,20 @@
     quarter = plane * tok
     cols = 6 * LANES
     sum_rows = M_DIM + 8 + WINDOW
-    proj, gates, summary = vmem_call(
+    proj, vrows, vcols, local, summary = vmem_call(
         project_kernel,
         (
             jax.ShapeDtypeStruct((quarter, cols), bf16),
-            jax.ShapeDtypeStruct((plane, 8, tok), f32),
+            jax.ShapeDtypeStruct((6 * plane, tok), f32),
+            jax.ShapeDtypeStruct((tok, LANES), f32),
+            jax.ShapeDtypeStruct((2, plane, M_DIM, 2 * LANES), f32),
             jax.ShapeDtypeStruct((2, sum_rows, LANES), f32),
         ),
         scratch=[
             pltpu.VMEM((width, cols), bf16),
             pltpu.VMEM((plane, tok, width), bf16),
             pltpu.VMEM((2, sp, n_rows, LANES), bf16),
+            pltpu.VMEM((plane, 8, tok), f32),
             pltpu.SemaphoreType.DMA((plane + 2,)),
         ],
         smem=2,
@@ -854,28 +888,44 @@
         flops=2 * quarter * width * cols,
     )(meta, bias, *same_xs, *other_xs, own_w, partner_w, gate_t, decay)
     column = jnp.concatenate(column, axis=0)
-    out_blocks = [column]
-    for r in range(1, plane):
-        out_blocks.append(lax.ppermute(column, "sp", [(a, a ^ r) for a in range(sp)]))
+    cut = column.shape[0] // 2
+    upper, lower = column[:cut], column[cut:]
+
+    def hop(x, r):
+        return lax.ppermute(x, "sp", [(a, a ^ r) for a in range(sp)])
+
+    upper_1, lower_2 = hop(upper, 1), hop(lower, 2)
+    upper_2, lower_1 = hop(upper, 2), hop(lower, 1)
+    upper_3, lower_3 = hop(upper_1, 2), hop(lower_2, 1)
+    out_blocks = [upper, lower, upper_1, lower_1, upper_2, lower_2, upper_3, lower_3]
     partner_sum = flip(summary)
     sent = vmem_call(
         combine_kernel, jax.ShapeDtypeStruct((sum_rows, LANES), f32), smem=1, n_in=2
     )(meta, summary, partner_sum)
     across = lax.ppermute(sent, "sp", [(a, (a + group) % sp) for a in range(sp)])
+    blocks = quarter // WINDOW
+    att, att_logs = vmem_call(
+        attend_kernel,
+        (
+            jax.ShapeDtypeStruct((blocks, WINDOW, LANES), bf16),
+            jax.ShapeDtypeStruct((blocks, 8, WINDOW), f32),
+        ),
+        scratch=[pltpu.VMEM((quarter + 2 * WINDOW, LANES), bf16)],
+        smem=2,
+        n_in=2,
+        flops=quarter * width * cols,
+    )(meta, sink, proj, partner_sum)
     spread, send = vmem_call(
         mixer_kernel,
         (
             jax.ShapeDtypeStruct((2, plane, tok + 16, LANES), bf16),
             jax.ShapeDtypeStruct((plane, tok + 16, LANES), bf16),
         ),
-        scratch=[
-            pltpu.VMEM((quarter + 2 * WINDOW, LANES), bf16),
-            pltpu.VMEM((plane, 2 * tok // WINDOW, LANES), f32),
-        ],
+        scratch=[pltpu.VMEM((blocks, WINDOW, LANES), bf16), pltpu.VMEM((blocks, 8, WINDOW), f32)],
         smem=2,
-        n_in=5,
-        flops=2 * quarter * width * cols,
-    )(meta, sink, proj, gates, partner_sum, across, gain)
+        n_in=9,
+        flops=quarter * width * cols,
+    )(meta, sink, proj, vrows, vcols, local, partner_sum, across, gain, att, att_logs)
     got = flip(send)
     spread = lax.dynamic_update_slice_in_dim(spread, got[None], 1 - t, 0)
     groups = [list(range(g * group, (g + 1) * group)) for g in range(sp // group)]
@@ -903,7 +953,7 @@
         ],
         smem=1,
         n_in=2,
-        n_any=plane,
+        n_any=2 * plane,
         flops=2 * tok * inner * out_m_weight.shape[1],
     )(meta, mine.reshape(shape), theirs.reshape(shape), *out_blocks)
 

time: 243 us -> 223 us (0.918)
  waiting for transfers between devices: 130 us -> 119 us
  Pallas kernels: 41.8 us -> 33.7 us
    pallas_call x1, Pallas kernels: 18.9 us -> 7.1 us  [on_device_split(): vmem_call(mixer_kernel, (jax.ShapeDtypeStruct((2, plane, tok + 16, LANES)...]
    ppermute x3 -> x6, waiting for transfers between devices: 44.9 us -> 33.5 us  [hop(): return lax.ppermute(x, 'sp', [(a, a ^ r) for a in range(sp)])]
    ppermute x3, waiting for transfers between devices: 17.5 us -> 23 us  [on_device_split(): lax.ppermute(out_block, 'sp', [(a, a ^ r * plane) for a in range(sp)])]
    pallas_call x0 -> x1, Pallas kernels: none -> 4.73 us  [on_device_split(): vmem_call(attend_kernel, (jax.ShapeDtypeStruct((blocks, WINDOW, LANES), b...]
    ppermute x1, waiting for transfers between devices: 6.49 us -> 2.92 us  [on_device_split(): lax.ppermute(sent, 'sp', [(a, (a + group) % sp) for a in range(sp)])]
  transfers between devices with their start and end apart: 22 -> 25, of which waited for: 13 -> 14; matrix products, arithmetic and copies ran while one was open for 3% -> 3% of each run, Pallas kernels for 0% -> 2%
where the time goes in v3:
time: 223 us
  waiting for transfers between devices  119 us (53%)
  starting transfers between devices  55.1 us (25%)
  Pallas kernels  33.7 us (15%)
  local copies, waits for them, and re-layouts  7.9 us (4%)
  other arithmetic  5.69 us (3%)
    all_to_all x1, waiting for transfers between devices, on_device_split(): lax.all_to_all(spread.reshape(sp * n_rows, LANES), 'sp', 0, 0, tiled=True)  34.4 us
    ppermute x6, waiting for transfers between devices, hop(): return lax.ppermute(x, 'sp', [(a, a ^ r) for a in range(sp)])  33.5 us
    ppermute x3, waiting for transfers between devices, on_device_split(): lax.ppermute(out_block, 'sp', [(a, a ^ r * plane) for a in range(sp)])  23 us
    ppermute x3, waiting for transfers between devices, on_device_split(): lax.ppermute(normed, both_axes, [(core(a, True), core(a ^ r, True)) for a...  20.3 us
    ppermute x6, starting transfers between devices, flip(): return lax.ppermute(x, 'tp', swap)  13.3 us
    pallas_call x1, Pallas kernels, on_device_split(): vmem_call(project_kernel, (jax.ShapeDtypeStruct((quarter, cols), bf16), j...  11.6 us
    ppermute x3, starting transfers between devices, on_device_split(): lax.ppermute(normed, both_axes, [(core(a, True), core(a ^ r, True)) for a...  9.22 us
    all_to_all x1, starting transfers between devices, on_device_split(): lax.all_to_all(spread.reshape(sp * n_rows, LANES), 'sp', 0, 0, tiled=True)  8.35 us
  transfers between devices with their start and end apart: 25, of which 14 were waited for; matrix products, arithmetic and copies ran while one was open for 3% of the time, Pallas kernels for 2%

profile of v3, /device:TPU:0, one launch (start us, length us, event | category | flops | bytes accessed | tf_op | source)
XLA Modules:
  0.0 222.7 jit_solution(6638925793201193063)
XLA Ops:
  0.7 0.7 fusion.5
  1.5 0.8 reshape.60
  2.3 0.1 reshape.61
  2.3 0.6 pad_maximum_fusion.1.small
  3.0 0.7 stack.62.meta
  3.6 2.7 %shard_map.167 = (bf16[2,2,4,392,128]{4,3,2,1,0:T(8,128)(2,1)}, bf16[4,392,128]{2,1,0:T(8,128)(2,1)}) custom-call(s32[7]{0:T(128)} %stack.62.meta, bf16[128,512]{1,0:T(8,128)(2,1)} %mq.1, bf16[128,512]{1,0:T(8,128)(2,1)} %mk.1, bf16[128,512]{1,0:T(8,128)(2,1)} %mv.1, bf16[128,512]{1,0:T(8,128)(2,1)} %mo.1, bf16[128,512]{1,0:T(8,128)(2,1)} %aq.1, ...), custom_call_target="tpu_custom_call" | custom-call | tf_op jit(solution)/shard_map/pallas_call | solution.py:825
  6.3 0.5 collective-permute-start.8
  6.8 1.6 collective-permute-done.8
  8.4 1.0 broadcast_dynamic-update-slice_fusion
  9.4 8.4 %all-to-all-start = ((bf16[16,392,128]{2,1,0:T(8,128)(2,1)}), bf16[16,392,128]{2,1,0:T(8,128)(2,1)S(1)}, u32[]{:S(2)}, u32[]{:S(2)}) async-start(bf16[16,392,128]{2,1,0:T(8,128)(2,1)} %bitcast.44), calls=%async_computation | async-start | bytes 3211264 | tf_op jit(solution)/shard_map/all_to_all | solution.py:837
  17.8 0.3 fusion
  18.1 34.4 %all-to-all-done.refs_8_ = bf16[16,392,128]{2,1,0:T(8,128)(2,1)S(1)} async-done(((bf16[16,392,128]{2,1,0:T(8,128)(2,1)}), bf16[16,392,128]{2,1,0:T(8,128)(2,1)S(1)}, u32[]{:S(2)}, u32[]{:S(2)}) %all-to-all-start) | async-done | bytes 1605664 | tf_op jit(solution)/shard_map/all_to_all | solution.py:837
  52.6 1.5 fusion.2.refs_0_
  54.0 6.8 %collective-permute-start.4 = (bf16[256,2048]{1,0:T(8,128)(2,1)}, bf16[256,2048]{1,0:T(8,128)(2,1)S(1)}, u32[]{:S(2)}, u32[]{:S(2)}) collective-permute-start(bf16[256,2048]{1,0:T(8,128)(2,1)} %fusion.2.refs_0_), channel_id=1, source_target_pairs={{0,8},{2,10},{4,12},{6,14},{9,1},{11,3},{13,5},{15,7},{16,24},{18,... | collective-permute-start | bytes 3145736 | tf_op jit(solution)/shard_map/ppermute | solution.py:807
  60.9 3.0 %collective-permute-start.1 = (bf16[256,2048]{1,0:T(8,128)(2,1)}, bf16[256,2048]{1,0:T(8,128)(2,1)}, u32[]{:S(2)}, u32[]{:S(2)}) collective-permute-start(bf16[256,2048]{1,0:T(8,128)(2,1)} %fusion.2.refs_0_), channel_id=1, source_target_pairs={{0,2},{2,0},{4,6},{6,4},{9,11},{11,9},{13,15},{15,13},{16,18},{18,... | collective-permute-start | bytes 3145736 | tf_op jit(solution)/shard_map/ppermute | solution.py:813
  63.9 0.1 reshape.58
  64.0 0.1 fusion.8
  64.1 3.7 %collective-permute-start.2 = (bf16[256,2048]{1,0:T(8,128)(2,1)}, bf16[256,2048]{1,0:T(8,128)(2,1)}, u32[]{:S(2)}, u32[]{:S(2)}) collective-permute-start(bf16[256,2048]{1,0:T(8,128)(2,1)} %fusion.2.refs_0_), channel_id=1, source_target_pairs={{0,4},{2,6},{4,0},{6,2},{9,13},{11,15},{13,9},{15,11},{16,20},{18,... | collective-permute-start | bytes 3145736 | tf_op jit(solution)/shard_map/ppermute | solution.py:813
  67.7 2.6 %collective-permute-start.3 = (bf16[256,2048]{1,0:T(8,128)(2,1)}, bf16[256,2048]{1,0:T(8,128)(2,1)}, u32[]{:S(2)}, u32[]{:S(2)}) collective-permute-start(bf16[256,2048]{1,0:T(8,128)(2,1)} %fusion.2.refs_0_), channel_id=1, source_target_pairs={{0,6},{2,4},{4,2},{6,0},{9,15},{11,13},{13,11},{15,9},{16,22},{18,... | collective-permute-start | bytes 3145736 | tf_op jit(solution)/shard_map/ppermute | solution.py:813
  70.3 3.1 %collective-permute-done.4.refs_4_ = bf16[256,2048]{1,0:T(8,128)(2,1)S(1)} collective-permute-done((bf16[256,2048]{1,0:T(8,128)(2,1)}, bf16[256,2048]{1,0:T(8,128)(2,1)S(1)}, u32[]{:S(2)}, u32[]{:S(2)}) %collective-permute-start.4) | collective-permute-done | bytes 1048608 | tf_op jit(solution)/shard_map/ppermute | solution.py:807
  73.4 1.7 collective-permute-start.5
  75.1 3.1 %collective-permute-done.1.refs_1_ = bf16[256,2048]{1,0:T(8,128)(2,1)} collective-permute-done((bf16[256,2048]{1,0:T(8,128)(2,1)}, bf16[256,2048]{1,0:T(8,128)(2,1)}, u32[]{:S(2)}, u32[]{:S(2)}) %collective-permute-start.1) | collective-permute-done | bytes 1048608 | tf_op jit(solution)/shard_map/ppermute | solution.py:813
  78.2 1.7 collective-permute-start.6
  79.9 1.6 collective-permute-start.7
  81.5 0.6 pad_maximum_fusion.4
  82.1 0.8 slice_bitcast_fusion
  83.0 0.1 reshape.64
  83.1 0.1 reshape.65
  83.2 0.6 reduce_sum.19.refs_11_
  83.9 0.8 pad.4.refs_10_
  84.7 2.2 collective-permute-done.2.refs_2_
  86.9 15.0 %collective-permute-done.3.refs_3_ = bf16[256,2048]{1,0:T(8,128)(2,1)} collective-permute-done((bf16[256,2048]{1,0:T(8,128)(2,1)}, bf16[256,2048]{1,0:T(8,128)(2,1)}, u32[]{:S(2)}, u32[]{:S(2)}) %collective-permute-start.3) | collective-permute-done | bytes 1048608 | tf_op jit(solution)/shard_map/ppermute | solution.py:813
  101.9 11.6 %shard_map.168 = (bf16[1024,768]{1,0:T(8,128)(2,1)}, f32[24,256]{1,0:T(8,128)}, f32[256,128]{1,0:T(8,128)}, f32[2,4,128,256]{3,2,1,0:T(8,128)}, f32[2,264,128]{2,1,0:T(8,128)}) custom-call(s32[7]{0:T(128)} %stack.62.meta, f32[2,16]{1,0:T(2,128)} %bitcast.52, bf16[256,2048]{1,0:T(8,128)(2,1)} %fusion.2.refs_0_, ...), custom_call_target="tpu_custom_call" | custom-call | flops 3221225472 | tf_op jit(solution)/shard_map/pallas_call | solution.py:869
  113.6 12.7 %collective-permute-start.10 = (f32[2,264,128]{2,1,0:T(8,128)}, f32[2,264,128]{2,1,0:T(8,128)S(1)}, u32[]{:S(2)}, u32[]{:S(2)}) collective-permute-start(f32[2,264,128]{2,1,0:T(8,128)} %get-tuple-element.19.own), channel_id=1, source_target_pairs={{0,1},{1,0},{2,3},{3,2},{4,5},{5,4},{6,7},{7,6},{8,9},{9,8},{10,11... | collective-permute-start | bytes 811016 | tf_op jit(solution)/shard_map/ppermute | solution.py:799
  126.3 0.6 pad_maximum_fusion.5
  126.9 0.6 pad_maximum_fusion.2.gain
  127.5 0.1 collective-permute-done.10.partner
  127.7 0.7 copy-done.13
  128.4 1.8 shard_map.169
  130.2 0.9 collective-permute-start.11
  131.1 4.7 %shard_map.170 = (bf16[8,128,128]{2,1,0:T(8,128)(2,1)}, f32[8,8,128]{2,1,0:T(8,128)}) custom-call(s32[7]{0:T(128)} %stack.62.meta, f32[2,8]{1,0:T(2,128)} %bitcast.53, bf16[1024,768]{1,0:T(8,128)(2,1)} %get-tuple-element.15.proj, f32[2,264,128]{2,1,0:T(8,128)} %copy-done.13), custom_call_target="tpu_custom_call" | custom-call | flops 1610612736 | tf_op jit(solution)/shard_map/pallas_call | solution.py:907
  135.8 2.9 %collective-permute-done.11.across = f32[264,128]{1,0:T(8,128)S(1)} collective-permute-done((f32[264,128]{1,0:T(8,128)}, f32[264,128]{1,0:T(8,128)S(1)}, u32[]{:S(2)}, u32[]{:S(2)}) %collective-permute-start.11) | collective-permute-done | bytes 135200 | tf_op jit(solution)/shard_map/ppermute | solution.py:905
  138.8 0.7 copy-done.20
  139.4 7.1 %shard_map.171 = (bf16[2,4,272,128]{3,2,1,0:T(8,128)(2,1)}, bf16[4,272,128]{2,1,0:T(8,128)(2,1)}) custom-call(s32[7]{0:T(128)} %stack.62.meta, f32[2,8]{1,0:T(2,128)} %bitcast.54, bf16[1024,768]{1,0:T(8,128)(2,1)} %get-tuple-element.15.proj, f32[24,256]{1,0:T(8,128)} %get-tuple-element.16.vrows, f32[256,128]{1,0:T(8,128)} %get-tuple-element.17.vcols, ...), custom_call_target="tpu_custom_call" | custom-call | flops 1610612736 | tf_op jit(solution)/shard_map/pallas_call | solution.py:918
  146.6 0.1 collective-permute-start.15
  146.7 2.6 %collective-permute-start.16 = (bf16[128,1024]{1,0:T(8,128)(2,1)S(1)}, bf16[128,1024]{1,0:T(8,128)(2,1)S(1)}, u32[]{:S(2)}, u32[]{:S(2)}) collective-permute-start(bf16[128,1024]{1,0:T(8,128)(2,1)S(1)} %get-tuple-element.24), channel_id=1, source_target_pairs={{0,24},{2,26},{4,28},{6,30},{8,16},{10,18},{12,20},{14,22},{16,8},... | collective-permute-start | bytes 786440 | tf_op jit(solution)/shard_map/ppermute | solution.py:847
  149.4 0.7 bitcast_dynamic-update-slice_fusion
  150.1 3.5 %all-to-all-start.1 = ((bf16[8,272,128]{2,1,0:T(8,128)(2,1)}), bf16[8,272,128]{2,1,0:T(8,128)(2,1)S(1)}, u32[]{:S(2)}, u32[]{:S(2)}) async-start(bf16[8,272,128]{2,1,0:T(8,128)(2,1)} %bitcast.45), calls=%async_computation.1 | async-start | bytes 1114112 | tf_op jit(solution)/shard_map/all_to_all | solution.py:932
  153.6 1.9 collective-permute-start.14
  155.6 12.0 %collective-permute-done.15 = bf16[128,1024]{1,0:T(8,128)(2,1)S(1)} collective-permute-done((bf16[128,1024]{1,0:T(8,128)(2,1)S(1)}, bf16[128,1024]{1,0:T(8,128)(2,1)S(1)}, u32[]{:S(2)}, u32[]{:S(2)}) %collective-permute-start.15) | collective-permute-done | bytes 262176 | tf_op jit(solution)/shard_map/ppermute | solution.py:847
  167.7 0.4 collective-permute-start.20
  168.1 11.0 %collective-permute-done.14 = bf16[128,1024]{1,0:T(8,128)(2,1)S(1)} collective-permute-done((bf16[128,1024]{1,0:T(8,128)(2,1)S(1)}, bf16[128,1024]{1,0:T(8,128)(2,1)S(1)}, u32[]{:S(2)}, u32[]{:S(2)}) %collective-permute-start.14) | collective-permute-done | bytes 262176 | tf_op jit(solution)/shard_map/ppermute | solution.py:847
  179.1 1.4 collective-permute-start.17
  180.5 0.8 collective-permute-start.18
  181.3 0.4 collective-permute-start.19
  181.7 1.4 collective-permute-done.20.refs_5_
  183.1 10.9 %collective-permute-done.17.refs_2_ = bf16[256,1024]{1,0:T(8,128)(2,1)S(1)} collective-permute-done((bf16[256,1024]{1,0:T(8,128)(2,1)S(1)}, bf16[256,1024]{1,0:T(8,128)(2,1)S(1)}, u32[]{:S(2)}, u32[]{:S(2)}) %collective-permute-start.17) | collective-permute-done | bytes 524320 | tf_op jit(solution)/shard_map/ppermute | solution.py:895
  194.0 0.4 collective-permute-start.21
  194.4 10.9 %collective-permute-done.18.refs_3_ = bf16[256,1024]{1,0:T(8,128)(2,1)S(1)} collective-permute-done((bf16[256,1024]{1,0:T(8,128)(2,1)S(1)}, bf16[256,1024]{1,0:T(8,128)(2,1)S(1)}, u32[]{:S(2)}, u32[]{:S(2)}) %collective-permute-start.18) | collective-permute-done | bytes 524320 | tf_op jit(solution)/shard_map/ppermute | solution.py:895
  205.2 10.3 %collective-permute-done.22.refs_7_ = bf16[256,1024]{1,0:T(8,128)(2,1)S(1)} collective-permute-done((bf16[256,1024]{1,0:T(8,128)(2,1)S(1)}, bf16[256,1024]{1,0:T(8,128)(2,1)S(1)}, u32[]{:S(2)}, u32[]{:S(2)}) %collective-permute-start.22) | collective-permute-done | bytes 524320 | tf_op jit(solution)/shard_map/ppermute | solution.py:895
  215.6 0.7 copy-done.11
  216.3 0.2 copy-done.12
  216.5 0.2 copy-done.6
  216.7 5.8 %shard_map.172 = (bf16[256,1024]{1,0:T(8,128)(2,1)}, f32[8,256]{1,0:T(8,128)}) custom-call(s32[7]{0:T(128)} %stack.62.meta, bf16[8,272,128]{2,1,0:T(8,128)(2,1)} %copy-done.2, bf16[8,272,128]{2,1,0:T(8,128)(2,1)} %bitcast.46, bf16[256,1024]{1,0:T(8,128)(2,1)} %copy-done.5, bf16[256,1024]{1,0:T(8,128)(2,1)} %copy-done.3, bf16[256,1024]{1,0:T(8,128)(2,1)} %copy-done.8, ...), custom_call_target="tpu_custom_call" | custom-call | flops 1073741824 | tf_op jit(solution)/shard_map/pallas_call | solution.py:943
  (72 shorter events, 0.5 us)
Async XLA Ops:
  6.3 2.1 collective-permute-start.8
  9.4 8.4 %copy-start.1 = (bf16[256,2048]{1,0:T(8,128)(2,1)S(1)}, bf16[256,2048]{1,0:T(8,128)(2,1)}, u32[]{:S(2)}) copy-start(bf16[256,2048]{1,0:T(8,128)(2,1)} %param.16) | copy-start | bytes 3145732
  9.4 43.2 %copy-start.16 = (f32[2048]{0:T(1024)S(1)}, f32[2048]{0:T(1024)}, u32[]{:S(2)}) copy-start(f32[2048]{0:T(1024)} %param.17) | copy-start | bytes 24580
  9.4 43.1 %all-to-all-start = ((bf16[16,392,128]{2,1,0:T(8,128)(2,1)}), bf16[16,392,128]{2,1,0:T(8,128)(2,1)S(1)}, u32[]{:S(2)}, u32[]{:S(2)}) async-start(bf16[16,392,128]{2,1,0:T(8,128)(2,1)} %bitcast.44), calls=%async_computation | async-start | bytes 3211264 | tf_op jit(solution)/shard_map/all_to_all | solution.py:837
  17.8 46.1 %copy-start.17 = (f32[4,4]{1,0:T(4,128)S(1)}, f32[4,4]{1,0:T(4,128)}, u32[]{:S(2)}) copy-start(f32[4,4]{1,0:T(4,128)} %param.23) | copy-start | bytes 196
  17.8 46.2 %copy-start.18 = (f32[512]{0:T(512)S(1)}, f32[512]{0:T(512)}, u32[]{:S(2)}) copy-start(f32[512]{0:T(512)} %param.25) | copy-start | bytes 6148
  17.8 46.2 %copy-start.19 = (f32[8]{0:T(128)S(1)}, f32[8]{0:T(128)}, u32[]{:S(2)}) copy-start(f32[8]{0:T(128)} %param.29) | copy-start | bytes 100
  52.5 32.2 %copy-start = (bf16[16,392,128]{2,1,0:T(8,128)(2,1)}, bf16[16,392,128]{2,1,0:T(8,128)(2,1)S(1)}, u32[]{:S(2)}) copy-start(bf16[16,392,128]{2,1,0:T(8,128)(2,1)S(1)} %all-to-all-done.refs_8_) | copy-start | bytes 4816900
  52.5 27.4 %collective-permute-start.9 = (bf16[6272,128]{1,0:T(8,128)(2,1)S(1)}, bf16[6272,128]{1,0:T(8,128)(2,1)}, u32[]{:S(2)}, u32[]{:S(2)}) collective-permute-start(bf16[6272,128]{1,0:T(8,128)(2,1)S(1)} %bitcast.42), channel_id=1, source_target_pairs={{0,1},{1,0},{2,3},{3,2},{4,5},{5,4},{6,7},{7,6},{8,9},{9,8},{10,11... | collective-permute-start | bytes 4816904 | tf_op jit(solution)/shard_map/ppermute | solution.py:799
  54.0 19.4 %collective-permute-start.4 = (bf16[256,2048]{1,0:T(8,128)(2,1)}, bf16[256,2048]{1,0:T(8,128)(2,1)S(1)}, u32[]{:S(2)}, u32[]{:S(2)}) collective-permute-start(bf16[256,2048]{1,0:T(8,128)(2,1)} %fusion.2.refs_0_), channel_id=1, source_target_pairs={{0,8},{2,10},{4,12},{6,14},{9,1},{11,3},{13,5},{15,7},{16,24},{18,... | collective-permute-start | bytes 3145736 | tf_op jit(solution)/shard_map/ppermute | solution.py:807
  60.9 17.3 %collective-permute-start.1 = (bf16[256,2048]{1,0:T(8,128)(2,1)}, bf16[256,2048]{1,0:T(8,128)(2,1)}, u32[]{:S(2)}, u32[]{:S(2)}) collective-permute-start(bf16[256,2048]{1,0:T(8,128)(2,1)} %fusion.2.refs_0_), channel_id=1, source_target_pairs={{0,2},{2,0},{4,6},{6,4},{9,11},{11,9},{13,15},{15,13},{16,18},{18,... | collective-permute-start | bytes 3145736 | tf_op jit(solution)/shard_map/ppermute | solution.py:813
  64.0 3.7 %collective-permute-start = (f32[5,128]{1,0:T(8,128)S(1)}, f32[5,128]{1,0:T(8,128)S(1)}, u32[]{:S(2)}, u32[]{:S(2)}) collective-permute-start(f32[5,128]{1,0:T(8,128)S(1)} %get-tuple-element.32), channel_id=1, source_target_pairs={{0,1},{1,0},{2,3},{3,2},{4,5},{5,4},{6,7},{7,6},{8,9},{9,8},{10,11... | collective-permute-start | bytes 7688 | tf_op jit(solution)/shard_map/ppermute | solution.py:799
  64.1 22.8 %collective-permute-start.2 = (bf16[256,2048]{1,0:T(8,128)(2,1)}, bf16[256,2048]{1,0:T(8,128)(2,1)}, u32[]{:S(2)}, u32[]{:S(2)}) collective-permute-start(bf16[256,2048]{1,0:T(8,128)(2,1)} %fusion.2.refs_0_), channel_id=1, source_target_pairs={{0,4},{2,6},{4,0},{6,2},{9,13},{11,15},{13,9},{15,11},{16,20},{18,... | collective-permute-start | bytes 3145736 | tf_op jit(solution)/shard_map/ppermute | solution.py:813
  67.7 34.2 %collective-permute-start.3 = (bf16[256,2048]{1,0:T(8,128)(2,1)}, bf16[256,2048]{1,0:T(8,128)(2,1)}, u32[]{:S(2)}, u32[]{:S(2)}) collective-permute-start(bf16[256,2048]{1,0:T(8,128)(2,1)} %fusion.2.refs_0_), channel_id=1, source_target_pairs={{0,6},{2,4},{4,2},{6,0},{9,15},{11,13},{13,11},{15,9},{16,22},{18,... | collective-permute-start | bytes 3145736 | tf_op jit(solution)/shard_map/ppermute | solution.py:813
  73.4 28.5 %copy-start.4 = (bf16[256,2048]{1,0:T(8,128)(2,1)}, bf16[256,2048]{1,0:T(8,128)(2,1)S(1)}, u32[]{:S(2)}) copy-start(bf16[256,2048]{1,0:T(8,128)(2,1)S(1)} %collective-permute-done.4.refs_4_) | copy-start | bytes 3145732
  73.4 28.5 %collective-permute-start.5 = (bf16[256,2048]{1,0:T(8,128)(2,1)S(1)}, bf16[256,2048]{1,0:T(8,128)(2,1)}, u32[]{:S(2)}, u32[]{:S(2)}) collective-permute-start(bf16[256,2048]{1,0:T(8,128)(2,1)S(1)} %collective-permute-done.4.refs_4_), channel_id=1, source_target_pairs={{1,3},{3,1},{5,7},{7,5},{8,10},{10,8},{12,14},{14,12},{17,19},{19,... | collective-permute-start | bytes 3145736 | tf_op jit(solution)/shard_map/ppermute | solution.py:840
  78.2 23.7 %collective-permute-start.6 = (bf16[256,2048]{1,0:T(8,128)(2,1)S(1)}, bf16[256,2048]{1,0:T(8,128)(2,1)}, u32[]{:S(2)}, u32[]{:S(2)}) collective-permute-start(bf16[256,2048]{1,0:T(8,128)(2,1)S(1)} %collective-permute-done.4.refs_4_), channel_id=1, source_target_pairs={{1,5},{3,7},{5,1},{7,3},{8,12},{10,14},{12,8},{14,10},{17,21},{19,... | collective-permute-start | bytes 3145736 | tf_op jit(solution)/shard_map/ppermute | solution.py:840
  79.9 22.0 %collective-permute-start.7 = (bf16[256,2048]{1,0:T(8,128)(2,1)S(1)}, bf16[256,2048]{1,0:T(8,128)(2,1)}, u32[]{:S(2)}, u32[]{:S(2)}) collective-permute-start(bf16[256,2048]{1,0:T(8,128)(2,1)S(1)} %collective-permute-done.4.refs_4_), channel_id=1, source_target_pairs={{1,7},{3,5},{5,3},{7,1},{8,14},{10,12},{12,10},{14,8},{17,23},{19,... | collective-permute-start | bytes 3145736 | tf_op jit(solution)/shard_map/ppermute | solution.py:840
  113.6 14.1 %collective-permute-start.10 = (f32[2,264,128]{2,1,0:T(8,128)}, f32[2,264,128]{2,1,0:T(8,128)S(1)}, u32[]{:S(2)}, u32[]{:S(2)}) collective-permute-start(f32[2,264,128]{2,1,0:T(8,128)} %get-tuple-element.19.own), channel_id=1, source_target_pairs={{0,1},{1,0},{2,3},{3,2},{4,5},{5,4},{6,7},{7,6},{8,9},{9,8},{10,11... | collective-permute-start | bytes 811016 | tf_op jit(solution)/shard_map/ppermute | solution.py:799
  127.7 0.7 copy-start.13
  130.2 8.6 %collective-permute-start.11 = (f32[264,128]{1,0:T(8,128)}, f32[264,128]{1,0:T(8,128)S(1)}, u32[]{:S(2)}, u32[]{:S(2)}) collective-permute-start(f32[264,128]{1,0:T(8,128)} %shard_map.169), channel_id=1, source_target_pairs={{0,16},{2,18},{4,20},{6,22},{8,24},{10,26},{12,28},{14,30},{16,0},... | collective-permute-start | bytes 405512 | tf_op jit(solution)/shard_map/ppermute | solution.py:905
  138.8 0.7 copy-start.20
  139.4 7.2 %copy-start.14 = (bf16[64,1024]{1,0:T(8,128)(2,1)S(1)}, bf16[64,1024]{1,0:T(8,128)(2,1)}, u32[]{:S(2)}) copy-start(bf16[64,1024]{1,0:T(8,128)(2,1)} %param.30) | copy-start | bytes 393220
  139.4 7.2 %copy-start.15 = (bf16[64,1024]{1,0:T(8,128)(2,1)S(1)}, bf16[64,1024]{1,0:T(8,128)(2,1)}, u32[]{:S(2)}) copy-start(bf16[64,1024]{1,0:T(8,128)(2,1)} %param.31) | copy-start | bytes 393220
  146.5 2.9 %collective-permute-start.12 = (bf16[4,272,128]{2,1,0:T(8,128)(2,1)}, bf16[4,272,128]{2,1,0:T(8,128)(2,1)S(1)}, u32[]{:S(2)}, u32[]{:S(2)}) collective-permute-start(bf16[4,272,128]{2,1,0:T(8,128)(2,1)} %get-tuple-element.23), channel_id=1, source_target_pairs={{0,1},{1,0},{2,3},{3,2},{4,5},{5,4},{6,7},{7,6},{8,9},{9,8},{10,11... | collective-permute-start | bytes 835592 | tf_op jit(solution)/shard_map/ppermute | solution.py:799
  146.6 21.0 %collective-permute-start.15 = (bf16[128,1024]{1,0:T(8,128)(2,1)S(1)}, bf16[128,1024]{1,0:T(8,128)(2,1)S(1)}, u32[]{:S(2)}, u32[]{:S(2)}) collective-permute-start(bf16[128,1024]{1,0:T(8,128)(2,1)S(1)} %get-tuple-element.24), channel_id=1, source_target_pairs={{0,16},{2,18},{4,20},{6,22},{8,24},{10,26},{12,28},{14,30},{16,0},... | collective-permute-start | bytes 786440 | tf_op jit(solution)/shard_map/ppermute | solution.py:847
  146.7 20.9 %collective-permute-start.16 = (bf16[128,1024]{1,0:T(8,128)(2,1)S(1)}, bf16[128,1024]{1,0:T(8,128)(2,1)S(1)}, u32[]{:S(2)}, u32[]{:S(2)}) collective-permute-start(bf16[128,1024]{1,0:T(8,128)(2,1)S(1)} %get-tuple-element.24), channel_id=1, source_target_pairs={{0,24},{2,26},{4,28},{6,30},{8,16},{10,18},{12,20},{14,22},{16,8},... | collective-permute-start | bytes 786440 | tf_op jit(solution)/shard_map/ppermute | solution.py:847
  150.1 30.4 %all-to-all-start.1 = ((bf16[8,272,128]{2,1,0:T(8,128)(2,1)}), bf16[8,272,128]{2,1,0:T(8,128)(2,1)S(1)}, u32[]{:S(2)}, u32[]{:S(2)}) async-start(bf16[8,272,128]{2,1,0:T(8,128)(2,1)} %bitcast.45), calls=%async_computation.1 | async-start | bytes 1114112 | tf_op jit(solution)/shard_map/all_to_all | solution.py:932
  153.6 25.4 %collective-permute-start.14 = (bf16[128,1024]{1,0:T(8,128)(2,1)S(1)}, bf16[128,1024]{1,0:T(8,128)(2,1)S(1)}, u32[]{:S(2)}, u32[]{:S(2)}) collective-permute-start(bf16[128,1024]{1,0:T(8,128)(2,1)S(1)} %get-tuple-element.24), channel_id=1, source_target_pairs={{0,8},{2,10},{4,12},{6,14},{8,0},{10,2},{12,4},{14,6},{16,24},{18,... | collective-permute-start | bytes 786440 | tf_op jit(solution)/shard_map/ppermute | solution.py:847
  167.7 47.9 %copy-start.3 = (bf16[256,1024]{1,0:T(8,128)(2,1)}, bf16[256,1024]{1,0:T(8,128)(2,1)S(1)}, u32[]{:S(2)}) copy-start(bf16[256,1024]{1,0:T(8,128)(2,1)S(1)} %constant_dynamic-update-slice_fusion.5.refs_1_) | copy-start | bytes 1572868
  167.7 15.4 %collective-permute-start.20 = (bf16[256,1024]{1,0:T(8,128)(2,1)S(1)}, bf16[256,1024]{1,0:T(8,128)(2,1)S(1)}, u32[]{:S(2)}, u32[]{:S(2)}) collective-permute-start(bf16[256,1024]{1,0:T(8,128)(2,1)S(1)} %constant_dynamic-update-slice_fusion.5.refs_1_), channel_id=1, source_target_pairs={{0,4},{2,6},{4,0},{6,2},{8,12},{10,14},{12,8},{14,10},{16,20},{18,... | collective-permute-start | bytes 1572872 | tf_op jit(solution)/shard_map/ppermute | solution.py:895
  179.1 36.5 %copy-start.5 = (bf16[256,1024]{1,0:T(8,128)(2,1)}, bf16[256,1024]{1,0:T(8,128)(2,1)S(1)}, u32[]{:S(2)}) copy-start(bf16[256,1024]{1,0:T(8,128)(2,1)S(1)} %constant_dynamic-update-slice_fusion.2.refs_0_) | copy-start | bytes 1572868
  179.1 14.9 %collective-permute-start.17 = (bf16[256,1024]{1,0:T(8,128)(2,1)S(1)}, bf16[256,1024]{1,0:T(8,128)(2,1)S(1)}, u32[]{:S(2)}, u32[]{:S(2)}) collective-permute-start(bf16[256,1024]{1,0:T(8,128)(2,1)S(1)} %constant_dynamic-update-slice_fusion.2.refs_0_), channel_id=1, source_target_pairs={{0,2},{2,0},{4,6},{6,4},{8,10},{10,8},{12,14},{14,12},{16,18},{18,... | collective-permute-start | bytes 1572872 | tf_op jit(solution)/shard_map/ppermute | solution.py:895
  180.5 35.1 %copy-start.2 = (bf16[8,272,128]{2,1,0:T(8,128)(2,1)}, bf16[8,272,128]{2,1,0:T(8,128)(2,1)S(1)}, u32[]{:S(2)}) copy-start(bf16[8,272,128]{2,1,0:T(8,128)(2,1)S(1)} %all-to-all-done.1.own) | copy-start | bytes 1671172
  180.5 35.0 %collective-permute-start.13 = (bf16[2176,128]{1,0:T(8,128)(2,1)S(1)}, bf16[2176,128]{1,0:T(8,128)(2,1)S(1)}, u32[]{:S(2)}, u32[]{:S(2)}) collective-permute-start(bf16[2176,128]{1,0:T(8,128)(2,1)S(1)} %bitcast.43), channel_id=1, source_target_pairs={{0,1},{1,0},{2,3},{3,2},{4,5},{5,4},{6,7},{7,6},{8,9},{9,8},{10,11... | collective-permute-start | bytes 1671176 | tf_op jit(solution)/shard_map/ppermute | solution.py:799
  180.5 24.7 %collective-permute-start.18 = (bf16[256,1024]{1,0:T(8,128)(2,1)S(1)}, bf16[256,1024]{1,0:T(8,128)(2,1)S(1)}, u32[]{:S(2)}, u32[]{:S(2)}) collective-permute-start(bf16[256,1024]{1,0:T(8,128)(2,1)S(1)} %constant_dynamic-update-slice_fusion.5.refs_1_), channel_id=1, source_target_pairs={{0,2},{2,0},{4,6},{6,4},{8,10},{10,8},{12,14},{14,12},{16,18},{18,... | collective-permute-start | bytes 1572872 | tf_op jit(solution)/shard_map/ppermute | solution.py:895
  181.3 23.9 %collective-permute-start.19 = (bf16[256,1024]{1,0:T(8,128)(2,1)S(1)}, bf16[256,1024]{1,0:T(8,128)(2,1)S(1)}, u32[]{:S(2)}, u32[]{:S(2)}) collective-permute-start(bf16[256,1024]{1,0:T(8,128)(2,1)S(1)} %constant_dynamic-update-slice_fusion.2.refs_0_), channel_id=1, source_target_pairs={{0,4},{2,6},{4,0},{6,2},{8,12},{10,14},{12,8},{14,10},{16,20},{18,... | collective-permute-start | bytes 1572872 | tf_op jit(solution)/shard_map/ppermute | solution.py:895
  183.1 32.5 %copy-start.7 = (bf16[256,1024]{1,0:T(8,128)(2,1)}, bf16[256,1024]{1,0:T(8,128)(2,1)S(1)}, u32[]{:S(2)}) copy-start(bf16[256,1024]{1,0:T(8,128)(2,1)S(1)} %collective-permute-done.20.refs_5_) | copy-start | bytes 1572868
  183.1 32.4 %collective-permute-start.22 = (bf16[256,1024]{1,0:T(8,128)(2,1)S(1)}, bf16[256,1024]{1,0:T(8,128)(2,1)S(1)}, u32[]{:S(2)}, u32[]{:S(2)}) collective-permute-start(bf16[256,1024]{1,0:T(8,128)(2,1)S(1)} %collective-permute-done.20.refs_5_), channel_id=1, source_target_pairs={{0,2},{2,0},{4,6},{6,4},{8,10},{10,8},{12,14},{14,12},{16,18},{18,... | collective-permute-start | bytes 1572872 | tf_op jit(solution)/shard_map/ppermute | solution.py:895
  194.0 21.6 %copy-start.8 = (bf16[256,1024]{1,0:T(8,128)(2,1)}, bf16[256,1024]{1,0:T(8,128)(2,1)S(1)}, u32[]{:S(2)}) copy-start(bf16[256,1024]{1,0:T(8,128)(2,1)S(1)} %collective-permute-done.17.refs_2_) | copy-start | bytes 1572868
  194.0 21.6 %collective-permute-start.21 = (bf16[256,1024]{1,0:T(8,128)(2,1)S(1)}, bf16[256,1024]{1,0:T(8,128)(2,1)S(1)}, u32[]{:S(2)}, u32[]{:S(2)}) collective-permute-start(bf16[256,1024]{1,0:T(8,128)(2,1)S(1)} %collective-permute-done.17.refs_2_), channel_id=1, source_target_pairs={{0,4},{2,6},{4,0},{6,2},{8,12},{10,14},{12,8},{14,10},{16,20},{18,... | collective-permute-start | bytes 1572872 | tf_op jit(solution)/shard_map/ppermute | solution.py:895
  205.2 10.4 %copy-start.9 = (bf16[256,1024]{1,0:T(8,128)(2,1)}, bf16[256,1024]{1,0:T(8,128)(2,1)S(1)}, u32[]{:S(2)}) copy-start(bf16[256,1024]{1,0:T(8,128)(2,1)S(1)} %collective-permute-done.18.refs_3_) | copy-start | bytes 1572868
  205.2 10.4 %copy-start.10 = (bf16[256,1024]{1,0:T(8,128)(2,1)}, bf16[256,1024]{1,0:T(8,128)(2,1)S(1)}, u32[]{:S(2)}) copy-start(bf16[256,1024]{1,0:T(8,128)(2,1)S(1)} %collective-permute-done.19.refs_4_) | copy-start | bytes 1572868
  215.5 0.8 copy-start.11
  215.5 1.0 copy-start.12
  215.5 1.2 copy-start.6

commit v4 on v3

--- a/solution.py
+++ b/solution.py
@@ -348,10 +348,10 @@
     )
 
 
-def vmem_call(kernel, outs, scratch=(), smem=0, n_in=0, flops=0, n_any=0, n_tail=0):
+def vmem_call(kernel, outs, scratch=(), smem=0, n_in=0, flops=0, n_any=0, n_tail=0, keep=False):
     return pl.pallas_call(
         kernel,
-        out_shape=outs,
+        out_shape=jax.tree.map(lambda x: pltpu.VMEM(x.shape, x.dtype), outs) if keep else outs,
         in_specs=[pl.BlockSpec(memory_space=pltpu.SMEM)] * smem
         + [pl.BlockSpec(memory_space=pltpu.VMEM)] * n_in
         + [pl.BlockSpec(memory_space=pl.ANY)] * n_any
@@ -359,8 +359,12 @@
         out_specs=jax.tree.map(lambda _: pl.BlockSpec(memory_space=pltpu.VMEM), outs),
         scratch_shapes=scratch,
         cost_estimate=pl.CostEstimate(flops=flops, bytes_accessed=0, transcendentals=0),
-        compiler_params=pltpu.CompilerParams(vmem_limit_bytes=56 * 1024 * 1024),
-    )
+        compiler_params=pltpu.CompilerParams(vmem_limit_bytes=24 * 1024 * 1024),
+    )
+
+
+def near(*arrays):
+    return [pltpu.with_memory_space_constraint(x, pltpu.VMEM) for x in arrays]
 
 
 def pack_kernel(meta, mq, mk, mv, mo, aq, ak, av, small, keep, send):
@@ -416,18 +420,52 @@
     return old * earlier[0] + new * later[0], peak
 
 
+def weave_kernel(meta, own, partner, weight, gate_t, decay):
+    t, hi = meta[0], meta[4]
+    sources = own.shape[0]
+    rows = weight.shape[0] // sources // 2
+    cols = weight.shape[1] // LANES
+    plane = decay.shape[1]
+    for i in range(sources):
+        first = pl.multiple_of((2 * i + t) * rows, rows)
+        second = pl.multiple_of((2 * i + 1 - t) * rows, rows)
+        for c in range(cols):
+            lanes = slice(c * LANES, (c + 1) * LANES)
+            span = slice(c * rows, (c + 1) * rows)
+            weight[pl.ds(first, rows), lanes] = own[i, span, :]
+            weight[pl.ds(second, rows), lanes] = partner[i, span, :]
+
+    def small(ref, i):
+        return ref[i, cols * rows :, :].astype(jnp.float32)
+
+    gate_t[...] = jnp.zeros(gate_t.shape, jnp.bfloat16)
+    for i in range(sources):
+        pair = [
+            jnp.concatenate(
+                [x[0:1, :rows], x[0:1, rows:], x[1:2, :rows], x[1:2, rows:]], axis=0
+            )
+            for x in (small(own, i), small(partner, i))
+        ]
+        piece = jnp.where(
+            t == 0,
+            jnp.concatenate(pair, axis=1),
+            jnp.concatenate(pair[::-1], axis=1),
+        )
+        piece = jnp.concatenate([piece, jnp.zeros((12, LANES), jnp.float32)], axis=0)
+        gate_t[:16, i * LANES : (i + 1) * LANES] = piece.astype(jnp.bfloat16)
+    for b in range(plane):
+        for ref, at in ((own, t), (partner, 1 - t)):
+            x = small(ref, (2 * hi + t) * plane + b)
+            x = x[2:4] + x[4:6] + x[6:8]
+            decay[at, b : b + 1, :] = jnp.concatenate([x[:1], x[1:]], axis=1)
+
+
 def project_kernel(meta, bias, *refs):
-    plane = (len(refs) - 14) // 2
+    plane = (len(refs) - 11) // 2
     same, other = refs[:plane], refs[plane : 2 * plane]
-    own, partner, gate_t, decay = refs[2 * plane : 2 * plane + 4]
-    proj, vrows, vcols, local, summary, weight, xs, raw, gates, sems = refs[2 * plane + 4 :]
+    weight, gate_t, decay = refs[2 * plane : 2 * plane + 3]
+    proj, vrows, vcols, local, summary, xs, gates, sems = refs[2 * plane + 3 :]
     t, k, sel, jl, near = meta[0], meta[1], meta[2], meta[3], meta[5]
-    copies = [
-        pltpu.make_async_copy(own, raw.at[0], sems.at[plane]),
-        pltpu.make_async_copy(partner, raw.at[1], sems.at[plane + 1]),
-    ]
-    for copy in copies:
-        copy.start()
 
     @pl.when(t == near)
     def _():
@@ -439,19 +477,6 @@
         for r in range(plane):
             pltpu.make_async_copy(other[r], xs.at[r], sems.at[r]).start()
 
-    for copy in copies:
-        copy.wait()
-    sources = own.shape[0]
-    rows = weight.shape[0] // sources // 2
-    cols = weight.shape[1] // LANES
-    for i in range(sources):
-        for c in range(cols):
-            lanes = slice(c * LANES, (c + 1) * LANES)
-            span = slice(c * rows, (c + 1) * rows)
-            first = pl.multiple_of((2 * i + t) * rows, rows)
-            second = pl.multiple_of((2 * i + 1 - t) * rows, rows)
-            weight[pl.ds(first, rows), lanes] = raw[0, i, span, :]
-            weight[pl.ds(second, rows), lanes] = raw[1, i, span, :]
     tok = xs.shape[1]
     for r in range(plane):
         pltpu.make_async_copy(same[r], xs.at[r], sems.at[r]).wait()
@@ -820,8 +845,7 @@
         2, lh, 3 * tok // LANES, LANES
     )
     small = jnp.concatenate([gate_rows, decay_rows], axis=2)
-    n_gate, n_small = gate_rows.shape[2], small.shape[2]
-    n_rows = 6 * half + n_small
+    n_rows = 6 * half + small.shape[2]
     spread, send = vmem_call(
         pack_kernel,
         (
@@ -846,15 +870,6 @@
     for r in range(1, sp // plane):
         column.append(lax.ppermute(out_block, "sp", [(a, a ^ (r * plane)) for a in range(sp)]))
     partner_w = flip(own_w)
-    own_w = own_w.reshape(sp, n_rows, LANES)
-    partner_w = partner_w.reshape(sp, n_rows, LANES)
-    small_both = jnp.stack([own_w[:, 6 * half :], partner_w[:, 6 * half :]])
-    small_both = jnp.where(t == 0, small_both, small_both[::-1])
-    gate_t = jnp.transpose(small_both[:, :, :n_gate].reshape(2, sp, 4, half), (2, 1, 0, 3))
-    gate_t = jnp.pad(gate_t.reshape(4, width), ((0, LANES - 4), (0, 0)))
-    first = (2 * hi + t) * plane
-    decay = lax.dynamic_slice_in_dim(small_both[:, :, n_gate:], first, plane, 1)
-    decay = jnp.sum(decay.reshape(2, plane, 3, tok).astype(f32), axis=2)
     params = jnp.concatenate(
         [m_gain, gate_bias.reshape(-1), sink_logit, jnp.zeros((LANES - 6 * lh,), f32)]
     ).reshape(-1, LANES)
@@ -866,6 +881,18 @@
     quarter = plane * tok
     cols = 6 * LANES
     sum_rows = M_DIM + 8 + WINDOW
+    woven, gate_t, decay = vmem_call(
+        weave_kernel,
+        (
+            jax.ShapeDtypeStruct((width, cols), bf16),
+            jax.ShapeDtypeStruct((LANES, width), bf16),
+            jax.ShapeDtypeStruct((2, plane, tok), f32),
+        ),
+        smem=1,
+        n_in=2,
+        keep=True,
+        flops=quarter * width,
+    )(meta, *near(*(x.reshape(sp, n_rows, LANES) for x in (own_w, partner_w))))
     proj, vrows, vcols, local, summary = vmem_call(
         project_kernel,
         (
@@ -876,17 +903,16 @@
             jax.ShapeDtypeStruct((2, sum_rows, LANES), f32),
         ),
         scratch=[
-            pltpu.VMEM((width, cols), bf16),
             pltpu.VMEM((plane, tok, width), bf16),
-            pltpu.VMEM((2, sp, n_rows, LANES), bf16),
             pltpu.VMEM((plane, 8, tok), f32),
-            pltpu.SemaphoreType.DMA((plane + 2,)),
+            pltpu.SemaphoreType.DMA((plane,)),
         ],
         smem=2,
-        n_any=2 * plane + 2,
-        n_tail=2,
+        n_any=2 * plane,
+        n_tail=3,
+        keep=True,
         flops=2 * quarter * width * cols,
-    )(meta, bias, *same_xs, *other_xs, own_w, partner_w, gate_t, decay)
+    )(meta, bias, *same_xs, *other_xs, *near(woven, gate_t, decay))
     column = jnp.concatenate(column, axis=0)
     cut = column.shape[0] // 2
     upper, lower = column[:cut], column[cut:]
@@ -901,7 +927,7 @@
     partner_sum = flip(summary)
     sent = vmem_call(
         combine_kernel, jax.ShapeDtypeStruct((sum_rows, LANES), f32), smem=1, n_in=2
-    )(meta, summary, partner_sum)
+    )(meta, *near(summary, partner_sum))
     across = lax.ppermute(sent, "sp", [(a, (a + group) % sp) for a in range(sp)])
     blocks = quarter // WINDOW
     att, att_logs = vmem_call(
@@ -913,8 +939,9 @@
         scratch=[pltpu.VMEM((quarter + 2 * WINDOW, LANES), bf16)],
         smem=2,
         n_in=2,
+        keep=True,
         flops=quarter * width * cols,
-    )(meta, sink, proj, partner_sum)
+    )(meta, sink, *near(proj, partner_sum))
     spread, send = vmem_call(
         mixer_kernel,
         (
@@ -925,7 +952,7 @@
         smem=2,
         n_in=9,
         flops=quarter * width * cols,
-    )(meta, sink, proj, vrows, vcols, local, partner_sum, across, gain, att, att_logs)
+    )(meta, sink, *near(proj, vrows, vcols, local, partner_sum, across), gain, *near(att, att_logs))
     got = flip(send)
     spread = lax.dynamic_update_slice_in_dim(spread, got[None], 1 - t, 0)
     groups = [list(range(g * group, (g + 1) * group)) for g in range(sp // group)]
@@ -955,7 +982,7 @@
         n_in=2,
         n_any=2 * plane,
         flops=2 * tok * inner * out_m_weight.shape[1],
-    )(meta, mine.reshape(shape), theirs.reshape(shape), *out_blocks)
+    )(meta, *near(mine.reshape(shape), theirs.reshape(shape)), *out_blocks)
 
 
 def solution(mesh):

time: 223 us -> 223 us (level)
  waiting for transfers between devices: 119 us -> 126 us
  Pallas kernels: 33.7 us -> 30.4 us
  other arithmetic: 5.69 us -> 2.72 us
    ppermute x3, waiting for transfers between devices: 20.3 us -> 25.7 us  [on_device_split(): lax.ppermute(normed, both_axes, [(core(a, True), core(a ^ r, True)) for a...]
    unnamed x44 -> x30, local copies, waits for them, and re-layouts: 2.56 us -> 6.27 us
    pallas_call x1, Pallas kernels: 11.6 us -> 8.01 us  [on_device_split(): vmem_call(project_kernel, (jax.ShapeDtypeStruct((quarter, cols), bf16), j...]
    pallas_call x1, Pallas kernels: 5.8 us -> 9.08 us  [on_device_split(): vmem_call(output_kernel, (jax.ShapeDtypeStruct((tok, out_m_weight.shape[1...]
    ppermute x3, starting transfers between devices: 4.99 us -> 2.16 us  [on_device_split(): lax.ppermute(other, both_axes, [(core(a, False), core(a ^ r, False)) for...]
  transfers between devices with their start and end apart: 25 -> 25, of which waited for: 14 -> 14; matrix products, arithmetic and copies ran while one was open for 3% -> 1% of each run, Pallas kernels for 2% -> 2%
where the time goes in v4:
time: 223 us
  waiting for transfers between devices  126 us (57%)
  starting transfers between devices  53.7 us (24%)
  Pallas kernels  30.4 us (14%)
  local copies, waits for them, and re-layouts  9.17 us (4%)
  other arithmetic  2.72 us (1%)
    all_to_all x1, waiting for transfers between devices, on_device_split(): lax.all_to_all(spread.reshape(sp * n_rows, LANES), 'sp', 0, 0, tiled=True)  34.4 us
    ppermute x6, waiting for transfers between devices, hop(): return lax.ppermute(x, 'sp', [(a, a ^ r) for a in range(sp)])  33.6 us
    ppermute x3, waiting for transfers between devices, on_device_split(): lax.ppermute(normed, both_axes, [(core(a, True), core(a ^ r, True)) for a...  25.7 us
    ppermute x3, waiting for transfers between devices, on_device_split(): lax.ppermute(out_block, 'sp', [(a, a ^ r * plane) for a in range(sp)])  23 us
    ppermute x6, starting transfers between devices, flip(): return lax.ppermute(x, 'tp', swap)  13.8 us
    ppermute x3, starting transfers between devices, on_device_split(): lax.ppermute(normed, both_axes, [(core(a, True), core(a ^ r, True)) for a...  9.2 us
    pallas_call x1, Pallas kernels, on_device_split(): vmem_call(output_kernel, (jax.ShapeDtypeStruct((tok, out_m_weight.shape[1...  9.08 us
    all_to_all x1, starting transfers between devices, on_device_split(): lax.all_to_all(spread.reshape(sp * n_rows, LANES), 'sp', 0, 0, tiled=True)  8.35 us
  transfers between devices with their start and end apart: 25, of which 14 were waited for; matrix products, arithmetic and copies ran while one was open for 1% of the time, Pallas kernels for 2%

profile of v4, /device:TPU:0, one launch (start us, length us, event | category | flops | bytes accessed | tf_op | source)
XLA Modules:
  0.0 222.7 jit_solution(5280400074712078799)
XLA Ops:
  0.7 0.7 fusion.5
  1.5 0.8 reshape.51
  2.3 0.1 reshape.52
  2.4 0.1 stack.53.meta
  2.5 0.9 copy-done
  3.4 0.9 copy-done.1
  4.3 0.9 copy-done.2
  5.2 0.9 copy-done.3
  6.1 0.9 copy-done.4
  7.0 0.8 copy-done.5
  7.8 0.8 copy-done.6
  8.7 1.9 shard_map.167
  10.6 0.5 collective-permute-start.8
  11.1 1.4 collective-permute-done.8
  12.4 1.0 broadcast_dynamic-update-slice_fusion
  13.5 8.4 %all-to-all-start = ((bf16[16,392,128]{2,1,0:T(8,128)(2,1)}), bf16[16,392,128]{2,1,0:T(8,128)(2,1)S(1)}, u32[]{:S(2)}, u32[]{:S(2)}) async-start(bf16[16,392,128]{2,1,0:T(8,128)(2,1)} %bitcast.17), calls=%async_computation | async-start | bytes 3211264 | tf_op jit(solution)/shard_map/all_to_all | solution.py:861
  21.8 0.0 copy-start.11
  21.8 0.0 copy-start.12
  21.9 0.0 copy-start.13
  21.9 0.3 fusion
  22.2 34.4 %all-to-all-done.own = bf16[16,392,128]{2,1,0:T(8,128)(2,1)S(1)} async-done(((bf16[16,392,128]{2,1,0:T(8,128)(2,1)}), bf16[16,392,128]{2,1,0:T(8,128)(2,1)S(1)}, u32[]{:S(2)}, u32[]{:S(2)}) %all-to-all-start) | async-done | bytes 1605664 | tf_op jit(solution)/shard_map/all_to_all | solution.py:861
  56.6 1.5 fusion.2.refs_0_
  58.2 7.8 %collective-permute-start.4 = (bf16[256,2048]{1,0:T(8,128)(2,1)S(1)}, bf16[256,2048]{1,0:T(8,128)(2,1)}, u32[]{:S(2)}, u32[]{:S(2)}) collective-permute-start(bf16[256,2048]{1,0:T(8,128)(2,1)S(1)} %fusion.2.refs_0_), channel_id=1, source_target_pairs={{0,8},{2,10},{4,12},{6,14},{9,1},{11,3},{13,5},{15,7},{16,24},{18,... | collective-permute-start | bytes 3145736 | tf_op jit(solution)/shard_map/ppermute | solution.py:832
  65.9 3.0 %collective-permute-start.1 = (bf16[256,2048]{1,0:T(8,128)(2,1)S(1)}, bf16[256,2048]{1,0:T(8,128)(2,1)}, u32[]{:S(2)}, u32[]{:S(2)}) collective-permute-start(bf16[256,2048]{1,0:T(8,128)(2,1)S(1)} %fusion.2.refs_0_), channel_id=1, source_target_pairs={{0,2},{2,0},{4,6},{6,4},{9,11},{11,9},{13,15},{15,13},{16,18},{18,... | collective-permute-start | bytes 3145736 | tf_op jit(solution)/shard_map/ppermute | solution.py:838
  68.9 0.1 reshape.49
  69.0 0.1 fusion.8
  69.1 0.0 collective-permute-start
  69.1 3.6 %collective-permute-start.2 = (bf16[256,2048]{1,0:T(8,128)(2,1)S(1)}, bf16[256,2048]{1,0:T(8,128)(2,1)S(1)}, u32[]{:S(2)}, u32[]{:S(2)}) collective-permute-start(bf16[256,2048]{1,0:T(8,128)(2,1)S(1)} %fusion.2.refs_0_), channel_id=1, source_target_pairs={{0,4},{2,6},{4,0},{6,2},{9,13},{11,15},{13,9},{15,11},{16,20},{18,... | collective-permute-start | bytes 3145736 | tf_op jit(solution)/shard_map/ppermute | solution.py:838
  72.8 2.6 %collective-permute-start.3 = (bf16[256,2048]{1,0:T(8,128)(2,1)S(1)}, bf16[256,2048]{1,0:T(8,128)(2,1)S(1)}, u32[]{:S(2)}, u32[]{:S(2)}) collective-permute-start(bf16[256,2048]{1,0:T(8,128)(2,1)S(1)} %fusion.2.refs_0_), channel_id=1, source_target_pairs={{0,6},{2,4},{4,2},{6,0},{9,15},{11,13},{13,11},{15,9},{16,22},{18,... | collective-permute-start | bytes 3145736 | tf_op jit(solution)/shard_map/ppermute | solution.py:838
  75.4 1.9 collective-permute-done.4.refs_4_
  77.2 0.7 collective-permute-start.5
  78.0 5.6 %collective-permute-done.1.refs_1_ = bf16[256,2048]{1,0:T(8,128)(2,1)} collective-permute-done((bf16[256,2048]{1,0:T(8,128)(2,1)S(1)}, bf16[256,2048]{1,0:T(8,128)(2,1)}, u32[]{:S(2)}, u32[]{:S(2)}) %collective-permute-start.1) | collective-permute-done | bytes 1048608 | tf_op jit(solution)/shard_map/ppermute | solution.py:838
  83.6 0.7 collective-permute-start.6
  84.3 0.7 collective-permute-start.7
  85.0 2.0 shard_map.168
  87.1 4.0 %collective-permute-done.2.refs_2_ = bf16[256,2048]{1,0:T(8,128)(2,1)S(1)} collective-permute-done((bf16[256,2048]{1,0:T(8,128)(2,1)S(1)}, bf16[256,2048]{1,0:T(8,128)(2,1)S(1)}, u32[]{:S(2)}, u32[]{:S(2)}) %collective-permute-start.2) | collective-permute-done | bytes 1048608 | tf_op jit(solution)/shard_map/ppermute | solution.py:838
  91.1 16.1 %collective-permute-done.3.refs_3_ = bf16[256,2048]{1,0:T(8,128)(2,1)S(1)} collective-permute-done((bf16[256,2048]{1,0:T(8,128)(2,1)S(1)}, bf16[256,2048]{1,0:T(8,128)(2,1)S(1)}, u32[]{:S(2)}, u32[]{:S(2)}) %collective-permute-start.3) | collective-permute-done | bytes 1048608 | tf_op jit(solution)/shard_map/ppermute | solution.py:838
  107.2 8.0 %shard_map.169 = (bf16[1024,768]{1,0:T(8,128)(2,1)S(1)}, f32[24,256]{1,0:T(8,128)S(1)}, f32[256,128]{1,0:T(8,128)S(1)}, f32[2,4,128,256]{3,2,1,0:T(8,128)S(1)}, f32[2,264,128]{2,1,0:T(8,128)S(1)}) custom-call(s32[7]{0:T(128)S(1)} %stack.53.meta, f32[2,16]{1,0:T(2,128)S(1)} %bitcast.38, bf16[256,2048]{1,0:T(8,128)(2,1)S(1)} %fusion.2.refs_0_, ...), custom_call_target="tpu_custom_call" | custom-call | flops 3221225472 | tf_op jit(solution)/shard_map/pallas_call | solution.py:896
  115.2 13.2 %collective-permute-start.10 = (f32[2,264,128]{2,1,0:T(8,128)S(1)}, f32[2,264,128]{2,1,0:T(8,128)S(1)}, u32[]{:S(2)}, u32[]{:S(2)}) collective-permute-start(f32[2,264,128]{2,1,0:T(8,128)S(1)} %get-tuple-element.25.own), channel_id=1, source_target_pairs={{0,1},{1,0},{2,3},{3,2},{4,5},{5,4},{6,7},{7,6},{8,9},{9,8},{10,11... | collective-permute-start | bytes 811016 | tf_op jit(solution)/shard_map/ppermute | solution.py:824
  128.4 0.1 pad_maximum_fusion.4
  128.5 1.1 collective-permute-done.10.partner
  129.6 0.6 shard_map.170
  130.2 1.0 collective-permute-start.11
  131.2 3.2 %shard_map.171 = (bf16[8,128,128]{2,1,0:T(8,128)(2,1)S(1)}, f32[8,8,128]{2,1,0:T(8,128)S(1)}) custom-call(s32[7]{0:T(128)S(1)} %stack.53.meta, f32[2,8]{1,0:T(2,128)S(1)} %bitcast.39, bf16[1024,768]{1,0:T(8,128)(2,1)S(1)} %get-tuple-element.21.proj, f32[2,264,128]{2,1,0:T(8,128)S(1)} %collective-permute-done.10.partner), custom_call_target="tpu_custom_call" | custom-call | flops 1610612736 | tf_op jit(solution)/shard_map/pallas_call | solution.py:933
  134.3 4.5 %collective-permute-done.11.across = f32[264,128]{1,0:T(8,128)S(1)} collective-permute-done((f32[264,128]{1,0:T(8,128)S(1)}, f32[264,128]{1,0:T(8,128)S(1)}, u32[]{:S(2)}, u32[]{:S(2)}) %collective-permute-start.11) | collective-permute-done | bytes 135200 | tf_op jit(solution)/shard_map/ppermute | solution.py:931
  138.8 5.6 %shard_map.172 = (bf16[2,4,272,128]{3,2,1,0:T(8,128)(2,1)}, bf16[4,272,128]{2,1,0:T(8,128)(2,1)S(1)}) custom-call(s32[7]{0:T(128)S(1)} %stack.53.meta, f32[2,8]{1,0:T(2,128)S(1)} %bitcast.40, bf16[1024,768]{1,0:T(8,128)(2,1)S(1)} %get-tuple-element.21.proj, f32[24,256]{1,0:T(8,128)S(1)} %get-tuple-element.22.vrows, f32[256,128]{1,0:T(8,128)S(1)} %get-tuple-element.23.vcols, ...), custom_call_target="tpu_custom_call" | custom-call | flops 1610612736 | tf_op jit(solution)/shard_map/pallas_call | solution.py:945
  144.4 0.1 collective-permute-start.12
  144.6 0.1 collective-permute-start.15
  144.6 2.6 %collective-permute-start.16 = (bf16[128,1024]{1,0:T(8,128)(2,1)S(1)}, bf16[128,1024]{1,0:T(8,128)(2,1)S(1)}, u32[]{:S(2)}, u32[]{:S(2)}) collective-permute-start(bf16[128,1024]{1,0:T(8,128)(2,1)S(1)} %get-tuple-element.30), channel_id=1, source_target_pairs={{0,24},{2,26},{4,28},{6,30},{8,16},{10,18},{12,20},{14,22},{16,8},... | collective-permute-start | bytes 786440 | tf_op jit(solution)/shard_map/ppermute | solution.py:871
  147.3 0.7 bitcast_dynamic-update-slice_fusion
  148.0 3.5 %all-to-all-start.1 = ((bf16[8,272,128]{2,1,0:T(8,128)(2,1)}), bf16[8,272,128]{2,1,0:T(8,128)(2,1)S(1)}, u32[]{:S(2)}, u32[]{:S(2)}) async-start(bf16[8,272,128]{2,1,0:T(8,128)(2,1)} %bitcast.21), calls=%async_computation.1 | async-start | bytes 1114112 | tf_op jit(solution)/shard_map/all_to_all | solution.py:959
  151.6 1.9 collective-permute-start.14
  153.5 12.0 %collective-permute-done.15 = bf16[128,1024]{1,0:T(8,128)(2,1)S(1)} collective-permute-done((bf16[128,1024]{1,0:T(8,128)(2,1)S(1)}, bf16[128,1024]{1,0:T(8,128)(2,1)S(1)}, u32[]{:S(2)}, u32[]{:S(2)}) %collective-permute-start.15) | collective-permute-done | bytes 262176 | tf_op jit(solution)/shard_map/ppermute | solution.py:871
  165.6 0.4 collective-permute-start.20
  166.0 11.0 %collective-permute-done.14 = bf16[128,1024]{1,0:T(8,128)(2,1)S(1)} collective-permute-done((bf16[128,1024]{1,0:T(8,128)(2,1)S(1)}, bf16[128,1024]{1,0:T(8,128)(2,1)S(1)}, u32[]{:S(2)}, u32[]{:S(2)}) %collective-permute-start.14) | collective-permute-done | bytes 262176 | tf_op jit(solution)/shard_map/ppermute | solution.py:871
  177.0 1.4 collective-permute-start.17
  178.4 0.7 collective-permute-start.18
  179.1 0.4 collective-permute-start.19
  179.5 1.5 collective-permute-done.20.refs_5_
  181.0 10.9 %collective-permute-done.17.refs_2_ = bf16[256,1024]{1,0:T(8,128)(2,1)S(1)} collective-permute-done((bf16[256,1024]{1,0:T(8,128)(2,1)S(1)}, bf16[256,1024]{1,0:T(8,128)(2,1)S(1)}, u32[]{:S(2)}, u32[]{:S(2)}) %collective-permute-start.17) | collective-permute-done | bytes 524320 | tf_op jit(solution)/shard_map/ppermute | solution.py:921
  191.9 0.4 collective-permute-start.21
  192.3 10.9 %collective-permute-done.18.refs_3_ = bf16[256,1024]{1,0:T(8,128)(2,1)S(1)} collective-permute-done((bf16[256,1024]{1,0:T(8,128)(2,1)S(1)}, bf16[256,1024]{1,0:T(8,128)(2,1)S(1)}, u32[]{:S(2)}, u32[]{:S(2)}) %collective-permute-start.18) | collective-permute-done | bytes 524320 | tf_op jit(solution)/shard_map/ppermute | solution.py:921
  203.1 10.3 %collective-permute-done.22.refs_7_ = bf16[256,1024]{1,0:T(8,128)(2,1)S(1)} collective-permute-done((bf16[256,1024]{1,0:T(8,128)(2,1)S(1)}, bf16[256,1024]{1,0:T(8,128)(2,1)S(1)}, u32[]{:S(2)}, u32[]{:S(2)}) %collective-permute-start.22) | collective-permute-done | bytes 524320 | tf_op jit(solution)/shard_map/ppermute | solution.py:921
  213.4 9.1 %shard_map.173 = (bf16[256,1024]{1,0:T(8,128)(2,1)}, f32[8,256]{1,0:T(8,128)}) custom-call(s32[7]{0:T(128)S(1)} %stack.53.meta, bf16[8,272,128]{2,1,0:T(8,128)(2,1)S(1)} %all-to-all-done.1.own, bf16[8,272,128]{2,1,0:T(8,128)(2,1)S(1)} %bitcast.37, bf16[256,1024]{1,0:T(8,128)(2,1)S(1)} %constant_dynamic-update-slice_fusion.2.refs_0_, ...), custom_call_target="tpu_custom_call" | custom-call | flops 1073741824 | tf_op jit(solution)/shard_map/pallas_call | solution.py:970
  (46 shorter events, 0.3 us)
Async XLA Ops:
  2.5 0.9 copy-start
  3.4 0.9 copy-start.1
  4.3 0.9 copy-start.2
  5.2 0.9 copy-start.3
  6.1 0.9 copy-start.4
  7.0 0.8 copy-start.5
  7.8 0.8 copy-start.6
  10.6 1.9 collective-permute-start.8
  12.4 9.4 %copy-start.7 = (bf16[256,2048]{1,0:T(8,128)(2,1)S(1)}, bf16[256,2048]{1,0:T(8,128)(2,1)}, u32[]{:S(2)}) copy-start(bf16[256,2048]{1,0:T(8,128)(2,1)} %param.16) | copy-start | bytes 3145732
  13.5 43.1 %copy-start.10 = (f32[2048]{0:T(1024)S(1)}, f32[2048]{0:T(1024)}, u32[]{:S(2)}) copy-start(f32[2048]{0:T(1024)} %param.17) | copy-start | bytes 24580
  13.5 43.1 %all-to-all-start = ((bf16[16,392,128]{2,1,0:T(8,128)(2,1)}), bf16[16,392,128]{2,1,0:T(8,128)(2,1)S(1)}, u32[]{:S(2)}, u32[]{:S(2)}) async-start(bf16[16,392,128]{2,1,0:T(8,128)(2,1)} %bitcast.17), calls=%async_computation | async-start | bytes 3211264 | tf_op jit(solution)/shard_map/all_to_all | solution.py:861
  21.8 47.1 %copy-start.11 = (f32[4,4]{1,0:T(4,128)S(1)}, f32[4,4]{1,0:T(4,128)}, u32[]{:S(2)}) copy-start(f32[4,4]{1,0:T(4,128)} %param.23) | copy-start | bytes 196
  21.8 47.1 %copy-start.12 = (f32[512]{0:T(512)S(1)}, f32[512]{0:T(512)}, u32[]{:S(2)}) copy-start(f32[512]{0:T(512)} %param.25) | copy-start | bytes 6148
  21.9 47.1 %copy-start.13 = (f32[8]{0:T(128)S(1)}, f32[8]{0:T(128)}, u32[]{:S(2)}) copy-start(f32[8]{0:T(128)} %param.29) | copy-start | bytes 100
  56.6 27.7 %collective-permute-start.9 = (bf16[6272,128]{1,0:T(8,128)(2,1)S(1)}, bf16[6272,128]{1,0:T(8,128)(2,1)}, u32[]{:S(2)}, u32[]{:S(2)}) collective-permute-start(bf16[6272,128]{1,0:T(8,128)(2,1)S(1)} %bitcast.35), channel_id=1, source_target_pairs={{0,1},{1,0},{2,3},{3,2},{4,5},{5,4},{6,7},{7,6},{8,9},{9,8},{10,11... | collective-permute-start | bytes 4816904 | tf_op jit(solution)/shard_map/ppermute | solution.py:824
  58.2 19.1 %collective-permute-start.4 = (bf16[256,2048]{1,0:T(8,128)(2,1)S(1)}, bf16[256,2048]{1,0:T(8,128)(2,1)}, u32[]{:S(2)}, u32[]{:S(2)}) collective-permute-start(bf16[256,2048]{1,0:T(8,128)(2,1)S(1)} %fusion.2.refs_0_), channel_id=1, source_target_pairs={{0,8},{2,10},{4,12},{6,14},{9,1},{11,3},{13,5},{15,7},{16,24},{18,... | collective-permute-start | bytes 3145736 | tf_op jit(solution)/shard_map/ppermute | solution.py:832
  65.9 17.6 %collective-permute-start.1 = (bf16[256,2048]{1,0:T(8,128)(2,1)S(1)}, bf16[256,2048]{1,0:T(8,128)(2,1)}, u32[]{:S(2)}, u32[]{:S(2)}) collective-permute-start(bf16[256,2048]{1,0:T(8,128)(2,1)S(1)} %fusion.2.refs_0_), channel_id=1, source_target_pairs={{0,2},{2,0},{4,6},{6,4},{9,11},{11,9},{13,15},{15,13},{16,18},{18,... | collective-permute-start | bytes 3145736 | tf_op jit(solution)/shard_map/ppermute | solution.py:838
  69.1 3.7 %collective-permute-start = (f32[5,128]{1,0:T(8,128)S(1)}, f32[5,128]{1,0:T(8,128)S(1)}, u32[]{:S(2)}, u32[]{:S(2)}) collective-permute-start(f32[5,128]{1,0:T(8,128)S(1)} %get-tuple-element.38), channel_id=1, source_target_pairs={{0,1},{1,0},{2,3},{3,2},{4,5},{5,4},{6,7},{7,6},{8,9},{9,8},{10,11... | collective-permute-start | bytes 7688 | tf_op jit(solution)/shard_map/ppermute | solution.py:824
  69.1 22.0 %collective-permute-start.2 = (bf16[256,2048]{1,0:T(8,128)(2,1)S(1)}, bf16[256,2048]{1,0:T(8,128)(2,1)S(1)}, u32[]{:S(2)}, u32[]{:S(2)}) collective-permute-start(bf16[256,2048]{1,0:T(8,128)(2,1)S(1)} %fusion.2.refs_0_), channel_id=1, source_target_pairs={{0,4},{2,6},{4,0},{6,2},{9,13},{11,15},{13,9},{15,11},{16,20},{18,... | collective-permute-start | bytes 3145736 | tf_op jit(solution)/shard_map/ppermute | solution.py:838
  72.8 34.4 %collective-permute-start.3 = (bf16[256,2048]{1,0:T(8,128)(2,1)S(1)}, bf16[256,2048]{1,0:T(8,128)(2,1)S(1)}, u32[]{:S(2)}, u32[]{:S(2)}) collective-permute-start(bf16[256,2048]{1,0:T(8,128)(2,1)S(1)} %fusion.2.refs_0_), channel_id=1, source_target_pairs={{0,6},{2,4},{4,2},{6,0},{9,15},{11,13},{13,11},{15,9},{16,22},{18,... | collective-permute-start | bytes 3145736 | tf_op jit(solution)/shard_map/ppermute | solution.py:838
  77.2 29.9 %collective-permute-start.5 = (bf16[256,2048]{1,0:T(8,128)(2,1)}, bf16[256,2048]{1,0:T(8,128)(2,1)S(1)}, u32[]{:S(2)}, u32[]{:S(2)}) collective-permute-start(bf16[256,2048]{1,0:T(8,128)(2,1)} %collective-permute-done.4.refs_4_), channel_id=1, source_target_pairs={{1,3},{3,1},{5,7},{7,5},{8,10},{10,8},{12,14},{14,12},{17,19},{19,... | collective-permute-start | bytes 3145736 | tf_op jit(solution)/shard_map/ppermute | solution.py:864
  83.6 23.6 %collective-permute-start.6 = (bf16[256,2048]{1,0:T(8,128)(2,1)}, bf16[256,2048]{1,0:T(8,128)(2,1)S(1)}, u32[]{:S(2)}, u32[]{:S(2)}) collective-permute-start(bf16[256,2048]{1,0:T(8,128)(2,1)} %collective-permute-done.4.refs_4_), channel_id=1, source_target_pairs={{1,5},{3,7},{5,1},{7,3},{8,12},{10,14},{12,8},{14,10},{17,21},{19,... | collective-permute-start | bytes 3145736 | tf_op jit(solution)/shard_map/ppermute | solution.py:864
  84.3 22.9 %collective-permute-start.7 = (bf16[256,2048]{1,0:T(8,128)(2,1)}, bf16[256,2048]{1,0:T(8,128)(2,1)S(1)}, u32[]{:S(2)}, u32[]{:S(2)}) collective-permute-start(bf16[256,2048]{1,0:T(8,128)(2,1)} %collective-permute-done.4.refs_4_), channel_id=1, source_target_pairs={{1,7},{3,5},{5,3},{7,1},{8,14},{10,12},{12,10},{14,8},{17,23},{19,... | collective-permute-start | bytes 3145736 | tf_op jit(solution)/shard_map/ppermute | solution.py:864
  115.2 14.4 %collective-permute-start.10 = (f32[2,264,128]{2,1,0:T(8,128)S(1)}, f32[2,264,128]{2,1,0:T(8,128)S(1)}, u32[]{:S(2)}, u32[]{:S(2)}) collective-permute-start(f32[2,264,128]{2,1,0:T(8,128)S(1)} %get-tuple-element.25.own), channel_id=1, source_target_pairs={{0,1},{1,0},{2,3},{3,2},{4,5},{5,4},{6,7},{7,6},{8,9},{9,8},{10,11... | collective-permute-start | bytes 811016 | tf_op jit(solution)/shard_map/ppermute | solution.py:824
  130.2 8.6 %collective-permute-start.11 = (f32[264,128]{1,0:T(8,128)S(1)}, f32[264,128]{1,0:T(8,128)S(1)}, u32[]{:S(2)}, u32[]{:S(2)}) collective-permute-start(f32[264,128]{1,0:T(8,128)S(1)} %shard_map.170), channel_id=1, source_target_pairs={{0,16},{2,18},{4,20},{6,22},{8,24},{10,26},{12,28},{14,30},{16,0},... | collective-permute-start | bytes 405512 | tf_op jit(solution)/shard_map/ppermute | solution.py:931
  138.8 5.7 %copy-start.8 = (bf16[64,1024]{1,0:T(8,128)(2,1)S(1)}, bf16[64,1024]{1,0:T(8,128)(2,1)}, u32[]{:S(2)}) copy-start(bf16[64,1024]{1,0:T(8,128)(2,1)} %param.30) | copy-start | bytes 393220
  138.8 5.7 %copy-start.9 = (bf16[64,1024]{1,0:T(8,128)(2,1)S(1)}, bf16[64,1024]{1,0:T(8,128)(2,1)}, u32[]{:S(2)}) copy-start(bf16[64,1024]{1,0:T(8,128)(2,1)} %param.31) | copy-start | bytes 393220
  144.4 2.9 %collective-permute-start.12 = (bf16[4,272,128]{2,1,0:T(8,128)(2,1)S(1)}, bf16[4,272,128]{2,1,0:T(8,128)(2,1)S(1)}, u32[]{:S(2)}, u32[]{:S(2)}) collective-permute-start(bf16[4,272,128]{2,1,0:T(8,128)(2,1)S(1)} %get-tuple-element.29), channel_id=1, source_target_pairs={{0,1},{1,0},{2,3},{3,2},{4,5},{5,4},{6,7},{7,6},{8,9},{9,8},{10,11... | collective-permute-start | bytes 835592 | tf_op jit(solution)/shard_map/ppermute | solution.py:824
  144.6 21.0 %collective-permute-start.15 = (bf16[128,1024]{1,0:T(8,128)(2,1)S(1)}, bf16[128,1024]{1,0:T(8,128)(2,1)S(1)}, u32[]{:S(2)}, u32[]{:S(2)}) collective-permute-start(bf16[128,1024]{1,0:T(8,128)(2,1)S(1)} %get-tuple-element.30), channel_id=1, source_target_pairs={{0,16},{2,18},{4,20},{6,22},{8,24},{10,26},{12,28},{14,30},{16,0},... | collective-permute-start | bytes 786440 | tf_op jit(solution)/shard_map/ppermute | solution.py:871
  144.6 20.9 %collective-permute-start.16 = (bf16[128,1024]{1,0:T(8,128)(2,1)S(1)}, bf16[128,1024]{1,0:T(8,128)(2,1)S(1)}, u32[]{:S(2)}, u32[]{:S(2)}) collective-permute-start(bf16[128,1024]{1,0:T(8,128)(2,1)S(1)} %get-tuple-element.30), channel_id=1, source_target_pairs={{0,24},{2,26},{4,28},{6,30},{8,16},{10,18},{12,20},{14,22},{16,8},... | collective-permute-start | bytes 786440 | tf_op jit(solution)/shard_map/ppermute | solution.py:871
  148.0 30.4 %all-to-all-start.1 = ((bf16[8,272,128]{2,1,0:T(8,128)(2,1)}), bf16[8,272,128]{2,1,0:T(8,128)(2,1)S(1)}, u32[]{:S(2)}, u32[]{:S(2)}) async-start(bf16[8,272,128]{2,1,0:T(8,128)(2,1)} %bitcast.21), calls=%async_computation.1 | async-start | bytes 1114112 | tf_op jit(solution)/shard_map/all_to_all | solution.py:959
  151.6 25.4 %collective-permute-start.14 = (bf16[128,1024]{1,0:T(8,128)(2,1)S(1)}, bf16[128,1024]{1,0:T(8,128)(2,1)S(1)}, u32[]{:S(2)}, u32[]{:S(2)}) collective-permute-start(bf16[128,1024]{1,0:T(8,128)(2,1)S(1)} %get-tuple-element.30), channel_id=1, source_target_pairs={{0,8},{2,10},{4,12},{6,14},{8,0},{10,2},{12,4},{14,6},{16,24},{18,... | collective-permute-start | bytes 786440 | tf_op jit(solution)/shard_map/ppermute | solution.py:871
  165.6 15.3 %collective-permute-start.20 = (bf16[256,1024]{1,0:T(8,128)(2,1)S(1)}, bf16[256,1024]{1,0:T(8,128)(2,1)S(1)}, u32[]{:S(2)}, u32[]{:S(2)}) collective-permute-start(bf16[256,1024]{1,0:T(8,128)(2,1)S(1)} %constant_dynamic-update-slice_fusion.5.refs_1_), channel_id=1, source_target_pairs={{0,4},{2,6},{4,0},{6,2},{8,12},{10,14},{12,8},{14,10},{16,20},{18,... | collective-permute-start | bytes 1572872 | tf_op jit(solution)/shard_map/ppermute | solution.py:921
  177.0 14.9 %collective-permute-start.17 = (bf16[256,1024]{1,0:T(8,128)(2,1)S(1)}, bf16[256,1024]{1,0:T(8,128)(2,1)S(1)}, u32[]{:S(2)}, u32[]{:S(2)}) collective-permute-start(bf16[256,1024]{1,0:T(8,128)(2,1)S(1)} %constant_dynamic-update-slice_fusion.2.refs_0_), channel_id=1, source_target_pairs={{0,2},{2,0},{4,6},{6,4},{8,10},{10,8},{12,14},{14,12},{16,18},{18,... | collective-permute-start | bytes 1572872 | tf_op jit(solution)/shard_map/ppermute | solution.py:921
  178.4 35.0 %collective-permute-start.13 = (bf16[2176,128]{1,0:T(8,128)(2,1)S(1)}, bf16[2176,128]{1,0:T(8,128)(2,1)S(1)}, u32[]{:S(2)}, u32[]{:S(2)}) collective-permute-start(bf16[2176,128]{1,0:T(8,128)(2,1)S(1)} %bitcast.36), channel_id=1, source_target_pairs={{0,1},{1,0},{2,3},{3,2},{4,5},{5,4},{6,7},{7,6},{8,9},{9,8},{10,11... | collective-permute-start | bytes 1671176 | tf_op jit(solution)/shard_map/ppermute | solution.py:824
  178.4 24.7 %collective-permute-start.18 = (bf16[256,1024]{1,0:T(8,128)(2,1)S(1)}, bf16[256,1024]{1,0:T(8,128)(2,1)S(1)}, u32[]{:S(2)}, u32[]{:S(2)}) collective-permute-start(bf16[256,1024]{1,0:T(8,128)(2,1)S(1)} %constant_dynamic-update-slice_fusion.5.refs_1_), channel_id=1, source_target_pairs={{0,2},{2,0},{4,6},{6,4},{8,10},{10,8},{12,14},{14,12},{16,18},{18,... | collective-permute-start | bytes 1572872 | tf_op jit(solution)/shard_map/ppermute | solution.py:921
  179.1 24.0 %collective-permute-start.19 = (bf16[256,1024]{1,0:T(8,128)(2,1)S(1)}, bf16[256,1024]{1,0:T(8,128)(2,1)S(1)}, u32[]{:S(2)}, u32[]{:S(2)}) collective-permute-start(bf16[256,1024]{1,0:T(8,128)(2,1)S(1)} %constant_dynamic-update-slice_fusion.2.refs_0_), channel_id=1, source_target_pairs={{0,4},{2,6},{4,0},{6,2},{8,12},{10,14},{12,8},{14,10},{16,20},{18,... | collective-permute-start | bytes 1572872 | tf_op jit(solution)/shard_map/ppermute | solution.py:921
  181.0 32.5 %collective-permute-start.22 = (bf16[256,1024]{1,0:T(8,128)(2,1)S(1)}, bf16[256,1024]{1,0:T(8,128)(2,1)S(1)}, u32[]{:S(2)}, u32[]{:S(2)}) collective-permute-start(bf16[256,1024]{1,0:T(8,128)(2,1)S(1)} %collective-permute-done.20.refs_5_), channel_id=1, source_target_pairs={{0,2},{2,0},{4,6},{6,4},{8,10},{10,8},{12,14},{14,12},{16,18},{18,... | collective-permute-start | bytes 1572872 | tf_op jit(solution)/shard_map/ppermute | solution.py:921
  191.9 21.6 %collective-permute-start.21 = (bf16[256,1024]{1,0:T(8,128)(2,1)S(1)}, bf16[256,1024]{1,0:T(8,128)(2,1)S(1)}, u32[]{:S(2)}, u32[]{:S(2)}) collective-permute-start(bf16[256,1024]{1,0:T(8,128)(2,1)S(1)} %collective-permute-done.17.refs_2_), channel_id=1, source_target_pairs={{0,4},{2,6},{4,0},{6,2},{8,12},{10,14},{12,8},{14,10},{16,20},{18,... | collective-permute-start | bytes 1572872 | tf_op jit(solution)/shard_map/ppermute | solution.py:921

commit v5 on v4

--- a/solution.py
+++ b/solution.py
@@ -367,8 +367,18 @@
     return [pltpu.with_memory_space_constraint(x, pltpu.VMEM) for x in arrays]
 
 
-def pack_kernel(meta, mq, mk, mv, mo, aq, ak, av, small, keep, send):
+def pack_kernel(meta, *refs):
+    sources, small, keep, send = refs[:7], refs[7], refs[8], refs[9]
+    held, sems = refs[10:17], refs[17]
     t = meta[0]
+    fetches = [
+        pltpu.make_async_copy(a, b, sems.at[i]) for i, (a, b) in enumerate(zip(sources, held))
+    ]
+    for fetch in fetches:
+        fetch.start()
+    for fetch in fetches:
+        fetch.wait()
+    mq, mk, mv, mo, aq, ak, av = held
     copies, heads = keep.shape[0], keep.shape[2]
     rows = mq.shape[0] // 2
     at = pl.multiple_of(t * rows, rows)
@@ -737,38 +747,25 @@
 
 
 def output_kernel(meta, own, partner, *refs):
-    mixed, log_total, left, weight, sems = refs[-5:]
-    blocks = refs[:-5]
+    mixed, log_total, left, weight = refs[-4:]
+    blocks = refs[:-4]
     t, p, z = meta[0], meta[1], meta[6]
     plane = len(blocks) // 2
     heads, tok = own.shape[0], mixed.shape[0]
-    planes = sems.shape[0] // plane
-    rows = 2 * blocks[0].shape[0] // planes
+    total = weight.shape[0] // 2
+    rows = 2 * total // (2 * heads)
     half = rows // 2
-    total = weight.shape[0] // 2
-    copies = []
     for r in range(plane):
-        for zr in range(planes):
+        for zr in range(2 * heads // plane):
             source = (z ^ zr) * plane + (p ^ r)
             for i in range(2):
                 to = pl.multiple_of(i * total + source * half, half)
-                copies.append(
-                    pltpu.make_async_copy(
-                        blocks[2 * r + 2 * zr // planes].at[
-                            pl.ds(zr % (planes // 2) * rows + i * half, half)
-                        ],
-                        weight.at[pl.ds(to, half)],
-                        sems.at[r * planes + zr, i],
-                    )
-                )
-    for copy in copies:
-        copy.start()
+                at = zr // 2 * rows + i * half
+                weight[pl.ds(to, half), :] = blocks[2 * r + zr % 2][at : at + half, :]
     for j in range(heads):
         left[t * heads + j] = own[j, :tok, :]
         left[(1 - t) * heads + j] = partner[j, :tok, :]
     lhs = jnp.concatenate([left[i] for i in range(2 * heads)], axis=1)
-    for copy in copies:
-        copy.wait()
     mixed[...] = mm(lhs, weight[...]).astype(jnp.bfloat16)
     per = tok // LANES
     n = 2 * per
@@ -846,15 +843,19 @@
     )
     small = jnp.concatenate([gate_rows, decay_rows], axis=2)
     n_rows = 6 * half + small.shape[2]
+    projections = (mq_weight, mk_weight, mv_weight, mo_weight, aq_weight, ak_weight, av_weight)
     spread, send = vmem_call(
         pack_kernel,
         (
             jax.ShapeDtypeStruct((2, 2, lh, n_rows, LANES), bf16),
             jax.ShapeDtypeStruct((lh, n_rows, LANES), bf16),
         ),
+        scratch=[pltpu.VMEM(w.shape, bf16) for w in projections]
+        + [pltpu.SemaphoreType.DMA((len(projections),))],
         smem=1,
-        n_in=8,
-    )(meta, mq_weight, mk_weight, mv_weight, mo_weight, aq_weight, ak_weight, av_weight, small)
+        n_any=7,
+        n_tail=1,
+    )(meta, *projections, small)
     got = flip(send)
     got = jnp.broadcast_to(got[None, None], (2, 1) + got.shape)
     spread = lax.dynamic_update_slice_in_dim(spread, got, 1 - t, 1)
@@ -866,9 +867,9 @@
             )
         )
     out_block = jnp.concatenate([out_m_weight, out_a_weight], axis=0)
-    column = [out_block]
-    for r in range(1, sp // plane):
-        column.append(lax.ppermute(out_block, "sp", [(a, a ^ (r * plane)) for a in range(sp)]))
+    out_next = lax.ppermute(out_block, "sp", [(a, (a + group) % sp) for a in range(sp)])
+    upper = jnp.concatenate([out_block, out_next], axis=0)
+    lower = lax.ppermute(upper, "sp", [(a, a ^ plane) for a in range(sp)])
     partner_w = flip(own_w)
     params = jnp.concatenate(
         [m_gain, gate_bias.reshape(-1), sink_logit, jnp.zeros((LANES - 6 * lh,), f32)]
@@ -913,9 +914,6 @@
         keep=True,
         flops=2 * quarter * width * cols,
     )(meta, bias, *same_xs, *other_xs, *near(woven, gate_t, decay))
-    column = jnp.concatenate(column, axis=0)
-    cut = column.shape[0] // 2
-    upper, lower = column[:cut], column[cut:]
 
     def hop(x, r):
         return lax.ppermute(x, "sp", [(a, a ^ r) for a in range(sp)])
@@ -976,13 +974,11 @@
         scratch=[
             pltpu.VMEM((2 * group, tok, LANES), bf16),
             pltpu.VMEM((inner, out_m_weight.shape[1]), bf16),
-            pltpu.SemaphoreType.DMA((sp, 2)),
         ],
         smem=1,
-        n_in=2,
-        n_any=2 * plane,
+        n_in=2 + 2 * plane,
         flops=2 * tok * inner * out_m_weight.shape[1],
-    )(meta, *near(mine.reshape(shape), theirs.reshape(shape)), *out_blocks)
+    )(meta, *near(mine.reshape(shape), theirs.reshape(shape), *out_blocks))
 
 
 def solution(mesh):

time: 223 us -> 212 us (0.951)
  waiting for transfers between devices: 126 us -> 118 us
  Pallas kernels: 30.4 us -> 25.3 us
    ppermute x3 -> x2, waiting for transfers between devices: 23 us -> 7.2 us  [the longest x1 7.2 us: on_device_split(): lower = lax.ppermute(upper, 'sp', [(a, a ^ plane) for a in range(sp)])]
    ppermute x1, waiting for transfers between devices: 4.5 us -> 13 us  [on_device_split(): lax.ppermute(sent, 'sp', [(a, (a + group) % sp) for a in range(sp)])]
    pallas_call x1, Pallas kernels: 9.08 us -> 2.91 us  [on_device_split(): vmem_call(output_kernel, (jax.ShapeDtypeStruct((tok, out_m_weight.shape[1...]
    ppermute x6, waiting for transfers between devices: 33.6 us -> 29 us  [hop(): return lax.ppermute(x, 'sp', [(a, a ^ r) for a in range(sp)])]
    all_to_all x1, waiting for transfers between devices: 0.01 us -> 4.3 us  [on_device_split(): lax.all_to_all(spread.reshape(group * (tok + 16), LANES), 'sp', 0, 0, axi...]
    ppermute x3 -> x2, starting transfers between devices: 4.65 us -> 1.06 us  [the longest x1 0.99 us: on_device_split(): lax.ppermute(out_block, 'sp', [(a, (a + group) % sp) for a in range(sp)])]
    ppermute x6, starting transfers between devices: 3.22 us -> 6.73 us  [hop(): return lax.ppermute(x, 'sp', [(a, a ^ r) for a in range(sp)])]
  transfers between devices with their start and end apart: 25 -> 24, of which waited for: 14 -> 15; matrix products, arithmetic and copies ran while one was open for 1% -> 1% of each run, Pallas kernels for 2% -> 5%
where the time goes in v5:
time: 212 us; the launch traced here: 211 us
  waiting for transfers between devices  118 us (56%)
  starting transfers between devices  54.6 us (26%)
  Pallas kernels  25.3 us (12%)
  local copies, waits for them, and re-layouts  9.13 us (4%)
  other arithmetic  2.74 us (1%)
    all_to_all x1, waiting for transfers between devices, on_device_split(): lax.all_to_all(spread.reshape(sp * n_rows, LANES), 'sp', 0, 0, tiled=True)  34.4 us
    ppermute x6, waiting for transfers between devices, hop(): return lax.ppermute(x, 'sp', [(a, a ^ r) for a in range(sp)])  29 us
    ppermute x3, waiting for transfers between devices, on_device_split(): lax.ppermute(normed, both_axes, [(core(a, True), core(a ^ r, True)) for a...  25.6 us
    ppermute x6, starting transfers between devices, flip(): return lax.ppermute(x, 'tp', swap)  13.8 us
    ppermute x1, waiting for transfers between devices, on_device_split(): lax.ppermute(sent, 'sp', [(a, (a + group) % sp) for a in range(sp)])  13 us
    ppermute x3, starting transfers between devices, on_device_split(): lax.ppermute(normed, both_axes, [(core(a, True), core(a ^ r, True)) for a...  9.2 us
    all_to_all x1, starting transfers between devices, on_device_split(): lax.all_to_all(spread.reshape(sp * n_rows, LANES), 'sp', 0, 0, tiled=True)  8.35 us
    pallas_call x1, Pallas kernels, on_device_split(): vmem_call(project_kernel, (jax.ShapeDtypeStruct((quarter, cols), bf16), j...  8.01 us
  transfers between devices with their start and end apart: 24, of which 15 were waited for; matrix products, arithmetic and copies ran while one was open for 1% of the time, Pallas kernels for 5%

profile of v5, /device:TPU:0, one launch (start us, length us, event | category | flops | bytes accessed | tf_op | source)
XLA Modules:
  0.0 211.1 jit_solution(8272083131346407957)
XLA Ops:
  0.7 0.7 fusion.5
  1.5 0.8 reshape.51
  2.3 0.1 reshape.52
  2.4 0.1 stack.53.meta
  2.5 0.9 copy-done
  3.4 0.9 copy-done.1
  4.3 0.9 copy-done.2
  5.2 0.9 copy-done.3
  6.1 0.9 copy-done.4
  7.0 0.8 copy-done.5
  7.8 0.8 copy-done.6
  8.7 3.0 %shard_map.167 = (bf16[2,2,4,392,128]{4,3,2,1,0:T(8,128)(2,1)}, bf16[4,392,128]{2,1,0:T(8,128)(2,1)S(1)}) custom-call(s32[7]{0:T(128)S(1)} %stack.53.meta, bf16[128,512]{1,0:T(8,128)(2,1)S(1)} %copy-done, bf16[128,512]{1,0:T(8,128)(2,1)S(1)} %copy-done.1, bf16[128,512]{1,0:T(8,128)(2,1)S(1)} %copy-done.2, bf16[128,512]{1,0:T(8,128)(2,1)S(1)} %copy-done.3, ...), custom_call_target="tpu_custom_call" | custom-call | tf_op jit(solution)/shard_map/pallas_call | solution.py:847
  11.6 0.6 collective-permute-start.8
  12.2 1.4 collective-permute-done.8
  13.6 1.0 broadcast_dynamic-update-slice_fusion
  14.6 8.4 %all-to-all-start = ((bf16[16,392,128]{2,1,0:T(8,128)(2,1)}), bf16[16,392,128]{2,1,0:T(8,128)(2,1)S(1)}, u32[]{:S(2)}, u32[]{:S(2)}) async-start(bf16[16,392,128]{2,1,0:T(8,128)(2,1)} %bitcast.17), calls=%async_computation | async-start | bytes 3211264 | tf_op jit(solution)/shard_map/all_to_all | solution.py:862
  23.0 0.0 copy-start.11
  23.0 0.0 copy-start.12
  23.0 0.3 fusion
  23.3 34.4 %all-to-all-done.own = bf16[16,392,128]{2,1,0:T(8,128)(2,1)S(1)} async-done(((bf16[16,392,128]{2,1,0:T(8,128)(2,1)}), bf16[16,392,128]{2,1,0:T(8,128)(2,1)S(1)}, u32[]{:S(2)}, u32[]{:S(2)}) %all-to-all-start) | async-done | bytes 1605664 | tf_op jit(solution)/shard_map/all_to_all | solution.py:862
  57.8 1.5 fusion.2.refs_0_
  59.3 7.8 %collective-permute-start.4 = (bf16[256,2048]{1,0:T(8,128)(2,1)S(1)}, bf16[256,2048]{1,0:T(8,128)(2,1)}, u32[]{:S(2)}, u32[]{:S(2)}) collective-permute-start(bf16[256,2048]{1,0:T(8,128)(2,1)S(1)} %fusion.2.refs_0_), channel_id=1, source_target_pairs={{0,8},{2,10},{4,12},{6,14},{9,1},{11,3},{13,5},{15,7},{16,24},{18,... | collective-permute-start | bytes 3145736 | tf_op jit(solution)/shard_map/ppermute | solution.py:829
  67.1 3.0 %collective-permute-start.1 = (bf16[256,2048]{1,0:T(8,128)(2,1)S(1)}, bf16[256,2048]{1,0:T(8,128)(2,1)}, u32[]{:S(2)}, u32[]{:S(2)}) collective-permute-start(bf16[256,2048]{1,0:T(8,128)(2,1)S(1)} %fusion.2.refs_0_), channel_id=1, source_target_pairs={{0,2},{2,0},{4,6},{6,4},{9,11},{11,9},{13,15},{15,13},{16,18},{18,... | collective-permute-start | bytes 3145736 | tf_op jit(solution)/shard_map/ppermute | solution.py:835
  70.0 0.1 reshape.49
  70.1 0.1 fusion.8
  70.2 0.0 collective-permute-start
  70.2 3.6 %collective-permute-start.2 = (bf16[256,2048]{1,0:T(8,128)(2,1)S(1)}, bf16[256,2048]{1,0:T(8,128)(2,1)S(1)}, u32[]{:S(2)}, u32[]{:S(2)}) collective-permute-start(bf16[256,2048]{1,0:T(8,128)(2,1)S(1)} %fusion.2.refs_0_), channel_id=1, source_target_pairs={{0,4},{2,6},{4,0},{6,2},{9,13},{11,15},{13,9},{15,11},{16,20},{18,... | collective-permute-start | bytes 3145736 | tf_op jit(solution)/shard_map/ppermute | solution.py:835
  73.9 2.6 %collective-permute-start.3 = (bf16[256,2048]{1,0:T(8,128)(2,1)S(1)}, bf16[256,2048]{1,0:T(8,128)(2,1)S(1)}, u32[]{:S(2)}, u32[]{:S(2)}) collective-permute-start(bf16[256,2048]{1,0:T(8,128)(2,1)S(1)} %fusion.2.refs_0_), channel_id=1, source_target_pairs={{0,6},{2,4},{4,2},{6,0},{9,15},{11,13},{13,11},{15,9},{16,22},{18,... | collective-permute-start | bytes 3145736 | tf_op jit(solution)/shard_map/ppermute | solution.py:835
  76.5 1.9 collective-permute-done.4.refs_4_
  78.4 0.7 collective-permute-start.5
  79.1 5.6 %collective-permute-done.1.refs_1_ = bf16[256,2048]{1,0:T(8,128)(2,1)} collective-permute-done((bf16[256,2048]{1,0:T(8,128)(2,1)S(1)}, bf16[256,2048]{1,0:T(8,128)(2,1)}, u32[]{:S(2)}, u32[]{:S(2)}) %collective-permute-start.1) | collective-permute-done | bytes 1048608 | tf_op jit(solution)/shard_map/ppermute | solution.py:835
  84.7 0.7 collective-permute-start.6
  85.4 0.7 collective-permute-start.7
  86.1 2.0 shard_map.168
  88.2 4.1 %collective-permute-done.2.refs_2_ = bf16[256,2048]{1,0:T(8,128)(2,1)S(1)} collective-permute-done((bf16[256,2048]{1,0:T(8,128)(2,1)S(1)}, bf16[256,2048]{1,0:T(8,128)(2,1)S(1)}, u32[]{:S(2)}, u32[]{:S(2)}) %collective-permute-start.2) | collective-permute-done | bytes 1048608 | tf_op jit(solution)/shard_map/ppermute | solution.py:835
  92.2 16.0 %collective-permute-done.3.refs_3_ = bf16[256,2048]{1,0:T(8,128)(2,1)S(1)} collective-permute-done((bf16[256,2048]{1,0:T(8,128)(2,1)S(1)}, bf16[256,2048]{1,0:T(8,128)(2,1)S(1)}, u32[]{:S(2)}, u32[]{:S(2)}) %collective-permute-start.3) | collective-permute-done | bytes 1048608 | tf_op jit(solution)/shard_map/ppermute | solution.py:835
  108.3 0.0 copy-start.8
  108.3 8.0 %shard_map.169 = (bf16[1024,768]{1,0:T(8,128)(2,1)S(1)}, f32[24,256]{1,0:T(8,128)S(1)}, f32[256,128]{1,0:T(8,128)S(1)}, f32[2,4,128,256]{3,2,1,0:T(8,128)S(1)}, f32[2,264,128]{2,1,0:T(8,128)S(1)}) custom-call(s32[7]{0:T(128)S(1)} %stack.53.meta, f32[2,16]{1,0:T(2,128)S(1)} %bitcast.38, bf16[256,2048]{1,0:T(8,128)(2,1)S(1)} %fusion.2.refs_0_, ...), custom_call_target="tpu_custom_call" | custom-call | flops 3221225472 | tf_op jit(solution)/shard_map/pallas_call | solution.py:897
  116.3 13.2 %collective-permute-start.10 = (f32[2,264,128]{2,1,0:T(8,128)S(1)}, f32[2,264,128]{2,1,0:T(8,128)S(1)}, u32[]{:S(2)}, u32[]{:S(2)}) collective-permute-start(f32[2,264,128]{2,1,0:T(8,128)S(1)} %get-tuple-element.25.own), channel_id=1, source_target_pairs={{0,1},{1,0},{2,3},{3,2},{4,5},{5,4},{6,7},{7,6},{8,9},{9,8},{10,11... | collective-permute-start | bytes 811016 | tf_op jit(solution)/shard_map/ppermute | solution.py:821
  129.6 1.0 collective-permute-start.14
  130.6 0.1 pad_maximum_fusion.5
  130.6 0.1 collective-permute-done.10.partner
  130.7 0.6 shard_map.170
  131.3 2.0 collective-permute-start.11
  133.3 3.1 %shard_map.171 = (bf16[8,128,128]{2,1,0:T(8,128)(2,1)S(1)}, f32[8,8,128]{2,1,0:T(8,128)S(1)}) custom-call(s32[7]{0:T(128)S(1)} %stack.53.meta, f32[2,8]{1,0:T(2,128)S(1)} %bitcast.39, bf16[1024,768]{1,0:T(8,128)(2,1)S(1)} %get-tuple-element.21.proj, f32[2,264,128]{2,1,0:T(8,128)S(1)} %collective-permute-done.10.partner), custom_call_target="tpu_custom_call" | custom-call | flops 1610612736 | tf_op jit(solution)/shard_map/pallas_call | solution.py:931
  136.5 13.0 %collective-permute-done.11.across = f32[264,128]{1,0:T(8,128)S(1)} collective-permute-done((f32[264,128]{1,0:T(8,128)S(1)}, f32[264,128]{1,0:T(8,128)S(1)}, u32[]{:S(2)}, u32[]{:S(2)}) %collective-permute-start.11) | collective-permute-done | bytes 135200 | tf_op jit(solution)/shard_map/ppermute | solution.py:929
  149.5 5.6 %shard_map.172 = (bf16[2,4,272,128]{3,2,1,0:T(8,128)(2,1)}, bf16[4,272,128]{2,1,0:T(8,128)(2,1)S(1)}) custom-call(s32[7]{0:T(128)S(1)} %stack.53.meta, f32[2,8]{1,0:T(2,128)S(1)} %bitcast.40, bf16[1024,768]{1,0:T(8,128)(2,1)S(1)} %get-tuple-element.21.proj, f32[24,256]{1,0:T(8,128)S(1)} %get-tuple-element.22.vrows, f32[256,128]{1,0:T(8,128)S(1)} %get-tuple-element.23.vcols, ...), custom_call_target="tpu_custom_call" | custom-call | flops 1610612736 | tf_op jit(solution)/shard_map/pallas_call | solution.py:943
  155.1 0.0 collective-permute-start.12
  155.2 0.1 collective-permute-start.15
  155.2 1.4 collective-permute-done.12
  156.6 0.7 bitcast_dynamic-update-slice_fusion
  157.4 3.5 %all-to-all-start.1 = ((bf16[8,272,128]{2,1,0:T(8,128)(2,1)}), bf16[8,272,128]{2,1,0:T(8,128)(2,1)S(1)}, u32[]{:S(2)}, u32[]{:S(2)}) async-start(bf16[8,272,128]{2,1,0:T(8,128)(2,1)} %bitcast.21), calls=%async_computation.1 | async-start | bytes 1114112 | tf_op jit(solution)/shard_map/all_to_all | solution.py:957
  160.9 1.9 collective-permute-start.16
  162.8 7.2 %collective-permute-done.15.refs_1_ = bf16[256,1024]{1,0:T(8,128)(2,1)S(1)} collective-permute-done((bf16[256,1024]{1,0:T(8,128)(2,1)S(1)}, bf16[256,1024]{1,0:T(8,128)(2,1)S(1)}, u32[]{:S(2)}, u32[]{:S(2)}) %collective-permute-start.15) | collective-permute-done | bytes 524320 | tf_op jit(solution)/shard_map/ppermute | solution.py:872
  170.0 1.2 collective-permute-start.19
  171.2 4.3 %all-to-all-done.1.own = bf16[8,272,128]{2,1,0:T(8,128)(2,1)S(1)} async-done(((bf16[8,272,128]{2,1,0:T(8,128)(2,1)}), bf16[8,272,128]{2,1,0:T(8,128)(2,1)S(1)}, u32[]{:S(2)}, u32[]{:S(2)}) %all-to-all-start.1) | async-done | bytes 557088 | tf_op jit(solution)/shard_map/all_to_all | solution.py:957
  175.5 1.2 collective-permute-start.18
  176.7 0.9 collective-permute-start.17
  177.7 4.1 %collective-permute-done.16.refs_2_ = bf16[256,1024]{1,0:T(8,128)(2,1)S(1)} collective-permute-done((bf16[256,1024]{1,0:T(8,128)(2,1)S(1)}, bf16[256,1024]{1,0:T(8,128)(2,1)S(1)}, u32[]{:S(2)}, u32[]{:S(2)}) %collective-permute-start.16) | collective-permute-done | bytes 524320 | tf_op jit(solution)/shard_map/ppermute | solution.py:919
  181.8 1.5 collective-permute-start.20
  183.2 2.8 %collective-permute-done.19.refs_5_ = bf16[256,1024]{1,0:T(8,128)(2,1)S(1)} collective-permute-done((bf16[256,1024]{1,0:T(8,128)(2,1)S(1)}, bf16[256,1024]{1,0:T(8,128)(2,1)S(1)}, u32[]{:S(2)}, u32[]{:S(2)}) %collective-permute-start.19) | collective-permute-done | bytes 524320 | tf_op jit(solution)/shard_map/ppermute | solution.py:919
  186.1 11.2 %collective-permute-done.18.refs_4_ = bf16[256,1024]{1,0:T(8,128)(2,1)S(1)} collective-permute-done((bf16[256,1024]{1,0:T(8,128)(2,1)S(1)}, bf16[256,1024]{1,0:T(8,128)(2,1)S(1)}, u32[]{:S(2)}, u32[]{:S(2)}) %collective-permute-start.18) | collective-permute-done | bytes 524320 | tf_op jit(solution)/shard_map/ppermute | solution.py:919
  197.3 10.8 %collective-permute-done.20.refs_6_ = bf16[256,1024]{1,0:T(8,128)(2,1)S(1)} collective-permute-done((bf16[256,1024]{1,0:T(8,128)(2,1)S(1)}, bf16[256,1024]{1,0:T(8,128)(2,1)S(1)}, u32[]{:S(2)}, u32[]{:S(2)}) %collective-permute-start.20) | collective-permute-done | bytes 524320 | tf_op jit(solution)/shard_map/ppermute | solution.py:919
  208.2 2.9 %shard_map.173 = (bf16[256,1024]{1,0:T(8,128)(2,1)}, f32[8,256]{1,0:T(8,128)}) custom-call(s32[7]{0:T(128)S(1)} %stack.53.meta, bf16[8,272,128]{2,1,0:T(8,128)(2,1)S(1)} %all-to-all-done.1.own, bf16[8,272,128]{2,1,0:T(8,128)(2,1)S(1)} %bitcast.37, bf16[256,1024]{1,0:T(8,128)(2,1)S(1)} %constant_dynamic-update-slice_fusion.refs_0_, ...), custom_call_target="tpu_custom_call" | custom-call | flops 1073741824 | tf_op jit(solution)/shard_map/pallas_call | solution.py:968
  (43 shorter events, 0.2 us)
Async XLA Ops:
  2.5 0.9 copy-start
  3.4 0.9 copy-start.1
  4.3 0.9 copy-start.2
  5.2 0.9 copy-start.3
  6.1 0.9 copy-start.4
  7.0 0.8 copy-start.5
  7.8 0.8 copy-start.6
  11.6 1.9 collective-permute-start.8
  13.6 9.4 %copy-start.7 = (bf16[256,2048]{1,0:T(8,128)(2,1)S(1)}, bf16[256,2048]{1,0:T(8,128)(2,1)}, u32[]{:S(2)}) copy-start(bf16[256,2048]{1,0:T(8,128)(2,1)} %param.16) | copy-start | bytes 3145732
  14.6 43.1 %copy-start.10 = (f32[2048]{0:T(1024)S(1)}, f32[2048]{0:T(1024)}, u32[]{:S(2)}) copy-start(f32[2048]{0:T(1024)} %param.17) | copy-start | bytes 24580
  14.6 43.1 %all-to-all-start = ((bf16[16,392,128]{2,1,0:T(8,128)(2,1)}), bf16[16,392,128]{2,1,0:T(8,128)(2,1)S(1)}, u32[]{:S(2)}, u32[]{:S(2)}) async-start(bf16[16,392,128]{2,1,0:T(8,128)(2,1)} %bitcast.17), calls=%async_computation | async-start | bytes 3211264 | tf_op jit(solution)/shard_map/all_to_all | solution.py:862
  23.0 47.1 %copy-start.11 = (f32[4,4]{1,0:T(4,128)S(1)}, f32[4,4]{1,0:T(4,128)}, u32[]{:S(2)}) copy-start(f32[4,4]{1,0:T(4,128)} %param.23) | copy-start | bytes 196
  23.0 47.1 %copy-start.12 = (f32[512]{0:T(512)S(1)}, f32[512]{0:T(512)}, u32[]{:S(2)}) copy-start(f32[512]{0:T(512)} %param.25) | copy-start | bytes 6148
  23.0 47.1 %copy-start.13 = (f32[8]{0:T(128)S(1)}, f32[8]{0:T(128)}, u32[]{:S(2)}) copy-start(f32[8]{0:T(128)} %param.29) | copy-start | bytes 100
  57.7 27.6 %collective-permute-start.9 = (bf16[6272,128]{1,0:T(8,128)(2,1)S(1)}, bf16[6272,128]{1,0:T(8,128)(2,1)}, u32[]{:S(2)}, u32[]{:S(2)}) collective-permute-start(bf16[6272,128]{1,0:T(8,128)(2,1)S(1)} %bitcast.35), channel_id=1, source_target_pairs={{0,1},{1,0},{2,3},{3,2},{4,5},{5,4},{6,7},{7,6},{8,9},{9,8},{10,11... | collective-permute-start | bytes 4816904 | tf_op jit(solution)/shard_map/ppermute | solution.py:821
  59.3 19.1 %collective-permute-start.4 = (bf16[256,2048]{1,0:T(8,128)(2,1)S(1)}, bf16[256,2048]{1,0:T(8,128)(2,1)}, u32[]{:S(2)}, u32[]{:S(2)}) collective-permute-start(bf16[256,2048]{1,0:T(8,128)(2,1)S(1)} %fusion.2.refs_0_), channel_id=1, source_target_pairs={{0,8},{2,10},{4,12},{6,14},{9,1},{11,3},{13,5},{15,7},{16,24},{18,... | collective-permute-start | bytes 3145736 | tf_op jit(solution)/shard_map/ppermute | solution.py:829
  67.1 17.6 %collective-permute-start.1 = (bf16[256,2048]{1,0:T(8,128)(2,1)S(1)}, bf16[256,2048]{1,0:T(8,128)(2,1)}, u32[]{:S(2)}, u32[]{:S(2)}) collective-permute-start(bf16[256,2048]{1,0:T(8,128)(2,1)S(1)} %fusion.2.refs_0_), channel_id=1, source_target_pairs={{0,2},{2,0},{4,6},{6,4},{9,11},{11,9},{13,15},{15,13},{16,18},{18,... | collective-permute-start | bytes 3145736 | tf_op jit(solution)/shard_map/ppermute | solution.py:835
  70.2 3.7 %collective-permute-start = (f32[5,128]{1,0:T(8,128)S(1)}, f32[5,128]{1,0:T(8,128)S(1)}, u32[]{:S(2)}, u32[]{:S(2)}) collective-permute-start(f32[5,128]{1,0:T(8,128)S(1)} %get-tuple-element.34), channel_id=1, source_target_pairs={{0,1},{1,0},{2,3},{3,2},{4,5},{5,4},{6,7},{7,6},{8,9},{9,8},{10,11... | collective-permute-start | bytes 7688 | tf_op jit(solution)/shard_map/ppermute | solution.py:821
  70.2 22.0 %collective-permute-start.2 = (bf16[256,2048]{1,0:T(8,128)(2,1)S(1)}, bf16[256,2048]{1,0:T(8,128)(2,1)S(1)}, u32[]{:S(2)}, u32[]{:S(2)}) collective-permute-start(bf16[256,2048]{1,0:T(8,128)(2,1)S(1)} %fusion.2.refs_0_), channel_id=1, source_target_pairs={{0,4},{2,6},{4,0},{6,2},{9,13},{11,15},{13,9},{15,11},{16,20},{18,... | collective-permute-start | bytes 3145736 | tf_op jit(solution)/shard_map/ppermute | solution.py:835
  73.9 34.4 %collective-permute-start.3 = (bf16[256,2048]{1,0:T(8,128)(2,1)S(1)}, bf16[256,2048]{1,0:T(8,128)(2,1)S(1)}, u32[]{:S(2)}, u32[]{:S(2)}) collective-permute-start(bf16[256,2048]{1,0:T(8,128)(2,1)S(1)} %fusion.2.refs_0_), channel_id=1, source_target_pairs={{0,6},{2,4},{4,2},{6,0},{9,15},{11,13},{13,11},{15,9},{16,22},{18,... | collective-permute-start | bytes 3145736 | tf_op jit(solution)/shard_map/ppermute | solution.py:835
  78.4 29.9 %collective-permute-start.5 = (bf16[256,2048]{1,0:T(8,128)(2,1)}, bf16[256,2048]{1,0:T(8,128)(2,1)S(1)}, u32[]{:S(2)}, u32[]{:S(2)}) collective-permute-start(bf16[256,2048]{1,0:T(8,128)(2,1)} %collective-permute-done.4.refs_4_), channel_id=1, source_target_pairs={{1,3},{3,1},{5,7},{7,5},{8,10},{10,8},{12,14},{14,12},{17,19},{19,... | collective-permute-start | bytes 3145736 | tf_op jit(solution)/shard_map/ppermute | solution.py:865
  84.7 23.6 %collective-permute-start.6 = (bf16[256,2048]{1,0:T(8,128)(2,1)}, bf16[256,2048]{1,0:T(8,128)(2,1)S(1)}, u32[]{:S(2)}, u32[]{:S(2)}) collective-permute-start(bf16[256,2048]{1,0:T(8,128)(2,1)} %collective-permute-done.4.refs_4_), channel_id=1, source_target_pairs={{1,5},{3,7},{5,1},{7,3},{8,12},{10,14},{12,8},{14,10},{17,21},{19,... | collective-permute-start | bytes 3145736 | tf_op jit(solution)/shard_map/ppermute | solution.py:865
  85.4 22.9 %collective-permute-start.7 = (bf16[256,2048]{1,0:T(8,128)(2,1)}, bf16[256,2048]{1,0:T(8,128)(2,1)S(1)}, u32[]{:S(2)}, u32[]{:S(2)}) collective-permute-start(bf16[256,2048]{1,0:T(8,128)(2,1)} %collective-permute-done.4.refs_4_), channel_id=1, source_target_pairs={{1,7},{3,5},{5,3},{7,1},{8,14},{10,12},{12,10},{14,8},{17,23},{19,... | collective-permute-start | bytes 3145736 | tf_op jit(solution)/shard_map/ppermute | solution.py:865
  108.3 21.3 %copy-start.8 = (bf16[64,1024]{1,0:T(8,128)(2,1)S(1)}, bf16[64,1024]{1,0:T(8,128)(2,1)}, u32[]{:S(2)}) copy-start(bf16[64,1024]{1,0:T(8,128)(2,1)} %param.30) | copy-start | bytes 393220
  108.3 21.3 %copy-start.9 = (bf16[64,1024]{1,0:T(8,128)(2,1)S(1)}, bf16[64,1024]{1,0:T(8,128)(2,1)}, u32[]{:S(2)}) copy-start(bf16[64,1024]{1,0:T(8,128)(2,1)} %param.31) | copy-start | bytes 393220
  116.3 14.4 %collective-permute-start.10 = (f32[2,264,128]{2,1,0:T(8,128)S(1)}, f32[2,264,128]{2,1,0:T(8,128)S(1)}, u32[]{:S(2)}, u32[]{:S(2)}) collective-permute-start(f32[2,264,128]{2,1,0:T(8,128)S(1)} %get-tuple-element.25.own), channel_id=1, source_target_pairs={{0,1},{1,0},{2,3},{3,2},{4,5},{5,4},{6,7},{7,6},{8,9},{9,8},{10,11... | collective-permute-start | bytes 811016 | tf_op jit(solution)/shard_map/ppermute | solution.py:821
  129.6 25.6 %collective-permute-start.14 = (bf16[128,1024]{1,0:T(8,128)(2,1)S(1)}, bf16[128,1024]{1,0:T(8,128)(2,1)S(1)}, u32[]{:S(2)}, u32[]{:S(2)}) collective-permute-start(bf16[128,1024]{1,0:T(8,128)(2,1)S(1)} %pad_maximum_fusion), channel_id=1, source_target_pairs={{0,16},{2,18},{4,20},{6,22},{8,24},{10,26},{12,28},{14,30},{16,0},... | collective-permute-start | bytes 786440 | tf_op jit(solution)/shard_map/ppermute | solution.py:870
  131.3 18.1 %collective-permute-start.11 = (f32[264,128]{1,0:T(8,128)S(1)}, f32[264,128]{1,0:T(8,128)S(1)}, u32[]{:S(2)}, u32[]{:S(2)}) collective-permute-start(f32[264,128]{1,0:T(8,128)S(1)} %shard_map.170), channel_id=1, source_target_pairs={{0,16},{2,18},{4,20},{6,22},{8,24},{10,26},{12,28},{14,30},{16,0},... | collective-permute-start | bytes 405512 | tf_op jit(solution)/shard_map/ppermute | solution.py:929
  155.1 1.6 collective-permute-start.12
  155.2 14.9 %collective-permute-start.15 = (bf16[256,1024]{1,0:T(8,128)(2,1)S(1)}, bf16[256,1024]{1,0:T(8,128)(2,1)S(1)}, u32[]{:S(2)}, u32[]{:S(2)}) collective-permute-start(bf16[256,1024]{1,0:T(8,128)(2,1)S(1)} %constant_dynamic-update-slice_fusion.refs_0_), channel_id=1, source_target_pairs={{0,8},{2,10},{4,12},{6,14},{8,0},{10,2},{12,4},{14,6},{16,24},{18,... | collective-permute-start | bytes 1572872 | tf_op jit(solution)/shard_map/ppermute | solution.py:872
  157.4 18.2 %all-to-all-start.1 = ((bf16[8,272,128]{2,1,0:T(8,128)(2,1)}), bf16[8,272,128]{2,1,0:T(8,128)(2,1)S(1)}, u32[]{:S(2)}, u32[]{:S(2)}) async-start(bf16[8,272,128]{2,1,0:T(8,128)(2,1)} %bitcast.21), calls=%async_computation.1 | async-start | bytes 1114112 | tf_op jit(solution)/shard_map/all_to_all | solution.py:957
  160.9 20.9 %collective-permute-start.16 = (bf16[256,1024]{1,0:T(8,128)(2,1)S(1)}, bf16[256,1024]{1,0:T(8,128)(2,1)S(1)}, u32[]{:S(2)}, u32[]{:S(2)}) collective-permute-start(bf16[256,1024]{1,0:T(8,128)(2,1)S(1)} %constant_dynamic-update-slice_fusion.refs_0_), channel_id=1, source_target_pairs={{0,2},{2,0},{4,6},{6,4},{8,10},{10,8},{12,14},{14,12},{16,18},{18,... | collective-permute-start | bytes 1572872 | tf_op jit(solution)/shard_map/ppermute | solution.py:919
  170.0 16.1 %collective-permute-start.19 = (bf16[256,1024]{1,0:T(8,128)(2,1)S(1)}, bf16[256,1024]{1,0:T(8,128)(2,1)S(1)}, u32[]{:S(2)}, u32[]{:S(2)}) collective-permute-start(bf16[256,1024]{1,0:T(8,128)(2,1)S(1)} %collective-permute-done.15.refs_1_), channel_id=1, source_target_pairs={{0,4},{2,6},{4,0},{6,2},{8,12},{10,14},{12,8},{14,10},{16,20},{18,... | collective-permute-start | bytes 1572872 | tf_op jit(solution)/shard_map/ppermute | solution.py:919
  175.5 32.6 %collective-permute-start.13 = (bf16[2176,128]{1,0:T(8,128)(2,1)S(1)}, bf16[2176,128]{1,0:T(8,128)(2,1)S(1)}, u32[]{:S(2)}, u32[]{:S(2)}) collective-permute-start(bf16[2176,128]{1,0:T(8,128)(2,1)S(1)} %bitcast.36), channel_id=1, source_target_pairs={{0,1},{1,0},{2,3},{3,2},{4,5},{5,4},{6,7},{7,6},{8,9},{9,8},{10,11... | collective-permute-start | bytes 1671176 | tf_op jit(solution)/shard_map/ppermute | solution.py:821
  175.5 21.8 %collective-permute-start.18 = (bf16[256,1024]{1,0:T(8,128)(2,1)S(1)}, bf16[256,1024]{1,0:T(8,128)(2,1)S(1)}, u32[]{:S(2)}, u32[]{:S(2)}) collective-permute-start(bf16[256,1024]{1,0:T(8,128)(2,1)S(1)} %constant_dynamic-update-slice_fusion.refs_0_), channel_id=1, source_target_pairs={{0,4},{2,6},{4,0},{6,2},{8,12},{10,14},{12,8},{14,10},{16,20},{18,... | collective-permute-start | bytes 1572872 | tf_op jit(solution)/shard_map/ppermute | solution.py:919
  176.7 20.6 %collective-permute-start.17 = (bf16[256,1024]{1,0:T(8,128)(2,1)S(1)}, bf16[256,1024]{1,0:T(8,128)(2,1)S(1)}, u32[]{:S(2)}, u32[]{:S(2)}) collective-permute-start(bf16[256,1024]{1,0:T(8,128)(2,1)S(1)} %collective-permute-done.15.refs_1_), channel_id=1, source_target_pairs={{0,2},{2,0},{4,6},{6,4},{8,10},{10,8},{12,14},{14,12},{16,18},{18,... | collective-permute-start | bytes 1572872 | tf_op jit(solution)/shard_map/ppermute | solution.py:919
  181.8 26.4 %collective-permute-start.20 = (bf16[256,1024]{1,0:T(8,128)(2,1)S(1)}, bf16[256,1024]{1,0:T(8,128)(2,1)S(1)}, u32[]{:S(2)}, u32[]{:S(2)}) collective-permute-start(bf16[256,1024]{1,0:T(8,128)(2,1)S(1)} %collective-permute-done.16.refs_2_), channel_id=1, source_target_pairs={{0,4},{2,6},{4,0},{6,2},{8,12},{10,14},{12,8},{14,10},{16,20},{18,... | collective-permute-start | bytes 1572872 | tf_op jit(solution)/shard_map/ppermute | solution.py:919
  186.1 22.1 %collective-permute-start.21 = (bf16[256,1024]{1,0:T(8,128)(2,1)S(1)}, bf16[256,1024]{1,0:T(8,128)(2,1)S(1)}, u32[]{:S(2)}, u32[]{:S(2)}) collective-permute-start(bf16[256,1024]{1,0:T(8,128)(2,1)S(1)} %collective-permute-done.19.refs_5_), channel_id=1, source_target_pairs={{0,2},{2,0},{4,6},{6,4},{8,10},{10,8},{12,14},{14,12},{16,18},{18,... | collective-permute-start | bytes 1572872 | tf_op jit(solution)/shard_map/ppermute | solution.py:919
